TPU v7x, 512 devices: a whole 4x4x16 slice. The times are simulated.
512 devices in a mesh: sp: 64 (over z, y), tp: 8 (over x, core).
Axes of the slice: x: 4, y: 4, z: 16, core: 2. Of those that a mesh axis runs over, the one named last changes fastest.
Arguments:
- queries: bfloat16 [24576, 2048], P('sp', 'tp'), may hold values from -6 to 6
- key_heads: bfloat16 [24576, 1024], P('sp', 'tp'), may hold values from -6 to 6
- value_heads: bfloat16 [24576, 1024], P('sp', 'tp'), may hold values from -6 to 6
- sink_logit: float32 [16], P('tp'), may hold values from 3 to 7
- doc_ids: int32 [24576], replicated, may hold values from 0 to 15, never falling along the last dimension, each value on 1 to 3072 neighbouring positions
- residual: bfloat16 [24576, 2048], P('sp'), may hold values from -6 to 6
- out_proj: bfloat16 [2048, 2048], P('tp'), may hold values from -0.125 to 0.125
- gain_mix: float32 [2048], replicated, may hold values from 0.1 to 1.9
- up_proj: bfloat16 [2048, 8192], P('sp', 'tp'), may hold values from -0.125 to 0.125
- down_proj: bfloat16 [8192, 2048], P('tp', 'sp'), may hold values from -0.0625 to 0.0625
- gain_ffn_in: float32 [2048], replicated, may hold values from 0.1 to 1.9
- gain_ffn_out: float32 [2048], replicated, may hold values from 0.1 to 1.9
Outputs:
- layer_out: bfloat16 [24576, 2048], P(('sp', 'tp'))
All inputs are finite; a program needn't handle non-finite values.
Results may differ from a plain program's by a relative error of at most 0.019.
Values may be sent and summed in bfloat16 or wider, within the bound.
No kernel may reach another device: no remote copies, remote signals or barrier semaphores. Data moves between devices by JAX's collectives and lax.ppermute only.
A program may use at most 64 MiB of HBM per device.

v0:
```python
import jax
import jax.numpy as jnp
from jax import lax
from jax.sharding import PartitionSpec as P

HD = 128
WINDOW = 128


def turned_gather(arrays, axis, dims):
    turned = [jnp.moveaxis(a, dim, 0) for a, dim in zip(arrays, dims)]
    both = jnp.concatenate([t.reshape(len(t), -1) for t in turned], axis=1)
    result, at, gathered = (lax.all_gather(both, axis, axis=0, tiled=True), 0, [])
    for t, dim in zip(turned, dims):
        section = result[:, at : at + t[0].size].reshape(-1, *t.shape[1:])
        gathered.append(jnp.moveaxis(section, 0, dim))
        at += t[0].size
    return tuple(gathered)


def padded(shard, sides, width):
    for axis, dim in sides:
        devices, length = (lax.axis_size(axis), shard.shape[dim])
        up = [(i, (i + 1) % devices) for i in range(devices - 1)]
        down = [(j, i) for i, j in up]
        last = lax.slice_in_dim(shard, length - width, length, axis=dim)
        first = lax.slice_in_dim(shard, 0, width, axis=dim)
        before = lax.ppermute(last, axis, up)
        after = lax.ppermute(first, axis, down)
        shard = jnp.concatenate([before, shard, after], axis=dim)
    return shard


def split_up(shard, dim, devices):
    before, after = (shard.shape[:dim], shard.shape[dim + 1 :])
    return jnp.moveaxis(shard.reshape(*before, devices, -1, *after), dim, 0)


def summed_on_arrival(shard, axis, dim):
    pieces = split_up(shard, dim, lax.axis_size(axis))
    arrived = lax.all_to_all(pieces, axis, split_axis=0, concat_axis=0, tiled=True)
    return arrived.astype(jnp.float32).sum(axis=0)


def joined_along(pieces, dim):
    pieces = jnp.moveaxis(pieces, 0, dim)
    lengths = pieces.shape
    return pieces.reshape(*lengths[:dim], lengths[dim] * lengths[dim + 1], *lengths[dim + 2 :])


def copy_for_each(shard, axis):
    devices = lax.axis_size(axis)
    return lax.all_to_all(
        jnp.broadcast_to(shard[None], (devices, *shard.shape)), axis, 0, 0, tiled=True
    )


def collect(shard, axis, dim):
    return joined_along(copy_for_each(shard, axis), dim)


def rotate(field, places):
    half_dim = HD // 2
    inv_freq = 10000.0 ** (-jnp.arange(0, HD, 2, dtype=jnp.float32) / HD)
    angles = places[:, None, None] * inv_freq[None, None, :]
    cosine = jnp.cos(angles)
    sine = jnp.sin(angles)
    lower = field[..., :half_dim].astype(jnp.float32)
    upper = field[..., half_dim:].astype(jnp.float32)
    return jnp.concatenate(
        [lower * cosine - upper * sine, upper * cosine + lower * sine], axis=-1
    ).astype(jnp.bfloat16)


def banded(field, blocks):
    framed = field.reshape((blocks + 2, WINDOW) + field.shape[1:])
    return jnp.concatenate([framed[:-2], framed[1:-1], framed[2:]], axis=1)


def rms_scale(field, gain_vec):
    return field * lax.rsqrt(jnp.mean(field * field, axis=-1, keepdims=True) + 1e-06) * gain_vec


def body(
    queries,
    key_heads,
    value_heads,
    sink_logit,
    doc_ids,
    residual,
    out_proj,
    gain_mix,
    up_proj,
    down_proj,
    gain_ffn_in,
    gain_ffn_out,
):
    tok_count = queries.shape[0]
    blocks = tok_count // WINDOW
    share_rows = tok_count // lax.axis_size("tp")
    q_local = queries.shape[1] // HD
    kv_local = key_heads.shape[1] // HD
    group_size = q_local // kv_local
    offset = lax.axis_index("sp") * tok_count
    up_whole, down_whole = turned_gather((up_proj, down_proj), "sp", (0, 1))
    places = (offset + jnp.arange(tok_count)).astype(jnp.float32)
    rotated_q = rotate(queries.reshape(tok_count, q_local, HD), places).reshape(
        blocks, WINDOW, kv_local, group_size, HD
    )
    rotated_k = rotate(key_heads.reshape(tok_count, kv_local, HD), places).reshape(
        tok_count, kv_local * HD
    )
    rimmed = padded(jnp.stack([rotated_k, value_heads]), (("sp", 1),), WINDOW)
    key_win = banded(rimmed[0].reshape(-1, kv_local, HD), blocks)
    val_win = banded(rimmed[1].reshape(-1, kv_local, HD), blocks)
    padded_docs = jnp.pad(doc_ids, (WINDOW, WINDOW), constant_values=-1)
    key_docs = banded(lax.dynamic_slice_in_dim(padded_docs, offset, tok_count + 2 * WINDOW), blocks)
    query_docs = lax.dynamic_slice_in_dim(doc_ids, offset, tok_count).reshape(blocks, WINDOW)
    q_index = jnp.arange(WINDOW)[:, None]
    k_index = jnp.arange(3 * WINDOW)[None, :]
    in_window = jnp.abs(k_index - WINDOW - q_index) <= WINDOW
    allowed = (in_window[None] & (query_docs[:, :, None] == key_docs[:, None, :]))[:, None, None]
    scores = jnp.einsum(
        "nqkgd,nskd->nkgqs", rotated_q, key_win, preferred_element_type=jnp.float32
    ) * HD ** (-0.5)
    masked = jnp.where(allowed, scores, -1e30)
    sink_col = sink_logit.reshape(kv_local, group_size)[None, :, :, None]
    top_score = jnp.maximum(jnp.max(masked, axis=-1), sink_col)
    exp_scores = jnp.where(allowed, jnp.exp(masked - top_score[..., None]), 0.0)
    denom_sum = jnp.sum(exp_scores, axis=-1) + jnp.exp(sink_col - top_score)
    probs = (exp_scores / denom_sum[..., None]).astype(jnp.bfloat16)
    attn = (
        jnp.einsum("nkgqs,nskd->nqkgd", probs, val_win, preferred_element_type=jnp.float32)
        .astype(jnp.bfloat16)
        .reshape(tok_count, q_local * HD)
    )
    mixed = summed_on_arrival(
        jnp.dot(attn, out_proj, preferred_element_type=jnp.float32).astype(jnp.bfloat16), "tp", 0
    )
    own_resid = lax.dynamic_slice_in_dim(residual, lax.axis_index("tp") * share_rows, share_rows, 0)
    after_mix = (own_resid.astype(jnp.float32) + rms_scale(mixed, gain_mix)).astype(jnp.bfloat16)
    own_normed = rms_scale(after_mix.astype(jnp.float32), gain_ffn_in).astype(jnp.bfloat16)
    normed = collect(own_normed, "tp", 0)
    up_acts = jnp.dot(normed, up_whole, preferred_element_type=jnp.float32)
    hidden = jnp.square(jax.nn.relu(up_acts)).astype(jnp.bfloat16)
    ffn_out = summed_on_arrival(
        jnp.dot(hidden, down_whole, preferred_element_type=jnp.float32).astype(jnp.bfloat16),
        "tp",
        0,
    )
    return (after_mix.astype(jnp.float32) + rms_scale(ffn_out, gain_ffn_out)).astype(jnp.bfloat16)


def solution(mesh):
    return jax.shard_map(
        body,
        mesh=mesh,
        in_specs=(
            P("sp", "tp"),
            P("sp", "tp"),
            P("sp", "tp"),
            P("tp"),
            P(),
            P("sp", None),
            P("tp", None),
            P(),
            P("sp", "tp"),
            P("tp", "sp"),
            P(),
            P(),
        ),
        out_specs=P(("sp", "tp"), None),
        check_vma=False,
    )
```

profile of v0, /device:TPU:1, one launch (start us, length us, event | category | flops | bytes accessed | tf_op | source)
XLA Modules:
  0.0 213.6 jit_solution(9553838884716437725)
XLA Ops:
  6.5 0.0 copy-start
  6.5 0.0 all-gather.2.cloned.1.call-start
  6.5 1.6 pad_maximum_fusion
  8.2 0.0 all-gather.2.cloned.1.call-update
  8.2 1.8 fusion.41
  10.1 0.0 copy-start.1
  10.1 0.9 pad_maximum_fusion.11
  11.0 4.0 %collective-permute-start = (bf16[2,128,128]{2,1,0:T(8,128)(2,1)S(1)}, bf16[2,128,128]{2,1,0:T(8,128)(2,1)S(1)}, u32[]{:S(2)}, u32[]{:S(2)}) collective-permute-start(bf16[2,128,128]{2,1,0:T(8,128)(2,1)S(1)} %get-tuple-element.15), channel_id=1, source_target_pairs={{0,8},{8,16},{16,24},{24,32},{32,40},{40,48},{48,56},{56,64},{64,7... | collective-permute-start | bytes 196616 | tf_op jit(solution)/shard_map/ppermute | solution.py:28
  15.0 1.3 collective-permute-start.1
  16.3 1.1 copy.26
  17.4 0.1 dynamic-slice_bitcast_fusion
  17.5 0.1 pad_dynamic-slice_fusion
  17.6 0.1 abs_compare_fusion
  17.7 0.4 multiply_cosine_fusion.1
  18.2 0.1 fusion.37
  18.2 0.2 compare_and_fusion
  18.5 0.2 copy.19
  18.7 0.2 copy.20
  18.9 0.1 copy.15
  19.1 0.0 collective-permute-done
  19.1 1.0 collective-permute-done.1
  20.0 0.1 pad_maximum_fusion.8
  20.1 0.0 copy-start.6
  20.2 0.1 copy.14
  20.3 0.1 copy.16
  20.4 0.4 fusion.53
  20.9 0.1 broadcast_maximum_fusion
  20.9 0.3 fusion.14
  21.2 0.1 exponential_add_fusion
  21.3 0.4 fusion.13
  21.7 0.2 copy.22
  21.9 1.8 convolution_convert_fusion
  23.7 8.7 %all-to-all-start = ((bf16[8,48,2048]{2,1,0:T(8,128)(2,1)}), bf16[8,48,2048]{2,1,0:T(8,128)(2,1)S(1)}, u32[]{:S(2)}, u32[]{:S(2)}) async-start(bf16[8,48,2048]{2,1,0:T(8,128)(2,1)} %bitcast.63), calls=%async_computation | async-start | bytes 3145728 | tf_op jit(solution)/shard_map/all_to_all | solution.py:41
  32.5 20.6 %all-to-all-done = bf16[8,48,2048]{2,1,0:T(8,128)(2,1)S(1)} async-done(((bf16[8,48,2048]{2,1,0:T(8,128)(2,1)}), bf16[8,48,2048]{2,1,0:T(8,128)(2,1)S(1)}, u32[]{:S(2)}, u32[]{:S(2)}) %all-to-all-start) | async-done | bytes 1572896 | tf_op jit(solution)/shard_map/all_to_all | solution.py:41
  53.1 0.2 convert_reduce_fusion.1
  53.3 0.1 multiply_reduce_fusion.1
  53.5 1.2 fusion.18
  54.7 0.0 copy-done.5
  54.7 0.1 fusion.20
  54.8 0.2 broadcast_in_dim.23
  55.0 24.0 %all_to_all.15 = bf16[8,48,2048]{2,1,0:T(8,128)(2,1)S(1)} all-to-all(bf16[8,48,2048]{2,1,0:T(8,128)(2,1)S(1)} %broadcast_in_dim.23), channel_id=1, replica_groups=mesh['sp'=64,'tp'=8] {'tp'}, dimensions={0} | all-to-all | bytes 3145728 | tf_op jit(solution)/shard_map/all_to_all | solution.py:53
  79.0 84.9 %all-gather.2.cloned.1.call-done = bf16[2048,2048]{1,0:T(8,128)(2,1)} async-done(((bf16[32,2048]{1,0:T(8,128)(2,1)}), bf16[2048,2048]{1,0:T(8,128)(2,1)}) %all-gather.2.cloned.1.call-update) | async-done | bytes 8388624 | tf_op jit(solution)/shard_map/all_gather | solution.py:13
  163.9 8.1 %fusion.4 = bf16[384,2048]{1,0:T(8,128)(2,1)} fusion(bf16[2048,2048]{1,0:T(8,128)(2,1)} %all-gather.2.cloned.1.call-done, bf16[384,2048]{1,0:T(8,128)(2,1)S(1)} %bitcast.64), kind=kOutput, calls=%fused_computation.6 | convolution fusion | flops 3223191552 | bytes 11534336 | tf_op jit(solution)/shard_map/dot_general | solution.py:147
  172.0 33.2 %all_to_all.16 = bf16[8,48,2048]{2,1,0:T(8,128)(2,1)S(1)} all-to-all(bf16[8,48,2048]{2,1,0:T(8,128)(2,1)} %bitcast.65), channel_id=1, replica_groups=mesh['sp'=64,'tp'=8] {'tp'}, dimensions={0} | all-to-all | bytes 3145728 | tf_op jit(solution)/shard_map/all_to_all | solution.py:41
  205.2 0.2 convert_reduce_fusion
  205.5 0.1 multiply_reduce_fusion
  205.6 0.3 copy-done.4
  205.9 0.8 fusion.21
  (19 shorter events, 0.1 us)
Async XLA Ops:
  6.5 15.4 %copy-start = (bf16[256,2048]{1,0:T(8,128)(2,1)S(1)}, bf16[256,2048]{1,0:T(8,128)(2,1)}, u32[]{:S(2)}) copy-start(bf16[256,2048]{1,0:T(8,128)(2,1)} %param.18) | copy-start | bytes 3145732
  6.5 10.9 %copy-start.2 = (s32[24576]{0:T(1024)S(1)}, s32[24576]{0:T(1024)}, u32[]{:S(2)}) copy-start(s32[24576]{0:T(1024)} %param.16) | copy-start | bytes 294916
  6.5 157.3 %all-gather.2.cloned.1.call-start = ((), (), s32[]{:S(2)}) async-start(), calls=%async_computation.3 | async-start | bytes 8519680 | tf_op jit(solution)/shard_map/all_gather | solution.py:13
  10.1 8.9 %copy-start.1 = (bf16[384,128]{1,0:T(8,128)(2,1)S(1)}, bf16[384,128]{1,0:T(8,128)(2,1)}, u32[]{:S(2)}) copy-start(bf16[384,128]{1,0:T(8,128)(2,1)} %param.14) | copy-start | bytes 294916
  11.0 8.1 %collective-permute-start = (bf16[2,128,128]{2,1,0:T(8,128)(2,1)S(1)}, bf16[2,128,128]{2,1,0:T(8,128)(2,1)S(1)}, u32[]{:S(2)}, u32[]{:S(2)}) collective-permute-start(bf16[2,128,128]{2,1,0:T(8,128)(2,1)S(1)} %get-tuple-element.15), channel_id=1, source_target_pairs={{0,8},{8,16},{16,24},{24,32},{32,40},{40,48},{48,56},{56,64},{64,7... | collective-permute-start | bytes 196616 | tf_op jit(solution)/shard_map/ppermute | solution.py:28
  15.0 5.0 %collective-permute-start.1 = (bf16[2,128,128]{2,1,0:T(8,128)(2,1)S(1)}, bf16[2,128,128]{2,1,0:T(8,128)(2,1)S(1)}, u32[]{:S(2)}, u32[]{:S(2)}) collective-permute-start(bf16[2,128,128]{2,1,0:T(8,128)(2,1)S(1)} %get-tuple-element.16), channel_id=1, source_target_pairs={{8,0},{16,8},{24,16},{32,24},{40,32},{48,40},{56,48},{64,56},{72,6... | collective-permute-start | bytes 196616 | tf_op jit(solution)/shard_map/ppermute | solution.py:29
  20.1 0.7 copy-start.6
  23.7 29.4 %all-to-all-start = ((bf16[8,48,2048]{2,1,0:T(8,128)(2,1)}), bf16[8,48,2048]{2,1,0:T(8,128)(2,1)S(1)}, u32[]{:S(2)}, u32[]{:S(2)}) async-start(bf16[8,48,2048]{2,1,0:T(8,128)(2,1)} %bitcast.63), calls=%async_computation | async-start | bytes 3145728 | tf_op jit(solution)/shard_map/all_to_all | solution.py:41
  32.5 21.0 %copy-start.3 = (f32[2048]{0:T(1024)S(1)}, f32[2048]{0:T(1024)}, u32[]{:S(2)}) copy-start(f32[2048]{0:T(1024)} %param.19) | copy-start | bytes 24580
  32.5 22.2 %copy-start.5 = (f32[2048]{0:T(1024)S(1)}, f32[2048]{0:T(1024)}, u32[]{:S(2)}) copy-start(f32[2048]{0:T(1024)} %param.22) | copy-start | bytes 24580
  205.2 0.7 copy-start.4
Sparse Core Ops, SparseCore 0:
  10.3 153.5 all-gather.1
where the time goes:
time: 214 us
  waiting for transfers between devices  106 us (50%)
  blocking collectives  57.2 us (27%)
  starting transfers between devices  14.1 us (7%)
  between operations  13.6 us (6%)
  matrix products  10.8 us (5%)
  other arithmetic  8.61 us (4%)
  local copies, waits for them, and re-layouts  2.78 us (1%)
    all_gather x1, waiting for transfers between devices, turned_gather(): lax.all_gather(both, axis, axis=0, tiled=True)  84.9 us
    all_to_all x1, blocking collectives, summed_on_arrival(): lax.all_to_all(pieces, axis, split_axis=0, concat_axis=0, tiled=True)  33.2 us
    all_to_all x1, blocking collectives, copy_for_each(): lax.all_to_all(jnp.broadcast_to(shard[None], (devices, *shard.shape)), ax...  24 us
    all_to_all x1, waiting for transfers between devices, summed_on_arrival(): lax.all_to_all(pieces, axis, split_axis=0, concat_axis=0, tiled=True)  20.6 us
    all_to_all x1, starting transfers between devices, summed_on_arrival(): lax.all_to_all(pieces, axis, split_axis=0, concat_axis=0, tiled=True)  8.74 us
    dot_general x1, matrix products, body(): jnp.dot(hidden, down_whole, preferred_element_type=jnp.float32)  8.11 us
  transfers between devices with their start and end apart: 4, of which 3 were waited for; matrix products, arithmetic and copies ran while one was open for 5% of the time, Pallas kernels for 0%

commit v1 on v0

--- a/solution.py
+++ b/solution.py
@@ -7,15 +7,30 @@
 WINDOW = 128
 
 
-def turned_gather(arrays, axis, dims):
-    turned = [jnp.moveaxis(a, dim, 0) for a, dim in zip(arrays, dims)]
-    both = jnp.concatenate([t.reshape(len(t), -1) for t in turned], axis=1)
-    result, at, gathered = (lax.all_gather(both, axis, axis=0, tiled=True), 0, [])
-    for t, dim in zip(turned, dims):
-        section = result[:, at : at + t[0].size].reshape(-1, *t.shape[1:])
-        gathered.append(jnp.moveaxis(section, 0, dim))
-        at += t[0].size
-    return tuple(gathered)
+def device(z, y, x, core):
+    return (4 * z + y) * 8 + 2 * x + core
+
+
+def group_weights(up_proj, down_proj):
+    columns = [w.reshape(32, 4, 256).swapaxes(0, 1) for w in (up_proj, down_proj.T)]
+    along_y = [[4 * z + y for y in range(4)] for z in range(16)]
+    along_z = [[4 * z + y for z in range(16)] for y in range(4)]
+    rows = lax.all_to_all(
+        jnp.concatenate(columns, axis=2), "sp", 0, 0, axis_index_groups=along_y, tiled=True
+    )
+    own = lax.all_gather(
+        rows.reshape(128, 512), "sp", axis=0, tiled=True, axis_index_groups=along_z
+    )
+    return own, lax.ppermute(own, "tp", [(i, i ^ 1) for i in range(8)])
+
+
+def exchanged(pieces):
+    groups = [
+        [device(z, y, x, core) for y in range(4) for x in range(4)]
+        for z in range(16)
+        for core in range(2)
+    ]
+    return lax.all_to_all(pieces, ("sp", "tp"), 0, 0, axis_index_groups=groups, tiled=True)
 
 
 def padded(shard, sides, width):
@@ -40,23 +55,6 @@
     pieces = split_up(shard, dim, lax.axis_size(axis))
     arrived = lax.all_to_all(pieces, axis, split_axis=0, concat_axis=0, tiled=True)
     return arrived.astype(jnp.float32).sum(axis=0)
-
-
-def joined_along(pieces, dim):
-    pieces = jnp.moveaxis(pieces, 0, dim)
-    lengths = pieces.shape
-    return pieces.reshape(*lengths[:dim], lengths[dim] * lengths[dim + 1], *lengths[dim + 2 :])
-
-
-def copy_for_each(shard, axis):
-    devices = lax.axis_size(axis)
-    return lax.all_to_all(
-        jnp.broadcast_to(shard[None], (devices, *shard.shape)), axis, 0, 0, tiled=True
-    )
-
-
-def collect(shard, axis, dim):
-    return joined_along(copy_for_each(shard, axis), dim)
 
 
 def rotate(field, places):
@@ -102,7 +100,7 @@
     kv_local = key_heads.shape[1] // HD
     group_size = q_local // kv_local
     offset = lax.axis_index("sp") * tok_count
-    up_whole, down_whole = turned_gather((up_proj, down_proj), "sp", (0, 1))
+    weights = group_weights(up_proj, down_proj)
     places = (offset + jnp.arange(tok_count)).astype(jnp.float32)
     rotated_q = rotate(queries.reshape(tok_count, q_local, HD), places).reshape(
         blocks, WINDOW, kv_local, group_size, HD
@@ -134,20 +132,23 @@
         .astype(jnp.bfloat16)
         .reshape(tok_count, q_local * HD)
     )
-    mixed = summed_on_arrival(
-        jnp.dot(attn, out_proj, preferred_element_type=jnp.float32).astype(jnp.bfloat16), "tp", 0
-    )
+    partial_mix = jnp.dot(attn, out_proj, preferred_element_type=jnp.float32).astype(jnp.bfloat16)
+    mixed = summed_on_arrival(partial_mix, "tp", 0)
     own_resid = lax.dynamic_slice_in_dim(residual, lax.axis_index("tp") * share_rows, share_rows, 0)
     after_mix = (own_resid.astype(jnp.float32) + rms_scale(mixed, gain_mix)).astype(jnp.bfloat16)
     own_normed = rms_scale(after_mix.astype(jnp.float32), gain_ffn_in).astype(jnp.bfloat16)
-    normed = collect(own_normed, "tp", 0)
-    up_acts = jnp.dot(normed, up_whole, preferred_element_type=jnp.float32)
-    hidden = jnp.square(jax.nn.relu(up_acts)).astype(jnp.bfloat16)
-    ffn_out = summed_on_arrival(
-        jnp.dot(hidden, down_whole, preferred_element_type=jnp.float32).astype(jnp.bfloat16),
-        "tp",
-        0,
-    )
+    normed = exchanged(jnp.broadcast_to(own_normed[None], (16, *own_normed.shape)))
+    normed = normed.reshape(-1, 2048)
+    across = (((1,), (1,)), ((), ()))
+    ffn_part = 0.0
+    for both in weights:
+        up_acts = jnp.dot(normed, both[:, :256], preferred_element_type=jnp.float32)
+        hidden = jnp.square(jax.nn.relu(up_acts)).astype(jnp.bfloat16)
+        ffn_part += lax.dot_general(
+            hidden, both[:, 256:], across, preferred_element_type=jnp.float32
+        )
+    arrived = exchanged(ffn_part.astype(jnp.bfloat16).reshape(16, -1, 2048))
+    ffn_out = arrived.astype(jnp.float32).sum(axis=0)
     return (after_mix.astype(jnp.float32) + rms_scale(ffn_out, gain_ffn_out)).astype(jnp.bfloat16)
 
 

time: 214 us -> 192 us (0.90)
  waiting for transfers between devices: 106 us -> 62.1 us
  starting transfers between devices: 14.1 us -> 36.5 us
  blocking collectives: 57.2 us -> 45.9 us
  matrix products: 10.8 us -> 19.8 us
  local copies, waits for them, and re-layouts: 2.78 us -> 5.92 us
    all_gather x1, waiting for transfers between devices: 84.9 us -> 39.7 us  [group_weights(): lax.all_gather(rows.reshape(128, 512), 'sp', axis=0, tiled=True, axis_ind...]
    all_to_all x2 -> x1, blocking collectives: 57.2 us -> 45.9 us  [exchanged(): lax.all_to_all(pieces, ('sp', 'tp'), 0, 0, axis_index_groups=groups, tile...]
    ppermute x0 -> x1, starting transfers between devices: none -> 11.3 us  [group_weights(): return (own, lax.ppermute(own, 'tp', [(i, i ^ 1) for i in range(8)]))]
    all_to_all x0 -> x2, starting transfers between devices: none -> 10.1 us  [the longest x1 5.06 us: exchanged(): lax.all_to_all(pieces, ('sp', 'tp'), 0, 0, axis_index_groups=groups, tile...]
    dot_general x1 -> x2, matrix products: 8.11 us -> 17.2 us  [body(): lax.dot_general(hidden, both[:, 256:], across, preferred_element_type=jnp...]
  transfers between devices with their start and end apart: 4 -> 7, of which waited for: 3 -> 3; matrix products, arithmetic and copies ran while one was open for 5% -> 11% of each run, Pallas kernels for 0% -> 0%
where the time goes in v1:
time: 192 us; the launch traced here: 191 us
  waiting for transfers between devices  62.1 us (32%)
  blocking collectives  45.9 us (24%)
  starting transfers between devices  36.5 us (19%)
  matrix products  19.8 us (10%)
  between operations  13.7 us (7%)
  other arithmetic  7.37 us (4%)
  local copies, waits for them, and re-layouts  5.92 us (3%)
    all_to_all x1, blocking collectives, exchanged(): lax.all_to_all(pieces, ('sp', 'tp'), 0, 0, axis_index_groups=groups, tile...  45.9 us
    all_gather x1, waiting for transfers between devices, group_weights(): lax.all_gather(rows.reshape(128, 512), 'sp', axis=0, tiled=True, axis_ind...  39.7 us
    all_to_all x1, waiting for transfers between devices, summed_on_arrival(): lax.all_to_all(pieces, axis, split_axis=0, concat_axis=0, tiled=True)  19.9 us
    dot_general x2, matrix products, body(): lax.dot_general(hidden, both[:, 256:], across, preferred_element_type=jnp...  17.2 us
    ppermute x1, starting transfers between devices, group_weights(): return (own, lax.ppermute(own, 'tp', [(i, i ^ 1) for i in range(8)]))  11.3 us
    all_to_all x1, starting transfers between devices, summed_on_arrival(): lax.all_to_all(pieces, axis, split_axis=0, concat_axis=0, tiled=True)  10.4 us
    all_to_all x1, starting transfers between devices, exchanged(): lax.all_to_all(pieces, ('sp', 'tp'), 0, 0, axis_index_groups=groups, tile...  5.06 us
    all_to_all x1, starting transfers between devices, group_weights(): lax.all_to_all(jnp.concatenate(columns, axis=2), 'sp', 0, 0, axis_index_g...  5 us
  transfers between devices with their start and end apart: 7, of which 3 were waited for; matrix products, arithmetic and copies ran while one was open for 11% of the time, Pallas kernels for 0%

profile of v1, /device:TPU:1, one launch (start us, length us, event | category | flops | bytes accessed | tf_op | source)
XLA Modules:
  0.0 191.3 jit_solution(8508207204269369890)
XLA Ops:
  6.5 1.0 reshape.363
  7.5 0.9 reshape.364
  8.4 0.1 pad_maximum_fusion
  8.5 0.7 copy.42
  9.2 5.0 %all-to-all-start.2 = ((bf16[4,32,512]{2,1,0:T(8,128)(2,1)}), bf16[4,32,512]{2,1,0:T(8,128)(2,1)S(1)}, u32[]{:S(2)}, u32[]{:S(2)}) async-start(bf16[4,32,512]{2,1,0:T(8,128)(2,1)} %copy.42), calls=%async_computation.2 | async-start | bytes 262144 | tf_op jit(solution)/shard_map/all_to_all | solution.py:18
  14.2 1.8 fusion.43
  16.0 0.9 pad_maximum_fusion.11
  16.9 3.4 %collective-permute-start = (bf16[2,128,128]{2,1,0:T(8,128)(2,1)S(1)}, bf16[2,128,128]{2,1,0:T(8,128)(2,1)S(1)}, u32[]{:S(2)}, u32[]{:S(2)}) collective-permute-start(bf16[2,128,128]{2,1,0:T(8,128)(2,1)S(1)} %get-tuple-element.15), channel_id=1, source_target_pairs={{0,8},{8,16},{16,24},{24,32},{32,40},{40,48},{48,56},{56,64},{64,7... | collective-permute-start | bytes 196616 | tf_op jit(solution)/shard_map/ppermute | solution.py:43
  20.3 1.3 collective-permute-start.1
  21.6 0.4 multiply_cosine_fusion.1
  22.0 0.1 dynamic-slice_bitcast_fusion
  22.1 0.1 pad_dynamic-slice_fusion
  22.2 0.1 abs_compare_fusion
  22.3 0.2 copy.46
  22.5 0.1 fusion.39
  22.6 0.2 compare_and_fusion
  22.8 0.1 copy.34
  23.0 0.2 copy.38
  23.2 0.2 copy.39
  23.4 0.0 copy-start.8
  23.4 1.9 collective-permute-done.1
  25.3 0.1 pad_maximum_fusion.8
  25.4 0.1 copy.33
  25.5 0.1 copy.35
  25.7 0.4 fusion.56
  26.1 0.1 broadcast_maximum_fusion
  26.2 0.3 fusion.13
  26.4 0.1 exponential_add_fusion
  26.5 0.4 fusion.7
  26.9 0.2 copy.41
  27.1 1.7 convolution_convert_fusion
  28.9 10.4 %all-to-all-start = ((bf16[8,48,2048]{2,1,0:T(8,128)(2,1)}), bf16[8,48,2048]{2,1,0:T(8,128)(2,1)S(1)}, u32[]{:S(2)}, u32[]{:S(2)}) async-start(bf16[8,48,2048]{2,1,0:T(8,128)(2,1)} %bitcast.26), calls=%async_computation | async-start | bytes 3145728 | tf_op jit(solution)/shard_map/all_to_all | solution.py:56
  39.3 0.7 all-gather.2.cloned.1.call-update
  40.0 19.9 %all-to-all-done = bf16[8,48,2048]{2,1,0:T(8,128)(2,1)S(1)} async-done(((bf16[8,48,2048]{2,1,0:T(8,128)(2,1)}), bf16[8,48,2048]{2,1,0:T(8,128)(2,1)S(1)}, u32[]{:S(2)}, u32[]{:S(2)}) %all-to-all-start) | async-done | bytes 1572896 | tf_op jit(solution)/shard_map/all_to_all | solution.py:56
  59.9 0.2 convert_reduce_fusion.1
  60.2 0.1 multiply_reduce_fusion.1
  60.3 1.2 fusion.18
  61.5 0.1 fusion.20
  61.7 2.0 %broadcast_in_dim.23 = bf16[16,48,2048]{2,1,0:T(8,128)(2,1)} broadcast(bf16[48,2048]{1,0:T(8,128)(2,1)S(1)} %fusion.20), dimensions={1,2} | broadcast | bytes 3342336 | tf_op jit(solution)/shard_map/broadcast_in_dim | solution.py:140
  63.7 5.1 %all-to-all-start.1 = ((bf16[16,48,2048]{2,1,0:T(8,128)(2,1)}), bf16[16,48,2048]{2,1,0:T(8,128)(2,1)}, u32[]{:S(2)}, u32[]{:S(2)}) async-start(bf16[16,48,2048]{2,1,0:T(8,128)(2,1)} %broadcast_in_dim.23), calls=%async_computation.1 | async-start | bytes 6291456 | tf_op jit(solution)/shard_map/all_to_all | solution.py:33
  68.8 39.7 %all-gather.2.cloned.1.call-done = bf16[2048,512]{1,0:T(8,128)(2,1)} async-done(((bf16[128,512]{1,0:T(8,128)(2,1)}), bf16[2048,512]{1,0:T(8,128)(2,1)}) %all-gather.2.cloned.1.call-update) | async-done | bytes 2097168 | tf_op jit(solution)/shard_map/all_gather | solution.py:21
  108.4 11.3 %collective-permute-start.2 = (bf16[2048,512]{1,0:T(8,128)(2,1)}, bf16[2048,512]{1,0:T(8,128)(2,1)S(1)}, u32[]{:S(2)}, u32[]{:S(2)}) collective-permute-start(bf16[2048,512]{1,0:T(8,128)(2,1)} %all-gather.2.cloned.1.call-done), channel_id=1, source_target_pairs={{0,1},{1,0},{2,3},{3,2},{4,5},{5,4},{6,7},{7,6},{8,9},{9,8},{10,11... | collective-permute-start | bytes 6291464 | tf_op jit(solution)/shard_map/ppermute | solution.py:24
  119.8 8.5 %fusion.5 = f32[768,2048]{1,0:T(8,128)} fusion(bf16[768,2048]{1,0:T(8,128)(2,1)} %bitcast.27, bf16[2048,512]{1,0:T(8,128)(2,1)} %all-gather.2.cloned.1.call-done), kind=kOutput, calls=%fused_computation.12 | convolution fusion | flops 1611202560 | bytes 11534336 | tf_op jit(solution)/shard_map/dot_general | solution.py:147
  128.2 8.7 %add_convert_fusion = bf16[768,2048]{1,0:T(8,128)(2,1)} fusion(f32[768,2048]{1,0:T(8,128)} %fusion.5, bf16[2048,512]{1,0:T(8,128)(2,1)S(1)} %collective-permute-done.2, bf16[768,2048]{1,0:T(8,128)(2,1)} %bitcast.27), kind=kOutput, calls=%fused_computation.1 | convolution fusion | flops 1614348288 | bytes 14680064 | tf_op jit(solution)/shard_map/dot_general | solution.py:147
  137.0 45.9 %all_to_all.20 = bf16[16,48,2048]{2,1,0:T(8,128)(2,1)S(1)} all-to-all(bf16[16,48,2048]{2,1,0:T(8,128)(2,1)} %bitcast.67), channel_id=1, replica_groups={{0,2,4,6,8,10,12,14,16,18,20,22,24,26,28,30},{1,3,5,7,9,11,13,15,17,19,..., dimensions={0} | all-to-all | bytes 6291456 | tf_op jit(solution)/shard_map/all_to_all | solution.py:33
  182.9 0.6 convert_reduce_fusion
  183.5 0.1 multiply_reduce_fusion
  183.6 0.8 fusion.21
  (32 shorter events, 0.2 us)
Async XLA Ops:
  6.5 20.6 %copy-start = (bf16[256,2048]{1,0:T(8,128)(2,1)S(1)}, bf16[256,2048]{1,0:T(8,128)(2,1)}, u32[]{:S(2)}) copy-start(bf16[256,2048]{1,0:T(8,128)(2,1)} %param.18) | copy-start | bytes 3145732
  6.5 16.3 %copy-start.1 = (bf16[384,128]{1,0:T(8,128)(2,1)S(1)}, bf16[384,128]{1,0:T(8,128)(2,1)}, u32[]{:S(2)}) copy-start(bf16[384,128]{1,0:T(8,128)(2,1)} %param.14) | copy-start | bytes 294916
  6.5 15.5 %copy-start.4 = (s32[24576]{0:T(1024)S(1)}, s32[24576]{0:T(1024)}, u32[]{:S(2)}) copy-start(s32[24576]{0:T(1024)} %param.16) | copy-start | bytes 294916
  6.5 15.8 %copy-start.3 = (bf16[384,256]{1,0:T(8,128)(2,1)S(1)}, bf16[384,256]{1,0:T(8,128)(2,1)}, u32[]{:S(2)}) copy-start(bf16[384,256]{1,0:T(8,128)(2,1)} %param.12) | copy-start | bytes 589828
  9.2 19.7 %all-to-all-start.2 = ((bf16[4,32,512]{2,1,0:T(8,128)(2,1)}), bf16[4,32,512]{2,1,0:T(8,128)(2,1)S(1)}, u32[]{:S(2)}, u32[]{:S(2)}) async-start(bf16[4,32,512]{2,1,0:T(8,128)(2,1)} %copy.42), calls=%async_computation.2 | async-start | bytes 262144 | tf_op jit(solution)/shard_map/all_to_all | solution.py:18
  16.9 6.5 %collective-permute-start = (bf16[2,128,128]{2,1,0:T(8,128)(2,1)S(1)}, bf16[2,128,128]{2,1,0:T(8,128)(2,1)S(1)}, u32[]{:S(2)}, u32[]{:S(2)}) collective-permute-start(bf16[2,128,128]{2,1,0:T(8,128)(2,1)S(1)} %get-tuple-element.15), channel_id=1, source_target_pairs={{0,8},{8,16},{16,24},{24,32},{32,40},{40,48},{48,56},{56,64},{64,7... | collective-permute-start | bytes 196616 | tf_op jit(solution)/shard_map/ppermute | solution.py:43
  20.3 5.0 %collective-permute-start.1 = (bf16[2,128,128]{2,1,0:T(8,128)(2,1)S(1)}, bf16[2,128,128]{2,1,0:T(8,128)(2,1)S(1)}, u32[]{:S(2)}, u32[]{:S(2)}) collective-permute-start(bf16[2,128,128]{2,1,0:T(8,128)(2,1)S(1)} %get-tuple-element.16), channel_id=1, source_target_pairs={{8,0},{16,8},{24,16},{32,24},{40,32},{48,40},{56,48},{64,56},{72,6... | collective-permute-start | bytes 196616 | tf_op jit(solution)/shard_map/ppermute | solution.py:44
  23.4 2.7 %copy-start.8 = (f32[2]{0:T(128)S(1)}, f32[2]{0:T(128)}, u32[]{:S(2)}) copy-start(f32[2]{0:T(128)} %param.15) | copy-start | bytes 28
  28.9 10.5 %copy-start.2 = (bf16[4,32,512]{2,1,0:T(8,128)(2,1)}, bf16[4,32,512]{2,1,0:T(8,128)(2,1)S(1)}, u32[]{:S(2)}) copy-start(bf16[4,32,512]{2,1,0:T(8,128)(2,1)S(1)} %all-to-all-done.2) | copy-start | bytes 393220
  28.9 31.4 %copy-start.5 = (f32[2048]{0:T(1024)S(1)}, f32[2048]{0:T(1024)}, u32[]{:S(2)}) copy-start(f32[2048]{0:T(1024)} %param.19) | copy-start | bytes 24580
  28.9 31.1 %all-to-all-start = ((bf16[8,48,2048]{2,1,0:T(8,128)(2,1)}), bf16[8,48,2048]{2,1,0:T(8,128)(2,1)S(1)}, u32[]{:S(2)}, u32[]{:S(2)}) async-start(bf16[8,48,2048]{2,1,0:T(8,128)(2,1)} %bitcast.26), calls=%async_computation | async-start | bytes 3145728 | tf_op jit(solution)/shard_map/all_to_all | solution.py:56
  39.3 22.2 %copy-start.7 = (f32[2048]{0:T(1024)S(1)}, f32[2048]{0:T(1024)}, u32[]{:S(2)}) copy-start(f32[2048]{0:T(1024)} %param.22) | copy-start | bytes 24580
  39.3 69.1 %all-gather.2.cloned.1.call-start = ((), (), s32[]{:S(2)}) async-start(), calls=%async_computation.4 | async-start | bytes 2228224 | tf_op jit(solution)/shard_map/all_gather | solution.py:21
  63.7 56.0 %all-to-all-start.1 = ((bf16[16,48,2048]{2,1,0:T(8,128)(2,1)}), bf16[16,48,2048]{2,1,0:T(8,128)(2,1)}, u32[]{:S(2)}, u32[]{:S(2)}) async-start(bf16[16,48,2048]{2,1,0:T(8,128)(2,1)} %broadcast_in_dim.23), calls=%async_computation.1 | async-start | bytes 6291456 | tf_op jit(solution)/shard_map/all_to_all | solution.py:33
  108.4 19.8 %collective-permute-start.2 = (bf16[2048,512]{1,0:T(8,128)(2,1)}, bf16[2048,512]{1,0:T(8,128)(2,1)S(1)}, u32[]{:S(2)}, u32[]{:S(2)}) collective-permute-start(bf16[2048,512]{1,0:T(8,128)(2,1)} %all-gather.2.cloned.1.call-done), channel_id=1, source_target_pairs={{0,1},{1,0},{2,3},{3,2},{4,5},{5,4},{6,7},{7,6},{8,9},{9,8},{10,11... | collective-permute-start | bytes 6291464 | tf_op jit(solution)/shard_map/ppermute | solution.py:24
  182.8 0.7 copy-start.6
Sparse Core Ops, SparseCore 0:
  42.2 66.1 all-gather.1

commit v2 on v1

--- a/solution.py
+++ b/solution.py
@@ -1,3 +1,5 @@
+import itertools
+
 import jax
 import jax.numpy as jnp
 from jax import lax
@@ -11,26 +13,46 @@
     return (4 * z + y) * 8 + 2 * x + core
 
 
-def group_weights(up_proj, down_proj):
-    columns = [w.reshape(32, 4, 256).swapaxes(0, 1) for w in (up_proj, down_proj.T)]
-    along_y = [[4 * z + y for y in range(4)] for z in range(16)]
-    along_z = [[4 * z + y for z in range(16)] for y in range(4)]
-    rows = lax.all_to_all(
-        jnp.concatenate(columns, axis=2), "sp", 0, 0, axis_index_groups=along_y, tiled=True
-    )
-    own = lax.all_gather(
-        rows.reshape(128, 512), "sp", axis=0, tiled=True, axis_index_groups=along_z
-    )
-    return own, lax.ppermute(own, "tp", [(i, i ^ 1) for i in range(8)])
-
-
-def exchanged(pieces):
-    groups = [
-        [device(z, y, x, core) for y in range(4) for x in range(4)]
+def dealt(shard, turn):
+    pairs = []
+    for z, y, x, core in itertools.product(range(16), range(4), range(4), range(2)):
+        target = core + 2 * ((y // 2 + turn) % 2)
+        pairs.append((device(z, y, x, core), device(z, target, x, y % 2)))
+    return lax.ppermute(shard, ("sp", "tp"), pairs)
+
+
+def swapped(shard):
+    return lax.ppermute(shard, "tp", [(i, i ^ 1) for i in range(8)])
+
+
+def token_groups():
+    return [
+        [device(z, 2 * q + par, x, core) for par in range(2) for x in range(4)]
         for z in range(16)
+        for q in range(2)
         for core in range(2)
     ]
-    return lax.all_to_all(pieces, ("sp", "tp"), 0, 0, axis_index_groups=groups, tiled=True)
+
+
+def exchanged(pieces):
+    return lax.all_to_all(
+        pieces, ("sp", "tp"), 0, 0, axis_index_groups=token_groups(), tiled=True
+    )
+
+
+def halves(field, core):
+    first, second = (field[:, 0], field[:, 1])
+    return jnp.where(core == 0, first, second), jnp.where(core == 0, second, first)
+
+
+def group_weights(up_proj, down_proj):
+    both = jnp.concatenate([up_proj, down_proj.T], axis=1)
+    same, other = (dealt(both, 0), dealt(both, 1))
+    low = (lax.axis_index("sp") // 2) % 2 == 0
+    rows = jnp.concatenate([jnp.where(low, same, other), jnp.where(low, other, same)], axis=0)
+    along_z = [[4 * z + y for z in range(16)] for y in range(4)]
+    own = lax.all_gather(rows, "sp", axis=0, tiled=True, axis_index_groups=along_z)
+    return own, swapped(own)
 
 
 def padded(shard, sides, width):
@@ -100,7 +122,8 @@
     kv_local = key_heads.shape[1] // HD
     group_size = q_local // kv_local
     offset = lax.axis_index("sp") * tok_count
-    weights = group_weights(up_proj, down_proj)
+    own, other = group_weights(up_proj, down_proj)
+    core = lax.axis_index("tp") % 2
     places = (offset + jnp.arange(tok_count)).astype(jnp.float32)
     rotated_q = rotate(queries.reshape(tok_count, q_local, HD), places).reshape(
         blocks, WINDOW, kv_local, group_size, HD
@@ -137,18 +160,23 @@
     own_resid = lax.dynamic_slice_in_dim(residual, lax.axis_index("tp") * share_rows, share_rows, 0)
     after_mix = (own_resid.astype(jnp.float32) + rms_scale(mixed, gain_mix)).astype(jnp.bfloat16)
     own_normed = rms_scale(after_mix.astype(jnp.float32), gain_ffn_in).astype(jnp.bfloat16)
-    normed = exchanged(jnp.broadcast_to(own_normed[None], (16, *own_normed.shape)))
+    first, second = halves(own_normed.reshape(-1, 32, 2, 32).swapaxes(1, 2), core)
+    ordered = jnp.concatenate([first.reshape(-1, 1024), second.reshape(-1, 1024)], axis=1)
+    normed = exchanged(jnp.broadcast_to(ordered[None], (8, *ordered.shape)))
     normed = normed.reshape(-1, 2048)
+    up_acts = jnp.dot(normed[:, :1024], own[:, :1024], preferred_element_type=jnp.float32)
+    up_acts += jnp.dot(normed[:, 1024:], other[:, :1024], preferred_element_type=jnp.float32)
+    hidden = jnp.square(jax.nn.relu(up_acts)).astype(jnp.bfloat16)
     across = (((1,), (1,)), ((), ()))
-    ffn_part = 0.0
-    for both in weights:
-        up_acts = jnp.dot(normed, both[:, :256], preferred_element_type=jnp.float32)
-        hidden = jnp.square(jax.nn.relu(up_acts)).astype(jnp.bfloat16)
-        ffn_part += lax.dot_general(
-            hidden, both[:, 256:], across, preferred_element_type=jnp.float32
+    parts = [
+        lax.dot_general(hidden, w[:, 1024:], across, preferred_element_type=jnp.float32).astype(
+            jnp.bfloat16
         )
-    arrived = exchanged(ffn_part.astype(jnp.bfloat16).reshape(16, -1, 2048))
-    ffn_out = arrived.astype(jnp.float32).sum(axis=0)
+        for w in (own, other)
+    ]
+    arrived = exchanged(jnp.concatenate(parts, axis=1).reshape(8, -1, 2048))
+    summed = arrived.astype(jnp.float32).sum(axis=0).reshape(-1, 2, 32, 32)
+    ffn_out = jnp.stack(halves(summed, core), axis=2).reshape(-1, 2048)
     return (after_mix.astype(jnp.float32) + rms_scale(ffn_out, gain_ffn_out)).astype(jnp.bfloat16)
 
 

time: 192 us -> 172 us (0.90)
  matrix products: 19.8 us -> 9.97 us
  starting transfers between devices: 36.5 us -> 29.4 us
  waiting for transfers between devices: 62.1 us -> 58.8 us
  blocking collectives: 45.9 us -> 49 us
  local copies, waits for them, and re-layouts: 5.92 us -> 3.16 us
    all_to_all x1, waiting for transfers between devices: 19.9 us -> 0.01 us  [summed_on_arrival(): lax.all_to_all(pieces, axis, split_axis=0, concat_axis=0, tiled=True)]
    all_gather x1, waiting for transfers between devices: 39.7 us -> 52.5 us  [group_weights(): lax.all_gather(rows, 'sp', axis=0, tiled=True, axis_index_groups=along_z)]
    all_to_all x2 -> x0, starting transfers between devices: 10.1 us -> none  [the longest x1 5.06 us: exchanged(): lax.all_to_all(pieces, ('sp', 'tp'), 0, 0, axis_index_groups=groups, tile...]
    dot_general x2 -> x4, matrix products: 17.2 us -> 7.33 us  [the longest x2 3.61 us: body(): lax.dot_general(hidden, w[:, 1024:], across, preferred_element_type=jnp.f...]
    ppermute x1 -> x3, starting transfers between devices: 11.3 us -> 19.3 us  [the longest x1 11.3 us: swapped(): return lax.ppermute(shard, 'tp', [(i, i ^ 1) for i in range(8)])]
    ppermute x1 -> x3, waiting for transfers between devices: 0.01 us -> 4.33 us  [the longest x2 4.33 us: dealt(): return lax.ppermute(shard, ('sp', 'tp'), pairs)]
    all_to_all x1 -> x2, blocking collectives: 45.9 us -> 49 us  [exchanged(): lax.all_to_all(pieces, ('sp', 'tp'), 0, 0, axis_index_groups=token_groups...]
    all_to_all x1, starting transfers between devices: 10.4 us -> 7.52 us  [summed_on_arrival(): lax.all_to_all(pieces, axis, split_axis=0, concat_axis=0, tiled=True)]
  transfers between devices with their start and end apart: 7 -> 7, of which waited for: 3 -> 4; matrix products, arithmetic and copies ran while one was open for 11% -> 5% of each run, Pallas kernels for 0% -> 0%
where the time goes in v2:
time: 172 us
  waiting for transfers between devices  58.8 us (34%)
  blocking collectives  49 us (28%)
  starting transfers between devices  29.4 us (17%)
  between operations  13.9 us (8%)
  matrix products  9.97 us (6%)
  other arithmetic  7.41 us (4%)
  local copies, waits for them, and re-layouts  3.16 us (2%)
    all_gather x1, waiting for transfers between devices, group_weights(): lax.all_gather(rows, 'sp', axis=0, tiled=True, axis_index_groups=along_z)  52.5 us
    all_to_all x2, blocking collectives, exchanged(): lax.all_to_all(pieces, ('sp', 'tp'), 0, 0, axis_index_groups=token_groups...  49 us
    ppermute x1, starting transfers between devices, swapped(): return lax.ppermute(shard, 'tp', [(i, i ^ 1) for i in range(8)])  11.3 us
    ppermute x2, starting transfers between devices, dealt(): return lax.ppermute(shard, ('sp', 'tp'), pairs)  7.94 us
    all_to_all x1, starting transfers between devices, summed_on_arrival(): lax.all_to_all(pieces, axis, split_axis=0, concat_axis=0, tiled=True)  7.52 us
    ppermute x2, waiting for transfers between devices, dealt(): return lax.ppermute(shard, ('sp', 'tp'), pairs)  4.33 us
    dot_general x2, matrix products, body(): lax.dot_general(hidden, w[:, 1024:], across, preferred_element_type=jnp.f...  3.61 us
  transfers between devices with their start and end apart: 7, of which 4 were waited for; matrix products, arithmetic and copies ran while one was open for 5% of the time, Pallas kernels for 0%

profile of v2, /device:TPU:1, one launch (start us, length us, event | category | flops | bytes accessed | tf_op | source)
XLA Modules:
  0.0 171.6 jit_solution(6591467955588564384)
XLA Ops:
  6.6 1.0 pad_maximum_fusion.4
  7.6 6.0 %collective-permute-start.3 = (bf16[32,2048]{1,0:T(8,128)(2,1)S(1)}, bf16[32,2048]{1,0:T(8,128)(2,1)S(1)}, u32[]{:S(2)}, u32[]{:S(2)}) collective-permute-start(bf16[32,2048]{1,0:T(8,128)(2,1)S(1)} %pad_maximum_fusion.4), channel_id=1, source_target_pairs={{0,16},{1,24},{2,18},{3,26},{4,20},{5,28},{6,22},{7,30},{8,17},{9,... | collective-permute-start | bytes 393224 | tf_op jit(solution)/shard_map/ppermute | solution.py:21
  13.6 1.9 %collective-permute-start.2 = (bf16[32,2048]{1,0:T(8,128)(2,1)S(1)}, bf16[32,2048]{1,0:T(8,128)(2,1)S(1)}, u32[]{:S(2)}, u32[]{:S(2)}) collective-permute-start(bf16[32,2048]{1,0:T(8,128)(2,1)S(1)} %pad_maximum_fusion.4), channel_id=1, source_target_pairs={{0,0},{1,8},{2,2},{3,10},{4,4},{5,12},{6,6},{7,14},{8,1},{9,9},{10... | collective-permute-start | bytes 393224 | tf_op jit(solution)/shard_map/ppermute | solution.py:21
  15.6 1.1 collective-permute-done.3
  16.6 3.3 %collective-permute-done.2 = bf16[32,2048]{1,0:T(8,128)(2,1)S(1)} collective-permute-done((bf16[32,2048]{1,0:T(8,128)(2,1)S(1)}, bf16[32,2048]{1,0:T(8,128)(2,1)S(1)}, u32[]{:S(2)}, u32[]{:S(2)}) %collective-permute-start.2) | collective-permute-done | bytes 131104 | tf_op jit(solution)/shard_map/ppermute | solution.py:21
  19.9 0.7 pad_maximum_fusion.2
  20.7 0.8 fusion.48
  21.7 1.3 collective-permute-start
  23.0 1.3 collective-permute-start.1
  24.3 0.2 copy.59
  24.6 0.1 abs_compare_fusion
  24.8 0.4 multiply_cosine_fusion.1
  25.3 0.2 compare_and_fusion
  25.5 0.1 copy.36
  25.7 0.2 copy.40
  25.9 0.2 copy.41
  26.1 1.9 %collective-permute-done.1 = bf16[2,128,128]{2,1,0:T(8,128)(2,1)S(1)} collective-permute-done((bf16[2,128,128]{2,1,0:T(8,128)(2,1)S(1)}, bf16[2,128,128]{2,1,0:T(8,128)(2,1)S(1)}, u32[]{:S(2)}, u32[]{:S(2)}) %collective-permute-start.1) | collective-permute-done | bytes 65568 | tf_op jit(solution)/shard_map/ppermute | solution.py:66
  28.1 0.1 copy.35
  28.2 0.1 copy.37
  28.4 0.4 fusion.59
  28.9 0.3 fusion.19
  29.2 0.4 fusion.18
  29.7 0.2 copy.43
  29.9 1.8 %convolution_convert_fusion = bf16[384,2048]{1,0:T(8,128)(2,1)} fusion(bf16[256,2048]{1,0:T(8,128)(2,1)S(1)} %copy-done, bf16[48,8,2,128]{3,2,1,0:T(2,128)(2,1)S(1)} %bitcast.103), kind=kOutput, calls=%fused_computation.2 | convolution fusion | flops 403439616 | bytes 2818048 | tf_op jit(solution)/shard_map/dot_general | solution.py:158
  31.6 7.5 %all-to-all-start = ((bf16[8,48,2048]{2,1,0:T(8,128)(2,1)}), bf16[8,48,2048]{2,1,0:T(8,128)(2,1)S(1)}, u32[]{:S(2)}, u32[]{:S(2)}) async-start(bf16[8,48,2048]{2,1,0:T(8,128)(2,1)} %bitcast.86), calls=%async_computation | async-start | bytes 3145728 | tf_op jit(solution)/shard_map/all_to_all | solution.py:78
  39.2 52.5 %all-gather.2.cloned.1.call-done = bf16[1024,2048]{1,0:T(8,128)(2,1)} async-done(((bf16[64,2048]{1,0:T(8,128)(2,1)}), bf16[1024,2048]{1,0:T(8,128)(2,1)}) %all-gather.2.cloned.1.call-update) | async-done | bytes 4194320 | tf_op jit(solution)/shard_map/all_gather | solution.py:54
  91.7 11.3 %collective-permute-start.4 = (bf16[1024,2048]{1,0:T(8,128)(2,1)}, bf16[1024,2048]{1,0:T(8,128)(2,1)}, u32[]{:S(2)}, u32[]{:S(2)}) collective-permute-start(bf16[1024,2048]{1,0:T(8,128)(2,1)} %all-gather.2.cloned.1.call-done), channel_id=1, source_target_pairs={{0,1},{1,0},{2,3},{3,2},{4,5},{5,4},{6,7},{7,6},{8,9},{9,8},{10,11... | collective-permute-start | bytes 12582920 | tf_op jit(solution)/shard_map/ppermute | solution.py:25
  103.1 0.2 convert_reduce_fusion.1
  103.3 0.1 multiply_reduce_fusion.1
  103.4 1.2 fusion.25
  104.6 0.1 fusion.27
  104.8 0.3 copy.44
  105.1 0.1 copy.57
  105.2 0.1 copy.58
  105.4 0.2 broadcast_in_dim.23
  105.6 26.0 %all_to_all.15 = bf16[8,48,2048]{2,1,0:T(8,128)(2,1)S(1)} all-to-all(bf16[8,48,2048]{2,1,0:T(8,128)(2,1)S(1)} %broadcast_in_dim.23), channel_id=1, replica_groups={{0,2,4,6,8,10,12,14},{1,3,5,7,9,11,13,15},{16,18,20,22,24,26,28,30},{17..., dimensions={0} | all-to-all | bytes 3145728 | tf_op jit(solution)/shard_map/all_to_all | solution.py:38
  131.6 2.7 %fusion.4 = f32[384,1024]{1,0:T(8,128)S(1)} fusion(bf16[1024,2048]{1,0:T(8,128)(2,1)} %collective-permute-done.4, bf16[384,2048]{1,0:T(8,128)(2,1)S(1)} %bitcast.89), kind=kOutput, calls=%fused_computation.7 | convolution fusion | flops 805306368 | bytes 4456448 | tf_op jit(solution)/shard_map/dot_general | solution.py:168
  134.4 1.0 multiply_convert_fusion
  135.4 2.6 %fusion.14 = bf16[384,1024]{1,0:T(8,128)(2,1)S(1)} fusion(bf16[384,1024]{1,0:T(8,128)(2,1)S(1)} %multiply_convert_fusion, bf16[1024,2048]{1,0:T(8,128)(2,1)} %collective-permute-done.4), kind=kOutput, calls=%fused_computation.16 | convolution fusion | flops 805699584 | bytes 3670016 | tf_op jit(solution)/shard_map/dot_general | solution.py:172
  138.1 1.0 fusion.11
  139.1 0.1 pad_maximum_fusion
  139.2 23.0 %all_to_all.16 = bf16[8,48,2048]{2,1,0:T(8,128)(2,1)S(1)} all-to-all(bf16[8,48,2048]{2,1,0:T(8,128)(2,1)S(1)} %bitcast.85), channel_id=1, replica_groups={{0,2,4,6,8,10,12,14},{1,3,5,7,9,11,13,15},{16,18,20,22,24,26,28,30},{17..., dimensions={0} | all-to-all | bytes 3145728 | tf_op jit(solution)/shard_map/all_to_all | solution.py:38
  162.2 0.2 convert_reduce_fusion
  162.4 0.3 copy.60
  162.9 0.3 multiply_reduce_fusion
  163.3 0.3 copy.53
  163.6 0.3 copy-done.6
  163.9 0.8 fusion.28
  (47 shorter events, 1.2 us)
Async XLA Ops:
  6.5 23.3 %copy-start = (bf16[256,2048]{1,0:T(8,128)(2,1)S(1)}, bf16[256,2048]{1,0:T(8,128)(2,1)}, u32[]{:S(2)}) copy-start(bf16[256,2048]{1,0:T(8,128)(2,1)} %param.18) | copy-start | bytes 3145732
  6.5 14.2 %copy-start.2 = (bf16[384,128]{1,0:T(8,128)(2,1)S(1)}, bf16[384,128]{1,0:T(8,128)(2,1)}, u32[]{:S(2)}) copy-start(bf16[384,128]{1,0:T(8,128)(2,1)} %param.13) | copy-start | bytes 294916
  6.5 15.0 %copy-start.1 = (bf16[384,128]{1,0:T(8,128)(2,1)S(1)}, bf16[384,128]{1,0:T(8,128)(2,1)}, u32[]{:S(2)}) copy-start(bf16[384,128]{1,0:T(8,128)(2,1)} %param.14) | copy-start | bytes 294916
  6.5 17.7 %copy-start.3 = (bf16[384,256]{1,0:T(8,128)(2,1)S(1)}, bf16[384,256]{1,0:T(8,128)(2,1)}, u32[]{:S(2)}) copy-start(bf16[384,256]{1,0:T(8,128)(2,1)} %param.12) | copy-start | bytes 589828
  6.5 17.9 %copy-start.4 = (s32[24576]{0:T(1024)S(1)}, s32[24576]{0:T(1024)}, u32[]{:S(2)}) copy-start(s32[24576]{0:T(1024)} %param.16) | copy-start | bytes 294916
  6.5 85.1 %all-gather.2.cloned.1.call-start = ((), (), s32[]{:S(2)}) async-start(), calls=%async_computation.3 | async-start | bytes 4456448 | tf_op jit(solution)/shard_map/all_gather | solution.py:54
  7.6 9.1 %collective-permute-start.3 = (bf16[32,2048]{1,0:T(8,128)(2,1)S(1)}, bf16[32,2048]{1,0:T(8,128)(2,1)S(1)}, u32[]{:S(2)}, u32[]{:S(2)}) collective-permute-start(bf16[32,2048]{1,0:T(8,128)(2,1)S(1)} %pad_maximum_fusion.4), channel_id=1, source_target_pairs={{0,16},{1,24},{2,18},{3,26},{4,20},{5,28},{6,22},{7,30},{8,17},{9,... | collective-permute-start | bytes 393224 | tf_op jit(solution)/shard_map/ppermute | solution.py:21
  13.6 6.3 %collective-permute-start.2 = (bf16[32,2048]{1,0:T(8,128)(2,1)S(1)}, bf16[32,2048]{1,0:T(8,128)(2,1)S(1)}, u32[]{:S(2)}, u32[]{:S(2)}) collective-permute-start(bf16[32,2048]{1,0:T(8,128)(2,1)S(1)} %pad_maximum_fusion.4), channel_id=1, source_target_pairs={{0,0},{1,8},{2,2},{3,10},{4,4},{5,12},{6,6},{7,14},{8,1},{9,9},{10... | collective-permute-start | bytes 393224 | tf_op jit(solution)/shard_map/ppermute | solution.py:21
  21.7 4.4 %collective-permute-start = (bf16[2,128,128]{2,1,0:T(8,128)(2,1)S(1)}, bf16[2,128,128]{2,1,0:T(8,128)(2,1)S(1)}, u32[]{:S(2)}, u32[]{:S(2)}) collective-permute-start(bf16[2,128,128]{2,1,0:T(8,128)(2,1)S(1)} %get-tuple-element.19), channel_id=1, source_target_pairs={{0,8},{8,16},{16,24},{24,32},{32,40},{40,48},{48,56},{56,64},{64,7... | collective-permute-start | bytes 196616 | tf_op jit(solution)/shard_map/ppermute | solution.py:65
  23.0 5.0 %collective-permute-start.1 = (bf16[2,128,128]{2,1,0:T(8,128)(2,1)S(1)}, bf16[2,128,128]{2,1,0:T(8,128)(2,1)S(1)}, u32[]{:S(2)}, u32[]{:S(2)}) collective-permute-start(bf16[2,128,128]{2,1,0:T(8,128)(2,1)S(1)} %get-tuple-element.20), channel_id=1, source_target_pairs={{8,0},{16,8},{24,16},{32,24},{40,32},{48,40},{56,48},{64,56},{72,6... | collective-permute-start | bytes 196616 | tf_op jit(solution)/shard_map/ppermute | solution.py:66
  28.1 0.7 copy-start.8
  31.6 71.4 %all-to-all-start = ((bf16[8,48,2048]{2,1,0:T(8,128)(2,1)}), bf16[8,48,2048]{2,1,0:T(8,128)(2,1)S(1)}, u32[]{:S(2)}, u32[]{:S(2)}) async-start(bf16[8,48,2048]{2,1,0:T(8,128)(2,1)} %bitcast.86), calls=%async_computation | async-start | bytes 3145728 | tf_op jit(solution)/shard_map/all_to_all | solution.py:78
  39.2 64.3 %copy-start.5 = (f32[2048]{0:T(1024)S(1)}, f32[2048]{0:T(1024)}, u32[]{:S(2)}) copy-start(f32[2048]{0:T(1024)} %param.19) | copy-start | bytes 24580
  91.7 39.9 %collective-permute-start.4 = (bf16[1024,2048]{1,0:T(8,128)(2,1)}, bf16[1024,2048]{1,0:T(8,128)(2,1)}, u32[]{:S(2)}, u32[]{:S(2)}) collective-permute-start(bf16[1024,2048]{1,0:T(8,128)(2,1)} %all-gather.2.cloned.1.call-done), channel_id=1, source_target_pairs={{0,1},{1,0},{2,3},{3,2},{4,5},{5,4},{6,7},{7,6},{8,9},{9,8},{10,11... | collective-permute-start | bytes 12582920 | tf_op jit(solution)/shard_map/ppermute | solution.py:25
  103.0 1.6 copy-start.7
  131.6 2.8 %copy-start.9 = (bf16[1024,2048]{1,0:T(8,128)(2,1)S(1)}, bf16[1024,2048]{1,0:T(8,128)(2,1)}, u32[]{:S(2)}) copy-start(bf16[1024,2048]{1,0:T(8,128)(2,1)} %all-gather.2.cloned.1.call-done) | copy-start | bytes 12582916
  163.2 0.7 copy-start.6
Sparse Core Ops, SparseCore 0:
  20.8 70.8 all-gather.1

commit v3 on v1

--- a/solution.py
+++ b/solution.py
@@ -11,26 +11,54 @@
     return (4 * z + y) * 8 + 2 * x + core
 
 
-def group_weights(up_proj, down_proj):
-    columns = [w.reshape(32, 4, 256).swapaxes(0, 1) for w in (up_proj, down_proj.T)]
-    along_y = [[4 * z + y for y in range(4)] for z in range(16)]
-    along_z = [[4 * z + y for z in range(16)] for y in range(4)]
-    rows = lax.all_to_all(
-        jnp.concatenate(columns, axis=2), "sp", 0, 0, axis_index_groups=along_y, tiled=True
-    )
-    own = lax.all_gather(
-        rows.reshape(128, 512), "sp", axis=0, tiled=True, axis_index_groups=along_z
-    )
-    return own, lax.ppermute(own, "tp", [(i, i ^ 1) for i in range(8)])
-
-
-def exchanged(pieces):
-    groups = [
-        [device(z, y, x, core) for y in range(4) for x in range(4)]
+def swapped(shard):
+    return lax.ppermute(shard, "tp", [(i, i ^ 1) for i in range(8)])
+
+
+def token_groups():
+    return [
+        [device(z, 2 * q + par, x, core) for par in range(2) for x in range(4)]
         for z in range(16)
+        for q in range(2)
         for core in range(2)
     ]
-    return lax.all_to_all(pieces, ("sp", "tp"), 0, 0, axis_index_groups=groups, tiled=True)
+
+
+def exchanged(pieces):
+    return lax.all_to_all(
+        pieces, ("sp", "tp"), 0, 0, axis_index_groups=token_groups(), tiled=True
+    )
+
+
+def group_weights(up_proj, down_proj):
+    down_rows = down_proj.T
+    halved = [
+        jnp.concatenate([w[:, at : at + 512] for w in (up_proj, down_rows)], axis=1)
+        for at in (0, 512)
+    ]
+    pieces = jnp.concatenate([jnp.broadcast_to(h[None], (4, 32, 1024)) for h in halved])
+    rings = [
+        [device(z, y, x, core) for core in range(2) for y in range(4)]
+        for z in range(16)
+        for x in range(4)
+    ]
+    dealt = lax.all_to_all(
+        pieces, ("sp", "tp"), 0, 0, axis_index_groups=rings, tiled=True
+    )
+    block = lax.axis_index("sp") % 2
+    rows = lax.dynamic_slice_in_dim(dealt, 4 * block, 4, axis=0).reshape(128, 1024)
+    along_z = [[4 * z + y for z in range(16)] for y in range(4)]
+    return lax.all_gather(rows, "sp", axis=0, tiled=True, axis_index_groups=along_z)
+
+
+def ffn_up(normed, both):
+    up_acts = jnp.dot(normed, both[:, :512], preferred_element_type=jnp.float32)
+    return jnp.square(jax.nn.relu(up_acts)).astype(jnp.bfloat16)
+
+
+def ffn_down(hidden, both):
+    across = (((1,), (1,)), ((), ()))
+    return lax.dot_general(hidden, both[:, 512:], across, preferred_element_type=jnp.float32)
 
 
 def padded(shard, sides, width):
@@ -137,18 +165,15 @@
     own_resid = lax.dynamic_slice_in_dim(residual, lax.axis_index("tp") * share_rows, share_rows, 0)
     after_mix = (own_resid.astype(jnp.float32) + rms_scale(mixed, gain_mix)).astype(jnp.bfloat16)
     own_normed = rms_scale(after_mix.astype(jnp.float32), gain_ffn_in).astype(jnp.bfloat16)
-    normed = exchanged(jnp.broadcast_to(own_normed[None], (16, *own_normed.shape)))
+    normed = exchanged(jnp.broadcast_to(own_normed[None], (8, *own_normed.shape)))
     normed = normed.reshape(-1, 2048)
-    across = (((1,), (1,)), ((), ()))
-    ffn_part = 0.0
-    for both in weights:
-        up_acts = jnp.dot(normed, both[:, :256], preferred_element_type=jnp.float32)
-        hidden = jnp.square(jax.nn.relu(up_acts)).astype(jnp.bfloat16)
-        ffn_part += lax.dot_general(
-            hidden, both[:, 256:], across, preferred_element_type=jnp.float32
-        )
-    arrived = exchanged(ffn_part.astype(jnp.bfloat16).reshape(16, -1, 2048))
-    ffn_out = arrived.astype(jnp.float32).sum(axis=0)
+    other_normed = swapped(normed)
+    other_part = ffn_down(ffn_up(other_normed, weights), weights).astype(jnp.bfloat16)
+    received = swapped(other_part)
+    hidden = lax.optimization_barrier(ffn_up(normed, weights))
+    own_part = ffn_down(hidden, weights)
+    both_parts = (own_part + received.astype(jnp.float32)).astype(jnp.bfloat16)
+    ffn_out = exchanged(both_parts.reshape(8, -1, 2048)).astype(jnp.float32).sum(axis=0)
     return (after_mix.astype(jnp.float32) + rms_scale(ffn_out, gain_ffn_out)).astype(jnp.bfloat16)
 
 

time: 192 us -> 165 us (0.86)
  waiting for transfers between devices: 62.1 us -> 44.9 us
  matrix products: 19.8 us -> 11.9 us
  starting transfers between devices: 36.5 us -> 32.5 us
  blocking collectives: 45.9 us -> 48.8 us
    all_gather x1, waiting for transfers between devices: 39.7 us -> 11.9 us  [group_weights(): lax.all_gather(rows, 'sp', axis=0, tiled=True, axis_index_groups=along_z)]
    all_to_all x2 -> x1, waiting for transfers between devices: 0.01 us -> 8.53 us  [group_weights(): lax.all_to_all(pieces, ('sp', 'tp'), 0, 0, axis_index_groups=rings, tiled...]
    dot_general x2 -> x3, matrix products: 17.2 us -> 9.29 us  [the longest x2 6.73 us: ffn_down(): lax.dot_general(hidden, both[:, 512:], across, preferred_element_type=jnp...]
    all_to_all x1, starting transfers between devices: 10.4 us -> 3.78 us  [summed_on_arrival(): lax.all_to_all(pieces, axis, split_axis=0, concat_axis=0, tiled=True)]
    ppermute x1 -> x2, starting transfers between devices: 11.3 us -> 15.3 us  [swapped(): return lax.ppermute(shard, 'tp', [(i, i ^ 1) for i in range(8)])]
    ppermute x1 -> x2, waiting for transfers between devices: 0.01 us -> 3.8 us  [swapped(): return lax.ppermute(shard, 'tp', [(i, i ^ 1) for i in range(8)])]
    all_to_all x1 -> x2, blocking collectives: 45.9 us -> 48.8 us  [exchanged(): lax.all_to_all(pieces, ('sp', 'tp'), 0, 0, axis_index_groups=token_groups...]
    all_to_all x2 -> x1, starting transfers between devices: 10.1 us -> 8.16 us  [group_weights(): lax.all_to_all(pieces, ('sp', 'tp'), 0, 0, axis_index_groups=rings, tiled...]
  transfers between devices with their start and end apart: 7 -> 7, of which waited for: 3 -> 5; matrix products, arithmetic and copies ran while one was open for 11% -> 8% of each run, Pallas kernels for 0% -> 0%
where the time goes in v3:
time: 165 us; the launch traced here: 164 us
  blocking collectives  48.8 us (30%)
  waiting for transfers between devices  44.9 us (27%)
  starting transfers between devices  32.5 us (20%)
  between operations  13.7 us (8%)
  matrix products  11.9 us (7%)
  other arithmetic  7.82 us (5%)
  local copies, waits for them, and re-layouts  4.26 us (3%)
    all_to_all x2, blocking collectives, exchanged(): lax.all_to_all(pieces, ('sp', 'tp'), 0, 0, axis_index_groups=token_groups...  48.8 us
    all_to_all x1, waiting for transfers between devices, summed_on_arrival(): lax.all_to_all(pieces, axis, split_axis=0, concat_axis=0, tiled=True)  20.6 us
    ppermute x2, starting transfers between devices, swapped(): return lax.ppermute(shard, 'tp', [(i, i ^ 1) for i in range(8)])  15.3 us
    all_gather x1, waiting for transfers between devices, group_weights(): lax.all_gather(rows, 'sp', axis=0, tiled=True, axis_index_groups=along_z)  11.9 us
    all_to_all x1, waiting for transfers between devices, group_weights(): lax.all_to_all(pieces, ('sp', 'tp'), 0, 0, axis_index_groups=rings, tiled...  8.53 us
    all_to_all x1, starting transfers between devices, group_weights(): lax.all_to_all(pieces, ('sp', 'tp'), 0, 0, axis_index_groups=rings, tiled...  8.16 us
    dot_general x2, matrix products, ffn_down(): lax.dot_general(hidden, both[:, 512:], across, preferred_element_type=jnp...  6.73 us
    ppermute x1, starting transfers between devices, padded(): before = lax.ppermute(last, axis, up)  4.02 us
  transfers between devices with their start and end apart: 7, of which 5 were waited for; matrix products, arithmetic and copies ran while one was open for 8% of the time, Pallas kernels for 0%

profile of v3, /device:TPU:1, one launch (start us, length us, event | category | flops | bytes accessed | tf_op | source)
XLA Modules:
  0.0 163.9 jit_solution(6758690959742080350)
XLA Ops:
  6.6 1.9 %fusion.59 = (bf16[384,1,64]{2,0,1:T(8,128)(2,1)S(1)}, bf16[384,1,64]{2,0,1:T(8,128)(2,1)S(1)}) fusion(f32[64]{0:T(128)S(1)} %multiply_power_fusion, f32[384]{0:T(512)S(1)} %add_convert_fusion.2, bf16[384,1,128]{2,0,1:T(8,128)(2,1)} %bitcast.82), kind=kLoop, calls=%fused_computation.68 | loop fusion | flops 270336 | bytes 198400 | tf_op jit(solution)/shard_map/convert.11
  8.4 0.9 pad_maximum_fusion.11
  9.3 4.0 %collective-permute-start = (bf16[2,128,128]{2,1,0:T(8,128)(2,1)S(1)}, bf16[2,128,128]{2,1,0:T(8,128)(2,1)S(1)}, u32[]{:S(2)}, u32[]{:S(2)}) collective-permute-start(bf16[2,128,128]{2,1,0:T(8,128)(2,1)S(1)} %get-tuple-element.15), channel_id=1, source_target_pairs={{0,8},{8,16},{16,24},{24,32},{32,40},{40,48},{48,56},{56,64},{64,7... | collective-permute-start | bytes 196616 | tf_op jit(solution)/shard_map/ppermute | solution.py:71
  13.3 1.3 collective-permute-start.1
  14.6 0.8 fusion.71
  15.4 0.8 fusion.72
  16.3 0.8 pad_maximum_fusion
  17.2 8.2 %all-to-all-start.2 = ((bf16[8,32,1024]{2,1,0:T(8,128)(2,1)}), bf16[8,32,1024]{2,1,0:T(8,128)(2,1)S(1)}, u32[]{:S(2)}, u32[]{:S(2)}) async-start(bf16[8,32,1024]{2,1,0:T(8,128)(2,1)} %pad_maximum_fusion), calls=%async_computation.2 | async-start | bytes 1048576 | tf_op jit(solution)/shard_map/all_to_all | solution.py:45
  25.3 0.1 pad_dynamic-slice_fusion
  25.4 0.2 copy.26
  25.6 0.4 multiply_cosine_fusion.1
  26.1 8.5 %all-to-all-done.2 = bf16[8,32,1024]{2,1,0:T(8,128)(2,1)S(1)} async-done(((bf16[8,32,1024]{2,1,0:T(8,128)(2,1)}), bf16[8,32,1024]{2,1,0:T(8,128)(2,1)S(1)}, u32[]{:S(2)}, u32[]{:S(2)}) %all-to-all-start.2) | async-done | bytes 524320 | tf_op jit(solution)/shard_map/all_to_all | solution.py:45
  34.7 0.7 constant_dynamic-slice_fusion
  35.4 0.1 dynamic-slice_bitcast_fusion
  35.5 0.1 abs_compare_fusion
  35.6 0.2 compare_and_fusion
  35.9 0.1 copy.15
  36.0 0.2 copy.19
  36.3 0.2 copy.20
  36.5 0.1 pad_maximum_fusion.8
  36.6 0.1 copy.14
  36.8 0.1 copy.16
  36.9 0.4 fusion.73
  37.4 0.3 fusion.32
  37.8 0.4 fusion.29
  38.2 0.2 copy.22
  38.4 1.8 %convolution_convert_fusion.1 = bf16[384,2048]{1,0:T(8,128)(2,1)} fusion(bf16[256,2048]{1,0:T(8,128)(2,1)S(1)} %copy-done, bf16[48,8,2,128]{3,2,1,0:T(2,128)(2,1)S(1)} %bitcast.81), kind=kOutput, calls=%fused_computation.4 | convolution fusion | flops 403439616 | bytes 2818048 | tf_op jit(solution)/shard_map/dot_general | solution.py:163
  40.1 3.8 %all-to-all-start = ((bf16[8,48,2048]{2,1,0:T(8,128)(2,1)}), bf16[8,48,2048]{2,1,0:T(8,128)(2,1)S(1)}, u32[]{:S(2)}, u32[]{:S(2)}) async-start(bf16[8,48,2048]{2,1,0:T(8,128)(2,1)} %bitcast.66), calls=%async_computation | async-start | bytes 3145728 | tf_op jit(solution)/shard_map/all_to_all | solution.py:84
  43.9 20.6 %all-to-all-done = bf16[8,48,2048]{2,1,0:T(8,128)(2,1)S(1)} async-done(((bf16[8,48,2048]{2,1,0:T(8,128)(2,1)}), bf16[8,48,2048]{2,1,0:T(8,128)(2,1)S(1)}, u32[]{:S(2)}, u32[]{:S(2)}) %all-to-all-start) | async-done | bytes 1572896 | tf_op jit(solution)/shard_map/all_to_all | solution.py:84
  64.5 0.2 convert_reduce_fusion.1
  64.8 0.1 multiply_reduce_fusion.1
  64.9 1.2 fusion.35
  66.1 0.1 fusion.37
  66.2 0.2 broadcast_in_dim.27
  66.4 22.9 %all_to_all.20 = bf16[8,48,2048]{2,1,0:T(8,128)(2,1)S(1)} all-to-all(bf16[8,48,2048]{2,1,0:T(8,128)(2,1)S(1)} %broadcast_in_dim.27), channel_id=1, replica_groups={{0,2,4,6,8,10,12,14},{1,3,5,7,9,11,13,15},{16,18,20,22,24,26,28,30},{17..., dimensions={0} | all-to-all | bytes 3145728 | tf_op jit(solution)/shard_map/all_to_all | solution.py:28
  89.4 3.7 %collective-permute-start.2 = (bf16[384,2048]{1,0:T(8,128)(2,1)S(1)}, bf16[384,2048]{1,0:T(8,128)(2,1)}, u32[]{:S(2)}, u32[]{:S(2)}) collective-permute-start(bf16[384,2048]{1,0:T(8,128)(2,1)S(1)} %bitcast.67), channel_id=1, source_target_pairs={{0,1},{1,0},{2,3},{3,2},{4,5},{5,4},{6,7},{7,6},{8,9},{9,8},{10,11... | collective-permute-start | bytes 4718600 | tf_op jit(solution)/shard_map/ppermute | solution.py:15
  93.0 3.1 %collective-permute-done.2 = bf16[384,2048]{1,0:T(8,128)(2,1)} collective-permute-done((bf16[384,2048]{1,0:T(8,128)(2,1)S(1)}, bf16[384,2048]{1,0:T(8,128)(2,1)}, u32[]{:S(2)}, u32[]{:S(2)}) %collective-permute-start.2) | collective-permute-done | bytes 1572896 | tf_op jit(solution)/shard_map/ppermute | solution.py:15
  96.2 11.9 %all-gather.2.cloned.1.call-done = bf16[2048,1024]{1,0:T(8,128)(2,1)} async-done(((bf16[128,1024]{1,0:T(8,128)(2,1)}), bf16[2048,1024]{1,0:T(8,128)(2,1)}) %all-gather.2.cloned.1.call-update) | async-done | bytes 4194320 | tf_op jit(solution)/shard_map/all_gather | solution.py:51
  108.1 5.7 %convolution_convert_fusion = bf16[384,2048]{1,0:T(8,128)(2,1)} fusion(bf16[2048,1024]{1,0:T(8,128)(2,1)} %all-gather.2.cloned.1.call-done, bf16[384,2048]{1,0:T(8,128)(2,1)} %collective-permute-done.2), kind=kOutput, calls=%fused_computation.3 | convolution fusion | flops 1611988992 | bytes 7340032 | tf_op jit(solution)/shard_map/dot_general | solution.py:61
  113.9 11.6 %collective-permute-start.3 = (bf16[384,2048]{1,0:T(8,128)(2,1)}, bf16[384,2048]{1,0:T(8,128)(2,1)S(1)}, u32[]{:S(2)}, u32[]{:S(2)}) collective-permute-start(bf16[384,2048]{1,0:T(8,128)(2,1)} %convolution_convert_fusion), channel_id=1, source_target_pairs={{0,1},{1,0},{2,3},{3,2},{4,5},{5,4},{6,7},{7,6},{8,9},{9,8},{10,11... | collective-permute-start | bytes 4718600 | tf_op jit(solution)/shard_map/ppermute | solution.py:15
  125.4 2.6 %fusion.26 = bf16[384,512]{1,0:T(8,128)(2,1)S(1)} fusion(bf16[384,2048]{1,0:T(8,128)(2,1)S(1)} %bitcast.68, bf16[2048,1024]{1,0:T(8,128)(2,1)} %all-gather.2.cloned.1.call-done), kind=kOutput, calls=%fused_computation.20 | convolution fusion | flops 805896192 | bytes 4063232 | tf_op jit(solution)/shard_map/dot_general | solution.py:55
  128.0 0.7 collective-permute-done.3
  128.7 1.0 add_convert_fusion
  129.7 25.8 %all_to_all.21 = bf16[8,48,2048]{2,1,0:T(8,128)(2,1)S(1)} all-to-all(bf16[8,48,2048]{2,1,0:T(8,128)(2,1)S(1)} %bitcast.69), channel_id=1, replica_groups={{0,2,4,6,8,10,12,14},{1,3,5,7,9,11,13,15},{16,18,20,22,24,26,28,30},{17..., dimensions={0} | all-to-all | bytes 3145728 | tf_op jit(solution)/shard_map/all_to_all | solution.py:28
  155.5 0.2 convert_reduce_fusion
  155.8 0.1 multiply_reduce_fusion
  155.9 0.3 copy-done.5
  156.2 0.8 fusion.38
  (37 shorter events, 0.5 us)
Async XLA Ops:
  6.5 31.8 %copy-start = (bf16[256,2048]{1,0:T(8,128)(2,1)S(1)}, bf16[256,2048]{1,0:T(8,128)(2,1)}, u32[]{:S(2)}) copy-start(bf16[256,2048]{1,0:T(8,128)(2,1)} %param.18) | copy-start | bytes 3145732
  9.3 27.2 %collective-permute-start = (bf16[2,128,128]{2,1,0:T(8,128)(2,1)S(1)}, bf16[2,128,128]{2,1,0:T(8,128)(2,1)S(1)}, u32[]{:S(2)}, u32[]{:S(2)}) collective-permute-start(bf16[2,128,128]{2,1,0:T(8,128)(2,1)S(1)} %get-tuple-element.15), channel_id=1, source_target_pairs={{0,8},{8,16},{16,24},{24,32},{32,40},{40,48},{48,56},{56,64},{64,7... | collective-permute-start | bytes 196616 | tf_op jit(solution)/shard_map/ppermute | solution.py:71
  13.3 23.2 %collective-permute-start.1 = (bf16[2,128,128]{2,1,0:T(8,128)(2,1)S(1)}, bf16[2,128,128]{2,1,0:T(8,128)(2,1)S(1)}, u32[]{:S(2)}, u32[]{:S(2)}) collective-permute-start(bf16[2,128,128]{2,1,0:T(8,128)(2,1)S(1)} %get-tuple-element.16), channel_id=1, source_target_pairs={{8,0},{16,8},{24,16},{32,24},{40,32},{48,40},{56,48},{64,56},{72,6... | collective-permute-start | bytes 196616 | tf_op jit(solution)/shard_map/ppermute | solution.py:72
  15.4 9.9 %copy-start.3 = (s32[24576]{0:T(1024)S(1)}, s32[24576]{0:T(1024)}, u32[]{:S(2)}) copy-start(s32[24576]{0:T(1024)} %param.16) | copy-start | bytes 294916
  16.2 9.2 %copy-start.2 = (bf16[384,256]{1,0:T(8,128)(2,1)S(1)}, bf16[384,256]{1,0:T(8,128)(2,1)}, u32[]{:S(2)}) copy-start(bf16[384,256]{1,0:T(8,128)(2,1)} %param.12) | copy-start | bytes 589828
  17.2 18.7 %copy-start.1 = (bf16[384,128]{1,0:T(8,128)(2,1)S(1)}, bf16[384,128]{1,0:T(8,128)(2,1)}, u32[]{:S(2)}) copy-start(bf16[384,128]{1,0:T(8,128)(2,1)} %param.14) | copy-start | bytes 294916
  17.2 17.5 %all-to-all-start.2 = ((bf16[8,32,1024]{2,1,0:T(8,128)(2,1)}), bf16[8,32,1024]{2,1,0:T(8,128)(2,1)S(1)}, u32[]{:S(2)}, u32[]{:S(2)}) async-start(bf16[8,32,1024]{2,1,0:T(8,128)(2,1)} %pad_maximum_fusion), calls=%async_computation.2 | async-start | bytes 1048576 | tf_op jit(solution)/shard_map/all_to_all | solution.py:45
  25.3 82.8 %all-gather.2.cloned.1.call-start = ((), (), s32[]{:S(2)}) async-start(), calls=%async_computation.4 | async-start | bytes 4456448 | tf_op jit(solution)/shard_map/all_gather | solution.py:51
  36.6 0.7 copy-start.7
  40.1 24.4 %all-to-all-start = ((bf16[8,48,2048]{2,1,0:T(8,128)(2,1)}), bf16[8,48,2048]{2,1,0:T(8,128)(2,1)S(1)}, u32[]{:S(2)}, u32[]{:S(2)}) async-start(bf16[8,48,2048]{2,1,0:T(8,128)(2,1)} %bitcast.66), calls=%async_computation | async-start | bytes 3145728 | tf_op jit(solution)/shard_map/all_to_all | solution.py:84
  43.9 21.0 %copy-start.4 = (f32[2048]{0:T(1024)S(1)}, f32[2048]{0:T(1024)}, u32[]{:S(2)}) copy-start(f32[2048]{0:T(1024)} %param.19) | copy-start | bytes 24580
  43.9 22.2 %copy-start.6 = (f32[2048]{0:T(1024)S(1)}, f32[2048]{0:T(1024)}, u32[]{:S(2)}) copy-start(f32[2048]{0:T(1024)} %param.22) | copy-start | bytes 24580
  89.4 6.8 %collective-permute-start.2 = (bf16[384,2048]{1,0:T(8,128)(2,1)S(1)}, bf16[384,2048]{1,0:T(8,128)(2,1)}, u32[]{:S(2)}, u32[]{:S(2)}) collective-permute-start(bf16[384,2048]{1,0:T(8,128)(2,1)S(1)} %bitcast.67), channel_id=1, source_target_pairs={{0,1},{1,0},{2,3},{3,2},{4,5},{5,4},{6,7},{7,6},{8,9},{9,8},{10,11... | collective-permute-start | bytes 4718600 | tf_op jit(solution)/shard_map/ppermute | solution.py:15
  113.8 14.8 %copy-start.8 = (bf16[2048,1024]{1,0:T(8,128)(2,1)S(1)}, bf16[2048,1024]{1,0:T(8,128)(2,1)}, u32[]{:S(2)}) copy-start(bf16[2048,1024]{1,0:T(8,128)(2,1)} %all-gather.2.cloned.1.call-done) | copy-start | bytes 12582916
  113.9 14.8 %collective-permute-start.3 = (bf16[384,2048]{1,0:T(8,128)(2,1)}, bf16[384,2048]{1,0:T(8,128)(2,1)S(1)}, u32[]{:S(2)}, u32[]{:S(2)}) collective-permute-start(bf16[384,2048]{1,0:T(8,128)(2,1)} %convolution_convert_fusion), channel_id=1, source_target_pairs={{0,1},{1,0},{2,3},{3,2},{4,5},{5,4},{6,7},{7,6},{8,9},{9,8},{10,11... | collective-permute-start | bytes 4718600 | tf_op jit(solution)/shard_map/ppermute | solution.py:15
  155.5 0.7 copy-start.5
Sparse Core Ops, SparseCore 0:
  35.5 72.5 all-gather.1

commit v4 on v3

--- a/solution.py
+++ b/solution.py
@@ -1,3 +1,5 @@
+import itertools
+
 import jax
 import jax.numpy as jnp
 from jax import lax
@@ -30,23 +32,30 @@
     )
 
 
+def dealt(shard, turn_y, turn_core):
+    pairs = []
+    for z, y, x, core in itertools.product(range(16), range(4), range(4), range(2)):
+        target = device(z, core + 2 * ((y // 2 + turn_y) % 2), x, (y + turn_core) % 2)
+        pairs.append((device(z, y, x, core), target))
+    return lax.ppermute(shard, ("sp", "tp"), pairs)
+
+
+def in_order(swap, first, second):
+    return [jnp.where(swap, second, first), jnp.where(swap, first, second)]
+
+
 def group_weights(up_proj, down_proj):
+    y, core = (lax.axis_index("sp") % 4, lax.axis_index("tp") % 2)
     down_rows = down_proj.T
     halved = [
         jnp.concatenate([w[:, at : at + 512] for w in (up_proj, down_rows)], axis=1)
         for at in (0, 512)
     ]
-    pieces = jnp.concatenate([jnp.broadcast_to(h[None], (4, 32, 1024)) for h in halved])
-    rings = [
-        [device(z, y, x, core) for core in range(2) for y in range(4)]
-        for z in range(16)
-        for x in range(4)
-    ]
-    dealt = lax.all_to_all(
-        pieces, ("sp", "tp"), 0, 0, axis_index_groups=rings, tiled=True
-    )
-    block = lax.axis_index("sp") % 2
-    rows = lax.dynamic_slice_in_dim(dealt, 4 * block, 4, axis=0).reshape(128, 1024)
+    sent = in_order(y % 2 == 1, *halved)
+    got = [[dealt(sent[b], a, b) for b in range(2)] for a in range(2)]
+    got = [in_order(core == 1, *pair) for pair in got]
+    low, high = ([in_order(y >= 2, got[0][b], got[1][b])[a] for b in range(2)] for a in range(2))
+    rows = jnp.concatenate(low + high, axis=0)
     along_z = [[4 * z + y for z in range(16)] for y in range(4)]
     return lax.all_gather(rows, "sp", axis=0, tiled=True, axis_index_groups=along_z)
 

time: 165 us -> 161 us (0.976)
  waiting for transfers between devices: 44.9 us -> 33.3 us
  starting transfers between devices: 32.5 us -> 41.6 us
    ppermute x0 -> x4, starting transfers between devices: none -> 17.3 us  [dealt(): return lax.ppermute(shard, ('sp', 'tp'), pairs)]
    all_to_all x1 -> x0, waiting for transfers between devices: 8.53 us -> none  [group_weights(): lax.all_to_all(pieces, ('sp', 'tp'), 0, 0, axis_index_groups=rings, tiled...]
    all_to_all x1 -> x0, starting transfers between devices: 8.16 us -> none  [group_weights(): lax.all_to_all(pieces, ('sp', 'tp'), 0, 0, axis_index_groups=rings, tiled...]
    all_gather x1, waiting for transfers between devices: 11.9 us -> 7.06 us  [group_weights(): lax.all_gather(rows, 'sp', axis=0, tiled=True, axis_index_groups=along_z)]
    all_to_all x1, starting transfers between devices: 3.78 us -> 5.66 us  [summed_on_arrival(): lax.all_to_all(pieces, axis, split_axis=0, concat_axis=0, tiled=True)]
    ppermute x1, waiting for transfers between devices: 0.01 us -> 1.84 us  [padded(): after = lax.ppermute(first, axis, down)]
  transfers between devices with their start and end apart: 7 -> 10, of which waited for: 5 -> 5; matrix products, arithmetic and copies ran while one was open for 8% -> 8% of each run, Pallas kernels for 0% -> 0%
where the time goes in v4:
time: 161 us; the launch traced here: 160 us
  blocking collectives  48.7 us (30%)
  starting transfers between devices  41.6 us (26%)
  waiting for transfers between devices  33.3 us (21%)
  between operations  13.8 us (9%)
  matrix products  11.9 us (7%)
  other arithmetic  7.7 us (5%)
  local copies, waits for them, and re-layouts  2.77 us (2%)
    all_to_all x2, blocking collectives, exchanged(): lax.all_to_all(pieces, ('sp', 'tp'), 0, 0, axis_index_groups=token_groups...  48.7 us
    all_to_all x1, waiting for transfers between devices, summed_on_arrival(): lax.all_to_all(pieces, axis, split_axis=0, concat_axis=0, tiled=True)  20.6 us
    ppermute x4, starting transfers between devices, dealt(): return lax.ppermute(shard, ('sp', 'tp'), pairs)  17.3 us
    ppermute x2, starting transfers between devices, swapped(): return lax.ppermute(shard, 'tp', [(i, i ^ 1) for i in range(8)])  14.8 us
    all_gather x1, waiting for transfers between devices, group_weights(): lax.all_gather(rows, 'sp', axis=0, tiled=True, axis_index_groups=along_z)  7.06 us
    dot_general x2, matrix products, ffn_down(): lax.dot_general(hidden, both[:, 512:], across, preferred_element_type=jnp...  6.73 us
    all_to_all x1, starting transfers between devices, summed_on_arrival(): lax.all_to_all(pieces, axis, split_axis=0, concat_axis=0, tiled=True)  5.66 us
    ppermute x2, waiting for transfers between devices, swapped(): return lax.ppermute(shard, 'tp', [(i, i ^ 1) for i in range(8)])  3.8 us
  transfers between devices with their start and end apart: 10, of which 5 were waited for; matrix products, arithmetic and copies ran while one was open for 8% of the time, Pallas kernels for 0%

profile of v4, /device:TPU:1, one launch (start us, length us, event | category | flops | bytes accessed | tf_op | source)
XLA Modules:
  0.0 159.9 jit_solution(13931081950764911759)
XLA Ops:
  6.6 0.9 fusion.71
  7.5 4.0 %collective-permute-start.4 = (bf16[32,1024]{1,0:T(8,128)(2,1)S(1)}, bf16[32,1024]{1,0:T(8,128)(2,1)S(1)}, u32[]{:S(2)}, u32[]{:S(2)}) collective-permute-start(bf16[32,1024]{1,0:T(8,128)(2,1)S(1)} %get-tuple-element.21), channel_id=1, source_target_pairs={{0,1},{1,9},{2,3},{3,11},{4,5},{5,13},{6,7},{7,15},{8,0},{9,8},{10... | collective-permute-start | bytes 196616 | tf_op jit(solution)/shard_map/ppermute | solution.py:40
  11.6 4.0 %collective-permute-start.2 = (bf16[32,1024]{1,0:T(8,128)(2,1)S(1)}, bf16[32,1024]{1,0:T(8,128)(2,1)S(1)}, u32[]{:S(2)}, u32[]{:S(2)}) collective-permute-start(bf16[32,1024]{1,0:T(8,128)(2,1)S(1)} %get-tuple-element.21), channel_id=1, source_target_pairs={{0,17},{1,25},{2,19},{3,27},{4,21},{5,29},{6,23},{7,31},{8,16},{9,... | collective-permute-start | bytes 196616 | tf_op jit(solution)/shard_map/ppermute | solution.py:40
  15.6 6.2 %collective-permute-start.5 = (bf16[32,1024]{1,0:T(8,128)(2,1)S(1)}, bf16[32,1024]{1,0:T(8,128)(2,1)S(1)}, u32[]{:S(2)}, u32[]{:S(2)}) collective-permute-start(bf16[32,1024]{1,0:T(8,128)(2,1)S(1)} %get-tuple-element.22), channel_id=1, source_target_pairs={{0,0},{1,8},{2,2},{3,10},{4,4},{5,12},{6,6},{7,14},{8,1},{9,9},{10... | collective-permute-start | bytes 196616 | tf_op jit(solution)/shard_map/ppermute | solution.py:40
  21.8 3.1 %collective-permute-start.3 = (bf16[32,1024]{1,0:T(8,128)(2,1)S(1)}, bf16[32,1024]{1,0:T(8,128)(2,1)S(1)}, u32[]{:S(2)}, u32[]{:S(2)}) collective-permute-start(bf16[32,1024]{1,0:T(8,128)(2,1)S(1)} %get-tuple-element.22), channel_id=1, source_target_pairs={{0,16},{1,24},{2,18},{3,26},{4,20},{5,28},{6,22},{7,30},{8,17},{9,... | collective-permute-start | bytes 196616 | tf_op jit(solution)/shard_map/ppermute | solution.py:40
  24.9 1.8 %fusion.59 = (bf16[384,1,64]{2,0,1:T(8,128)(2,1)S(1)}, bf16[384,1,64]{2,0,1:T(8,128)(2,1)S(1)}) fusion(f32[64]{0:T(128)S(1)} %multiply_power_fusion, f32[384]{0:T(512)S(1)} %add_convert_fusion.2, bf16[384,1,128]{2,0,1:T(8,128)(2,1)} %bitcast.80), kind=kLoop, calls=%fused_computation.68 | loop fusion | flops 270336 | bytes 198400 | tf_op jit(solution)/shard_map/convert.11
  26.8 0.9 pad_maximum_fusion.11
  27.6 2.5 %collective-permute-start = (bf16[2,128,128]{2,1,0:T(8,128)(2,1)S(1)}, bf16[2,128,128]{2,1,0:T(8,128)(2,1)S(1)}, u32[]{:S(2)}, u32[]{:S(2)}) collective-permute-start(bf16[2,128,128]{2,1,0:T(8,128)(2,1)S(1)} %get-tuple-element.15), channel_id=1, source_target_pairs={{0,8},{8,16},{16,24},{24,32},{32,40},{40,48},{48,56},{56,64},{64,7... | collective-permute-start | bytes 196616 | tf_op jit(solution)/shard_map/ppermute | solution.py:80
  30.2 0.4 multiply_cosine_fusion.1
  30.6 0.1 pad_dynamic-slice_fusion
  30.7 0.2 copy.26
  31.0 1.3 collective-permute-start.1
  32.4 0.7 pad_maximum_fusion
  33.2 0.1 abs_compare_fusion
  33.3 0.2 compare_and_fusion
  33.6 0.1 copy.15
  33.7 0.2 copy.19
  34.0 0.2 copy.20
  34.2 1.8 %collective-permute-done.1 = bf16[2,128,128]{2,1,0:T(8,128)(2,1)S(1)} collective-permute-done((bf16[2,128,128]{2,1,0:T(8,128)(2,1)S(1)}, bf16[2,128,128]{2,1,0:T(8,128)(2,1)S(1)}, u32[]{:S(2)}, u32[]{:S(2)}) %collective-permute-start.1) | collective-permute-done | bytes 65568 | tf_op jit(solution)/shard_map/ppermute | solution.py:81
  36.0 0.1 pad_maximum_fusion.8
  36.1 0.1 copy.14
  36.3 0.1 copy.16
  36.4 0.4 fusion.73
  36.9 0.3 fusion.32
  37.3 0.4 fusion.29
  37.7 0.2 copy.22
  37.9 1.7 %convolution_convert_fusion.1 = bf16[384,2048]{1,0:T(8,128)(2,1)} fusion(bf16[256,2048]{1,0:T(8,128)(2,1)S(1)} %copy-done, bf16[48,8,2,128]{3,2,1,0:T(2,128)(2,1)S(1)} %bitcast.79), kind=kOutput, calls=%fused_computation.4 | convolution fusion | flops 403439616 | bytes 2818048 | tf_op jit(solution)/shard_map/dot_general | solution.py:172
  39.6 5.7 %all-to-all-start = ((bf16[8,48,2048]{2,1,0:T(8,128)(2,1)}), bf16[8,48,2048]{2,1,0:T(8,128)(2,1)S(1)}, u32[]{:S(2)}, u32[]{:S(2)}) async-start(bf16[8,48,2048]{2,1,0:T(8,128)(2,1)} %bitcast.65), calls=%async_computation | async-start | bytes 3145728 | tf_op jit(solution)/shard_map/all_to_all | solution.py:93
  45.3 20.6 %all-to-all-done = bf16[8,48,2048]{2,1,0:T(8,128)(2,1)S(1)} async-done(((bf16[8,48,2048]{2,1,0:T(8,128)(2,1)}), bf16[8,48,2048]{2,1,0:T(8,128)(2,1)S(1)}, u32[]{:S(2)}, u32[]{:S(2)}) %all-to-all-start) | async-done | bytes 1572896 | tf_op jit(solution)/shard_map/all_to_all | solution.py:93
  65.9 0.2 convert_reduce_fusion.1
  66.1 0.1 multiply_reduce_fusion.1
  66.3 1.2 fusion.35
  67.5 0.1 fusion.37
  67.6 0.2 broadcast_in_dim.23
  67.8 22.9 %all_to_all.15 = bf16[8,48,2048]{2,1,0:T(8,128)(2,1)S(1)} all-to-all(bf16[8,48,2048]{2,1,0:T(8,128)(2,1)S(1)} %broadcast_in_dim.23), channel_id=1, replica_groups={{0,2,4,6,8,10,12,14},{1,3,5,7,9,11,13,15},{16,18,20,22,24,26,28,30},{17..., dimensions={0} | all-to-all | bytes 3145728 | tf_op jit(solution)/shard_map/all_to_all | solution.py:30
  90.8 3.7 %collective-permute-start.6 = (bf16[384,2048]{1,0:T(8,128)(2,1)S(1)}, bf16[384,2048]{1,0:T(8,128)(2,1)}, u32[]{:S(2)}, u32[]{:S(2)}) collective-permute-start(bf16[384,2048]{1,0:T(8,128)(2,1)S(1)} %bitcast.66), channel_id=1, source_target_pairs={{0,1},{1,0},{2,3},{3,2},{4,5},{5,4},{6,7},{7,6},{8,9},{9,8},{10,11... | collective-permute-start | bytes 4718600 | tf_op jit(solution)/shard_map/ppermute | solution.py:17
  94.4 3.1 %collective-permute-done.6 = bf16[384,2048]{1,0:T(8,128)(2,1)} collective-permute-done((bf16[384,2048]{1,0:T(8,128)(2,1)S(1)}, bf16[384,2048]{1,0:T(8,128)(2,1)}, u32[]{:S(2)}, u32[]{:S(2)}) %collective-permute-start.6) | collective-permute-done | bytes 1572896 | tf_op jit(solution)/shard_map/ppermute | solution.py:17
  97.6 7.1 %all-gather.2.cloned.1.call-done = bf16[2048,1024]{1,0:T(8,128)(2,1)} async-done(((bf16[128,1024]{1,0:T(8,128)(2,1)}), bf16[2048,1024]{1,0:T(8,128)(2,1)}) %all-gather.2.cloned.1.call-update) | async-done | bytes 4194320 | tf_op jit(solution)/shard_map/all_gather | solution.py:60
  104.6 5.7 %convolution_convert_fusion = bf16[384,2048]{1,0:T(8,128)(2,1)} fusion(bf16[2048,1024]{1,0:T(8,128)(2,1)} %all-gather.2.cloned.1.call-done, bf16[384,2048]{1,0:T(8,128)(2,1)} %collective-permute-done.6), kind=kOutput, calls=%fused_computation.3 | convolution fusion | flops 1611988992 | bytes 7340032 | tf_op jit(solution)/shard_map/dot_general | solution.py:70
  110.4 11.1 %collective-permute-start.7 = (bf16[384,2048]{1,0:T(8,128)(2,1)}, bf16[384,2048]{1,0:T(8,128)(2,1)S(1)}, u32[]{:S(2)}, u32[]{:S(2)}) collective-permute-start(bf16[384,2048]{1,0:T(8,128)(2,1)} %convolution_convert_fusion), channel_id=1, source_target_pairs={{0,1},{1,0},{2,3},{3,2},{4,5},{5,4},{6,7},{7,6},{8,9},{9,8},{10,11... | collective-permute-start | bytes 4718600 | tf_op jit(solution)/shard_map/ppermute | solution.py:17
  121.5 2.6 %fusion.26 = bf16[384,512]{1,0:T(8,128)(2,1)S(1)} fusion(bf16[384,2048]{1,0:T(8,128)(2,1)S(1)} %bitcast.67, bf16[2048,1024]{1,0:T(8,128)(2,1)} %all-gather.2.cloned.1.call-done), kind=kOutput, calls=%fused_computation.20 | convolution fusion | flops 805896192 | bytes 4063232 | tf_op jit(solution)/shard_map/dot_general | solution.py:64
  124.1 0.7 collective-permute-done.7
  124.7 1.0 add_convert_fusion
  125.7 25.8 %all_to_all.16 = bf16[8,48,2048]{2,1,0:T(8,128)(2,1)S(1)} all-to-all(bf16[8,48,2048]{2,1,0:T(8,128)(2,1)S(1)} %bitcast.68), channel_id=1, replica_groups={{0,2,4,6,8,10,12,14},{1,3,5,7,9,11,13,15},{16,18,20,22,24,26,28,30},{17..., dimensions={0} | all-to-all | bytes 3145728 | tf_op jit(solution)/shard_map/all_to_all | solution.py:30
  151.5 0.2 convert_reduce_fusion
  151.8 0.1 multiply_reduce_fusion
  151.9 0.3 copy-done.5
  152.2 0.8 fusion.38
  (40 shorter events, 0.5 us)
Async XLA Ops:
  6.5 31.3 %copy-start = (bf16[256,2048]{1,0:T(8,128)(2,1)S(1)}, bf16[256,2048]{1,0:T(8,128)(2,1)}, u32[]{:S(2)}) copy-start(bf16[256,2048]{1,0:T(8,128)(2,1)} %param.18) | copy-start | bytes 3145732
  6.5 24.1 %copy-start.3 = (s32[24576]{0:T(1024)S(1)}, s32[24576]{0:T(1024)}, u32[]{:S(2)}) copy-start(s32[24576]{0:T(1024)} %param.16) | copy-start | bytes 294916
  6.5 24.2 %copy-start.2 = (bf16[384,256]{1,0:T(8,128)(2,1)S(1)}, bf16[384,256]{1,0:T(8,128)(2,1)}, u32[]{:S(2)}) copy-start(bf16[384,256]{1,0:T(8,128)(2,1)} %param.12) | copy-start | bytes 589828
  6.5 98.1 %all-gather.2.cloned.1.call-start = ((), (), s32[]{:S(2)}) async-start(), calls=%async_computation.3 | async-start | bytes 4456448 | tf_op jit(solution)/shard_map/all_gather | solution.py:60
  7.5 23.5 %collective-permute-start.4 = (bf16[32,1024]{1,0:T(8,128)(2,1)S(1)}, bf16[32,1024]{1,0:T(8,128)(2,1)S(1)}, u32[]{:S(2)}, u32[]{:S(2)}) collective-permute-start(bf16[32,1024]{1,0:T(8,128)(2,1)S(1)} %get-tuple-element.21), channel_id=1, source_target_pairs={{0,1},{1,9},{2,3},{3,11},{4,5},{5,13},{6,7},{7,15},{8,0},{9,8},{10... | collective-permute-start | bytes 196616 | tf_op jit(solution)/shard_map/ppermute | solution.py:40
  11.6 20.7 %collective-permute-start.2 = (bf16[32,1024]{1,0:T(8,128)(2,1)S(1)}, bf16[32,1024]{1,0:T(8,128)(2,1)S(1)}, u32[]{:S(2)}, u32[]{:S(2)}) collective-permute-start(bf16[32,1024]{1,0:T(8,128)(2,1)S(1)} %get-tuple-element.21), channel_id=1, source_target_pairs={{0,17},{1,25},{2,19},{3,27},{4,21},{5,29},{6,23},{7,31},{8,16},{9,... | collective-permute-start | bytes 196616 | tf_op jit(solution)/shard_map/ppermute | solution.py:40
  15.6 16.7 %collective-permute-start.5 = (bf16[32,1024]{1,0:T(8,128)(2,1)S(1)}, bf16[32,1024]{1,0:T(8,128)(2,1)S(1)}, u32[]{:S(2)}, u32[]{:S(2)}) collective-permute-start(bf16[32,1024]{1,0:T(8,128)(2,1)S(1)} %get-tuple-element.22), channel_id=1, source_target_pairs={{0,0},{1,8},{2,2},{3,10},{4,4},{5,12},{6,6},{7,14},{8,1},{9,9},{10... | collective-permute-start | bytes 196616 | tf_op jit(solution)/shard_map/ppermute | solution.py:40
  21.8 10.6 %collective-permute-start.3 = (bf16[32,1024]{1,0:T(8,128)(2,1)S(1)}, bf16[32,1024]{1,0:T(8,128)(2,1)S(1)}, u32[]{:S(2)}, u32[]{:S(2)}) collective-permute-start(bf16[32,1024]{1,0:T(8,128)(2,1)S(1)} %get-tuple-element.22), channel_id=1, source_target_pairs={{0,16},{1,24},{2,18},{3,26},{4,20},{5,28},{6,22},{7,30},{8,17},{9,... | collective-permute-start | bytes 196616 | tf_op jit(solution)/shard_map/ppermute | solution.py:40
  27.6 5.9 %copy-start.1 = (bf16[384,128]{1,0:T(8,128)(2,1)S(1)}, bf16[384,128]{1,0:T(8,128)(2,1)}, u32[]{:S(2)}) copy-start(bf16[384,128]{1,0:T(8,128)(2,1)} %param.14) | copy-start | bytes 294916
  27.6 6.5 %collective-permute-start = (bf16[2,128,128]{2,1,0:T(8,128)(2,1)S(1)}, bf16[2,128,128]{2,1,0:T(8,128)(2,1)S(1)}, u32[]{:S(2)}, u32[]{:S(2)}) collective-permute-start(bf16[2,128,128]{2,1,0:T(8,128)(2,1)S(1)} %get-tuple-element.15), channel_id=1, source_target_pairs={{0,8},{8,16},{16,24},{24,32},{32,40},{40,48},{48,56},{56,64},{64,7... | collective-permute-start | bytes 196616 | tf_op jit(solution)/shard_map/ppermute | solution.py:80
  31.0 5.0 %collective-permute-start.1 = (bf16[2,128,128]{2,1,0:T(8,128)(2,1)S(1)}, bf16[2,128,128]{2,1,0:T(8,128)(2,1)S(1)}, u32[]{:S(2)}, u32[]{:S(2)}) collective-permute-start(bf16[2,128,128]{2,1,0:T(8,128)(2,1)S(1)} %get-tuple-element.16), channel_id=1, source_target_pairs={{8,0},{16,8},{24,16},{32,24},{40,32},{48,40},{56,48},{64,56},{72,6... | collective-permute-start | bytes 196616 | tf_op jit(solution)/shard_map/ppermute | solution.py:81
  36.1 0.7 copy-start.7
  39.6 26.3 %all-to-all-start = ((bf16[8,48,2048]{2,1,0:T(8,128)(2,1)}), bf16[8,48,2048]{2,1,0:T(8,128)(2,1)S(1)}, u32[]{:S(2)}, u32[]{:S(2)}) async-start(bf16[8,48,2048]{2,1,0:T(8,128)(2,1)} %bitcast.65), calls=%async_computation | async-start | bytes 3145728 | tf_op jit(solution)/shard_map/all_to_all | solution.py:93
  45.3 21.0 %copy-start.4 = (f32[2048]{0:T(1024)S(1)}, f32[2048]{0:T(1024)}, u32[]{:S(2)}) copy-start(f32[2048]{0:T(1024)} %param.19) | copy-start | bytes 24580
  45.3 22.2 %copy-start.6 = (f32[2048]{0:T(1024)S(1)}, f32[2048]{0:T(1024)}, u32[]{:S(2)}) copy-start(f32[2048]{0:T(1024)} %param.22) | copy-start | bytes 24580
  90.8 6.8 %collective-permute-start.6 = (bf16[384,2048]{1,0:T(8,128)(2,1)S(1)}, bf16[384,2048]{1,0:T(8,128)(2,1)}, u32[]{:S(2)}, u32[]{:S(2)}) collective-permute-start(bf16[384,2048]{1,0:T(8,128)(2,1)S(1)} %bitcast.66), channel_id=1, source_target_pairs={{0,1},{1,0},{2,3},{3,2},{4,5},{5,4},{6,7},{7,6},{8,9},{9,8},{10,11... | collective-permute-start | bytes 4718600 | tf_op jit(solution)/shard_map/ppermute | solution.py:17
  110.3 14.4 %copy-start.8 = (bf16[2048,1024]{1,0:T(8,128)(2,1)S(1)}, bf16[2048,1024]{1,0:T(8,128)(2,1)}, u32[]{:S(2)}) copy-start(bf16[2048,1024]{1,0:T(8,128)(2,1)} %all-gather.2.cloned.1.call-done) | copy-start | bytes 12582916
  110.4 14.4 %collective-permute-start.7 = (bf16[384,2048]{1,0:T(8,128)(2,1)}, bf16[384,2048]{1,0:T(8,128)(2,1)S(1)}, u32[]{:S(2)}, u32[]{:S(2)}) collective-permute-start(bf16[384,2048]{1,0:T(8,128)(2,1)} %convolution_convert_fusion), channel_id=1, source_target_pairs={{0,1},{1,0},{2,3},{3,2},{4,5},{5,4},{6,7},{7,6},{8,9},{9,8},{10,11... | collective-permute-start | bytes 4718600 | tf_op jit(solution)/shard_map/ppermute | solution.py:17
  151.5 0.7 copy-start.5
Sparse Core Ops, SparseCore 0:
  33.3 71.3 all-gather.1

commit v5 on v3

--- a/solution.py
+++ b/solution.py
@@ -36,19 +36,12 @@
         jnp.concatenate([w[:, at : at + 512] for w in (up_proj, down_rows)], axis=1)
         for at in (0, 512)
     ]
-    pieces = jnp.concatenate([jnp.broadcast_to(h[None], (4, 32, 1024)) for h in halved])
-    rings = [
-        [device(z, y, x, core) for core in range(2) for y in range(4)]
-        for z in range(16)
-        for x in range(4)
-    ]
-    dealt = lax.all_to_all(
-        pieces, ("sp", "tp"), 0, 0, axis_index_groups=rings, tiled=True
+    along_y = [[4 * z + y for y in range(4)] for z in range(16)]
+    along_z = [[4 * z + y for z in range(16)] for y in range(4)]
+    rows = lax.all_to_all(jnp.stack(halved * 2), "sp", 0, 0, axis_index_groups=along_y, tiled=True)
+    return lax.all_gather(
+        rows.reshape(128, 1024), "sp", axis=0, tiled=True, axis_index_groups=along_z
     )
-    block = lax.axis_index("sp") % 2
-    rows = lax.dynamic_slice_in_dim(dealt, 4 * block, 4, axis=0).reshape(128, 1024)
-    along_z = [[4 * z + y for z in range(16)] for y in range(4)]
-    return lax.all_gather(rows, "sp", axis=0, tiled=True, axis_index_groups=along_z)
 
 
 def ffn_up(normed, both):

time: 165 us -> 153 us (0.927)
  waiting for transfers between devices: 44.9 us -> 33.9 us
  starting transfers between devices: 32.5 us -> 34.5 us
  other arithmetic: 7.82 us -> 5.92 us
    all_to_all x1, waiting for transfers between devices: 8.53 us -> 0.01 us  [group_weights(): lax.all_to_all(jnp.stack(halved * 2), 'sp', 0, 0, axis_index_groups=along...]
    all_to_all x1, starting transfers between devices: 3.78 us -> 9.4 us  [summed_on_arrival(): lax.all_to_all(pieces, axis, split_axis=0, concat_axis=0, tiled=True)]
    all_gather x1, waiting for transfers between devices: 11.9 us -> 7.34 us  [group_weights(): lax.all_gather(rows.reshape(128, 1024), 'sp', axis=0, tiled=True, axis_in...]
    all_to_all x1, starting transfers between devices: 8.16 us -> 5 us  [group_weights(): lax.all_to_all(jnp.stack(halved * 2), 'sp', 0, 0, axis_index_groups=along...]
    ppermute x1, waiting for transfers between devices: 0.01 us -> 2.13 us  [padded(): after = lax.ppermute(first, axis, down)]
  transfers between devices with their start and end apart: 7 -> 7, of which waited for: 5 -> 5; matrix products, arithmetic and copies ran while one was open for 8% -> 7% of each run, Pallas kernels for 0% -> 0%
where the time goes in v5:
time: 153 us
  blocking collectives  48.7 us (32%)
  starting transfers between devices  34.5 us (23%)
  waiting for transfers between devices  33.9 us (22%)
  between operations  13.7 us (9%)
  matrix products  11.9 us (8%)
  other arithmetic  5.92 us (4%)
  local copies, waits for them, and re-layouts  4.23 us (3%)
    all_to_all x2, blocking collectives, exchanged(): lax.all_to_all(pieces, ('sp', 'tp'), 0, 0, axis_index_groups=token_groups...  48.7 us
    all_to_all x1, waiting for transfers between devices, summed_on_arrival(): lax.all_to_all(pieces, axis, split_axis=0, concat_axis=0, tiled=True)  20.6 us
    ppermute x2, starting transfers between devices, swapped(): return lax.ppermute(shard, 'tp', [(i, i ^ 1) for i in range(8)])  15.4 us
    all_to_all x1, starting transfers between devices, summed_on_arrival(): lax.all_to_all(pieces, axis, split_axis=0, concat_axis=0, tiled=True)  9.4 us
    all_gather x1, waiting for transfers between devices, group_weights(): lax.all_gather(rows.reshape(128, 1024), 'sp', axis=0, tiled=True, axis_in...  7.34 us
    dot_general x2, matrix products, ffn_down(): lax.dot_general(hidden, both[:, 512:], across, preferred_element_type=jnp...  6.72 us
    all_to_all x1, starting transfers between devices, group_weights(): lax.all_to_all(jnp.stack(halved * 2), 'sp', 0, 0, axis_index_groups=along...  5 us
    ppermute x2, waiting for transfers between devices, swapped(): return lax.ppermute(shard, 'tp', [(i, i ^ 1) for i in range(8)])  3.8 us
  transfers between devices with their start and end apart: 7, of which 5 were waited for; matrix products, arithmetic and copies ran while one was open for 7% of the time, Pallas kernels for 0%

profile of v5, /device:TPU:1, one launch (start us, length us, event | category | flops | bytes accessed | tf_op | source)
XLA Modules:
  0.0 152.8 jit_solution(12239071226685344175)
XLA Ops:
  6.5 0.9 fusion.71
  7.4 0.8 fusion.72
  8.2 0.7 pad_maximum_fusion
  9.0 5.0 %all-to-all-start.2 = ((bf16[4,32,1024]{2,1,0:T(8,128)(2,1)}), bf16[4,32,1024]{2,1,0:T(8,128)(2,1)S(1)}, u32[]{:S(2)}, u32[]{:S(2)}) async-start(bf16[4,32,1024]{2,1,0:T(8,128)(2,1)} %pad_maximum_fusion), calls=%async_computation.2 | async-start | bytes 524288 | tf_op jit(solution)/shard_map/all_to_all | solution.py:41
  14.0 0.8 fusion.59
  14.9 0.1 pad_maximum_fusion.11
  15.0 3.4 %collective-permute-start = (bf16[2,128,128]{2,1,0:T(8,128)(2,1)S(1)}, bf16[2,128,128]{2,1,0:T(8,128)(2,1)S(1)}, u32[]{:S(2)}, u32[]{:S(2)}) collective-permute-start(bf16[2,128,128]{2,1,0:T(8,128)(2,1)S(1)} %get-tuple-element.15), channel_id=1, source_target_pairs={{0,8},{8,16},{16,24},{24,32},{32,40},{40,48},{48,56},{56,64},{64,7... | collective-permute-start | bytes 196616 | tf_op jit(solution)/shard_map/ppermute | solution.py:64
  18.4 1.3 collective-permute-start.1
  19.7 0.4 multiply_cosine_fusion.1
  20.1 0.1 pad_dynamic-slice_fusion
  20.2 0.2 copy.26
  20.5 0.7 copy-done.1
  21.2 0.1 dynamic-slice_bitcast_fusion
  21.3 0.1 abs_compare_fusion
  21.4 0.2 compare_and_fusion
  21.6 0.1 copy.15
  21.8 0.2 copy.19
  22.0 0.2 copy.20
  22.2 2.1 %collective-permute-done.1 = bf16[2,128,128]{2,1,0:T(8,128)(2,1)S(1)} collective-permute-done((bf16[2,128,128]{2,1,0:T(8,128)(2,1)S(1)}, bf16[2,128,128]{2,1,0:T(8,128)(2,1)S(1)}, u32[]{:S(2)}, u32[]{:S(2)}) %collective-permute-start.1) | collective-permute-done | bytes 65568 | tf_op jit(solution)/shard_map/ppermute | solution.py:65
  24.4 0.1 pad_maximum_fusion.8
  24.5 0.1 copy.14
  24.6 0.1 copy.16
  24.8 0.4 fusion.73
  25.3 0.3 fusion.32
  25.6 0.4 fusion.29
  26.0 0.2 copy.22
  26.2 1.7 %convolution_convert_fusion.1 = bf16[384,2048]{1,0:T(8,128)(2,1)} fusion(bf16[256,2048]{1,0:T(8,128)(2,1)S(1)} %copy-done, bf16[48,8,2,128]{3,2,1,0:T(2,128)(2,1)S(1)} %bitcast.85), kind=kOutput, calls=%fused_computation.4 | convolution fusion | flops 403439616 | bytes 2818048 | tf_op jit(solution)/shard_map/dot_general | solution.py:156
  28.0 9.4 %all-to-all-start = ((bf16[8,48,2048]{2,1,0:T(8,128)(2,1)}), bf16[8,48,2048]{2,1,0:T(8,128)(2,1)S(1)}, u32[]{:S(2)}, u32[]{:S(2)}) async-start(bf16[8,48,2048]{2,1,0:T(8,128)(2,1)} %bitcast.70), calls=%async_computation | async-start | bytes 3145728 | tf_op jit(solution)/shard_map/all_to_all | solution.py:77
  37.4 20.6 %all-to-all-done = bf16[8,48,2048]{2,1,0:T(8,128)(2,1)S(1)} async-done(((bf16[8,48,2048]{2,1,0:T(8,128)(2,1)}), bf16[8,48,2048]{2,1,0:T(8,128)(2,1)S(1)}, u32[]{:S(2)}, u32[]{:S(2)}) %all-to-all-start) | async-done | bytes 1572896 | tf_op jit(solution)/shard_map/all_to_all | solution.py:77
  58.0 0.2 convert_reduce_fusion.1
  58.2 0.1 multiply_reduce_fusion.1
  58.4 1.2 fusion.35
  59.6 0.1 fusion.37
  59.7 0.2 broadcast_in_dim.23
  59.9 23.0 %all_to_all.20 = bf16[8,48,2048]{2,1,0:T(8,128)(2,1)S(1)} all-to-all(bf16[8,48,2048]{2,1,0:T(8,128)(2,1)S(1)} %broadcast_in_dim.23), channel_id=1, replica_groups={{0,2,4,6,8,10,12,14},{1,3,5,7,9,11,13,15},{16,18,20,22,24,26,28,30},{17..., dimensions={0} | all-to-all | bytes 3145728 | tf_op jit(solution)/shard_map/all_to_all | solution.py:28
  82.9 4.0 %collective-permute-start.2 = (bf16[384,2048]{1,0:T(8,128)(2,1)S(1)}, bf16[384,2048]{1,0:T(8,128)(2,1)}, u32[]{:S(2)}, u32[]{:S(2)}) collective-permute-start(bf16[384,2048]{1,0:T(8,128)(2,1)S(1)} %bitcast.71), channel_id=1, source_target_pairs={{0,1},{1,0},{2,3},{3,2},{4,5},{5,4},{6,7},{7,6},{8,9},{9,8},{10,11... | collective-permute-start | bytes 4718600 | tf_op jit(solution)/shard_map/ppermute | solution.py:15
  86.9 3.1 %collective-permute-done.2 = bf16[384,2048]{1,0:T(8,128)(2,1)} collective-permute-done((bf16[384,2048]{1,0:T(8,128)(2,1)S(1)}, bf16[384,2048]{1,0:T(8,128)(2,1)}, u32[]{:S(2)}, u32[]{:S(2)}) %collective-permute-start.2) | collective-permute-done | bytes 1572896 | tf_op jit(solution)/shard_map/ppermute | solution.py:15
  90.1 7.3 %all-gather.2.cloned.1.call-done = bf16[2048,1024]{1,0:T(8,128)(2,1)} async-done(((bf16[128,1024]{1,0:T(8,128)(2,1)}), bf16[2048,1024]{1,0:T(8,128)(2,1)}) %all-gather.2.cloned.1.call-update) | async-done | bytes 4194320 | tf_op jit(solution)/shard_map/all_gather | solution.py:42
  97.4 5.7 %convolution_convert_fusion = bf16[384,2048]{1,0:T(8,128)(2,1)} fusion(bf16[2048,1024]{1,0:T(8,128)(2,1)} %all-gather.2.cloned.1.call-done, bf16[384,2048]{1,0:T(8,128)(2,1)} %collective-permute-done.2), kind=kOutput, calls=%fused_computation.3 | convolution fusion | flops 1611988992 | bytes 7340032 | tf_op jit(solution)/shard_map/dot_general | solution.py:54
  103.1 11.4 %collective-permute-start.3 = (bf16[384,2048]{1,0:T(8,128)(2,1)}, bf16[384,2048]{1,0:T(8,128)(2,1)S(1)}, u32[]{:S(2)}, u32[]{:S(2)}) collective-permute-start(bf16[384,2048]{1,0:T(8,128)(2,1)} %convolution_convert_fusion), channel_id=1, source_target_pairs={{0,1},{1,0},{2,3},{3,2},{4,5},{5,4},{6,7},{7,6},{8,9},{9,8},{10,11... | collective-permute-start | bytes 4718600 | tf_op jit(solution)/shard_map/ppermute | solution.py:15
  114.5 2.6 %fusion.26 = bf16[384,512]{1,0:T(8,128)(2,1)S(1)} fusion(bf16[384,2048]{1,0:T(8,128)(2,1)S(1)} %bitcast.72, bf16[2048,1024]{1,0:T(8,128)(2,1)} %all-gather.2.cloned.1.call-done), kind=kOutput, calls=%fused_computation.20 | convolution fusion | flops 805896192 | bytes 4063232 | tf_op jit(solution)/shard_map/dot_general | solution.py:48
  117.1 0.7 collective-permute-done.3
  117.8 1.0 add_convert_fusion
  118.8 25.7 %all_to_all.21 = bf16[8,48,2048]{2,1,0:T(8,128)(2,1)S(1)} all-to-all(bf16[8,48,2048]{2,1,0:T(8,128)(2,1)S(1)} %bitcast.73), channel_id=1, replica_groups={{0,2,4,6,8,10,12,14},{1,3,5,7,9,11,13,15},{16,18,20,22,24,26,28,30},{17..., dimensions={0} | all-to-all | bytes 3145728 | tf_op jit(solution)/shard_map/all_to_all | solution.py:28
  144.4 0.2 convert_reduce_fusion
  144.7 0.1 multiply_reduce_fusion
  144.8 0.3 copy-done.7
  145.1 0.8 fusion.38
  (38 shorter events, 0.4 us)
Async XLA Ops:
  6.5 19.7 %copy-start = (bf16[256,2048]{1,0:T(8,128)(2,1)S(1)}, bf16[256,2048]{1,0:T(8,128)(2,1)}, u32[]{:S(2)}) copy-start(bf16[256,2048]{1,0:T(8,128)(2,1)} %param.18) | copy-start | bytes 3145732
  6.5 7.5 %copy-start.3 = (bf16[384,128]{1,0:T(8,128)(2,1)S(1)}, bf16[384,128]{1,0:T(8,128)(2,1)}, u32[]{:S(2)}) copy-start(bf16[384,128]{1,0:T(8,128)(2,1)} %param.13) | copy-start | bytes 294916
  6.5 8.3 %copy-start.2 = (bf16[384,128]{1,0:T(8,128)(2,1)S(1)}, bf16[384,128]{1,0:T(8,128)(2,1)}, u32[]{:S(2)}) copy-start(bf16[384,128]{1,0:T(8,128)(2,1)} %param.14) | copy-start | bytes 294916
  6.5 13.6 %copy-start.5 = (s32[24576]{0:T(1024)S(1)}, s32[24576]{0:T(1024)}, u32[]{:S(2)}) copy-start(s32[24576]{0:T(1024)} %param.16) | copy-start | bytes 294916
  6.5 13.7 %copy-start.4 = (bf16[384,256]{1,0:T(8,128)(2,1)S(1)}, bf16[384,256]{1,0:T(8,128)(2,1)}, u32[]{:S(2)}) copy-start(bf16[384,256]{1,0:T(8,128)(2,1)} %param.12) | copy-start | bytes 589828
  9.0 11.5 %all-to-all-start.2 = ((bf16[4,32,1024]{2,1,0:T(8,128)(2,1)}), bf16[4,32,1024]{2,1,0:T(8,128)(2,1)S(1)}, u32[]{:S(2)}, u32[]{:S(2)}) async-start(bf16[4,32,1024]{2,1,0:T(8,128)(2,1)} %pad_maximum_fusion), calls=%async_computation.2 | async-start | bytes 524288 | tf_op jit(solution)/shard_map/all_to_all | solution.py:41
  14.0 83.4 %all-gather.2.cloned.1.call-start = ((), (), s32[]{:S(2)}) async-start(), calls=%async_computation.4 | async-start | bytes 4456448 | tf_op jit(solution)/shard_map/all_gather | solution.py:42
  15.0 7.2 %collective-permute-start = (bf16[2,128,128]{2,1,0:T(8,128)(2,1)S(1)}, bf16[2,128,128]{2,1,0:T(8,128)(2,1)S(1)}, u32[]{:S(2)}, u32[]{:S(2)}) collective-permute-start(bf16[2,128,128]{2,1,0:T(8,128)(2,1)S(1)} %get-tuple-element.15), channel_id=1, source_target_pairs={{0,8},{8,16},{16,24},{24,32},{32,40},{40,48},{48,56},{56,64},{64,7... | collective-permute-start | bytes 196616 | tf_op jit(solution)/shard_map/ppermute | solution.py:64
  18.4 6.0 %collective-permute-start.1 = (bf16[2,128,128]{2,1,0:T(8,128)(2,1)S(1)}, bf16[2,128,128]{2,1,0:T(8,128)(2,1)S(1)}, u32[]{:S(2)}, u32[]{:S(2)}) collective-permute-start(bf16[2,128,128]{2,1,0:T(8,128)(2,1)S(1)} %get-tuple-element.16), channel_id=1, source_target_pairs={{8,0},{16,8},{24,16},{32,24},{40,32},{48,40},{56,48},{64,56},{72,6... | collective-permute-start | bytes 196616 | tf_op jit(solution)/shard_map/ppermute | solution.py:65
  20.5 0.7 copy-start.1
  24.5 0.7 copy-start.9
  28.0 30.0 %all-to-all-start = ((bf16[8,48,2048]{2,1,0:T(8,128)(2,1)}), bf16[8,48,2048]{2,1,0:T(8,128)(2,1)S(1)}, u32[]{:S(2)}, u32[]{:S(2)}) async-start(bf16[8,48,2048]{2,1,0:T(8,128)(2,1)} %bitcast.70), calls=%async_computation | async-start | bytes 3145728 | tf_op jit(solution)/shard_map/all_to_all | solution.py:77
  37.4 21.0 %copy-start.6 = (f32[2048]{0:T(1024)S(1)}, f32[2048]{0:T(1024)}, u32[]{:S(2)}) copy-start(f32[2048]{0:T(1024)} %param.19) | copy-start | bytes 24580
  37.4 22.2 %copy-start.8 = (f32[2048]{0:T(1024)S(1)}, f32[2048]{0:T(1024)}, u32[]{:S(2)}) copy-start(f32[2048]{0:T(1024)} %param.22) | copy-start | bytes 24580
  82.9 7.1 %collective-permute-start.2 = (bf16[384,2048]{1,0:T(8,128)(2,1)S(1)}, bf16[384,2048]{1,0:T(8,128)(2,1)}, u32[]{:S(2)}, u32[]{:S(2)}) collective-permute-start(bf16[384,2048]{1,0:T(8,128)(2,1)S(1)} %bitcast.71), channel_id=1, source_target_pairs={{0,1},{1,0},{2,3},{3,2},{4,5},{5,4},{6,7},{7,6},{8,9},{9,8},{10,11... | collective-permute-start | bytes 4718600 | tf_op jit(solution)/shard_map/ppermute | solution.py:15
  103.1 14.6 %copy-start.10 = (bf16[2048,1024]{1,0:T(8,128)(2,1)S(1)}, bf16[2048,1024]{1,0:T(8,128)(2,1)}, u32[]{:S(2)}) copy-start(bf16[2048,1024]{1,0:T(8,128)(2,1)} %all-gather.2.cloned.1.call-done) | copy-start | bytes 12582916
  103.1 14.6 %collective-permute-start.3 = (bf16[384,2048]{1,0:T(8,128)(2,1)}, bf16[384,2048]{1,0:T(8,128)(2,1)S(1)}, u32[]{:S(2)}, u32[]{:S(2)}) collective-permute-start(bf16[384,2048]{1,0:T(8,128)(2,1)} %convolution_convert_fusion), channel_id=1, source_target_pairs={{0,1},{1,0},{2,3},{3,2},{4,5},{5,4},{6,7},{7,6},{8,9},{9,8},{10,11... | collective-permute-start | bytes 4718600 | tf_op jit(solution)/shard_map/ppermute | solution.py:15
  144.4 0.7 copy-start.7
Sparse Core Ops, SparseCore 0:
  21.3 76.0 all-gather.1

commit v6 on v5

--- a/solution.py
+++ b/solution.py
@@ -1,10 +1,13 @@
 import jax
 import jax.numpy as jnp
 from jax import lax
+from jax.experimental import pallas as pl
+from jax.experimental.pallas import tpu as pltpu
 from jax.sharding import PartitionSpec as P
 
 HD = 128
 WINDOW = 128
+CHUNKS = 4
 
 
 def device(z, y, x, core):
@@ -52,6 +55,53 @@
 def ffn_down(hidden, both):
     across = (((1,), (1,)), ((), ()))
     return lax.dot_general(hidden, both[:, 512:], across, preferred_element_type=jnp.float32)
+
+
+def ffn_kernel(tokens, both, out, held, arrivals):
+    chunks = arrivals.shape[0]
+    size = held.shape[0] // chunks
+    half = held.shape[1] // 2
+    spans = [pl.ds(k * size, size) for k in range(chunks)]
+    copies = [
+        pltpu.make_async_copy(both.at[span], held.at[span], arrivals.at[k])
+        for k, span in enumerate(spans)
+    ]
+    for copy in copies:
+        copy.start()
+    up_acts = jnp.zeros((tokens.shape[0], half), jnp.float32)
+    for copy, span in zip(copies, spans):
+        copy.wait()
+        up_acts += jnp.dot(
+            tokens[:, span], held[span, :half], preferred_element_type=jnp.float32
+        )
+    hidden = jnp.square(jax.nn.relu(up_acts)).astype(jnp.bfloat16)
+    for span in spans:
+        out[:, span] = lax.dot_general(
+            hidden,
+            held[span, half:],
+            (((1,), (1,)), ((), ())),
+            preferred_element_type=jnp.float32,
+        ).astype(jnp.bfloat16)
+
+
+def ffn_in_kernel(tokens, both):
+    return pl.pallas_call(
+        ffn_kernel,
+        out_shape=jax.ShapeDtypeStruct(tokens.shape, jnp.bfloat16),
+        in_specs=[
+            pl.BlockSpec(memory_space=pltpu.VMEM),
+            pl.BlockSpec(memory_space=pl.ANY),
+        ],
+        out_specs=pl.BlockSpec(memory_space=pltpu.VMEM),
+        scratch_shapes=[
+            pltpu.VMEM(both.shape, jnp.bfloat16),
+            pltpu.SemaphoreType.DMA((CHUNKS,)),
+        ],
+        cost_estimate=pl.CostEstimate(
+            flops=2 * 384 * 2048 * 1024, bytes_accessed=7 << 20, transcendentals=0
+        ),
+        name="ffn_other",
+    )(tokens, both)
 
 
 def padded(shard, sides, width):
@@ -161,7 +211,7 @@
     normed = exchanged(jnp.broadcast_to(own_normed[None], (8, *own_normed.shape)))
     normed = normed.reshape(-1, 2048)
     other_normed = swapped(normed)
-    other_part = ffn_down(ffn_up(other_normed, weights), weights).astype(jnp.bfloat16)
+    other_part = ffn_in_kernel(other_normed, weights)
     received = swapped(other_part)
     hidden = lax.optimization_barrier(ffn_up(normed, weights))
     own_part = ffn_down(hidden, weights)

time: 153 us -> 155 us (1.013)
  Pallas kernels: 0 us -> 6.11 us
  matrix products: 11.9 us -> 6.68 us
  waiting for transfers between devices: 33.9 us -> 31.8 us
    pallas_call x0 -> x1, Pallas kernels: none -> 6.11 us  [ffn_in_kernel(): pl.pallas_call(ffn_kernel, out_shape=jax.ShapeDtypeStruct(tokens.shape, j...]
    dot_general x2 -> x1, matrix products: 6.72 us -> 1.01 us  [ffn_down(): lax.dot_general(hidden, both[:, 512:], across, preferred_element_type=jnp...]
  transfers between devices with their start and end apart: 7 -> 7, of which waited for: 5 -> 4; matrix products, arithmetic and copies ran while one was open for 7% -> 8% of each run, Pallas kernels for 0% -> 0%
where the time goes in v6:
time: 155 us; the launch traced here: 154 us
  blocking collectives  49.2 us (32%)
  starting transfers between devices  34.6 us (22%)
  waiting for transfers between devices  31.8 us (21%)
  between operations  13.7 us (9%)
  matrix products  6.68 us (4%)
  other arithmetic  6.43 us (4%)
  Pallas kernels  6.11 us (4%)
  local copies, waits for them, and re-layouts  5.43 us (4%)
    all_to_all x2, blocking collectives, exchanged(): lax.all_to_all(pieces, ('sp', 'tp'), 0, 0, axis_index_groups=token_groups...  49.2 us
    all_to_all x1, waiting for transfers between devices, summed_on_arrival(): lax.all_to_all(pieces, axis, split_axis=0, concat_axis=0, tiled=True)  20.6 us
    ppermute x2, starting transfers between devices, swapped(): return lax.ppermute(shard, 'tp', [(i, i ^ 1) for i in range(8)])  15.5 us
    all_to_all x1, starting transfers between devices, summed_on_arrival(): lax.all_to_all(pieces, axis, split_axis=0, concat_axis=0, tiled=True)  9.42 us
    pallas_call x1, Pallas kernels, ffn_in_kernel(): pl.pallas_call(ffn_kernel, out_shape=jax.ShapeDtypeStruct(tokens.shape, j...  6.11 us
    all_gather x1, waiting for transfers between devices, group_weights(): lax.all_gather(rows.reshape(128, 1024), 'sp', axis=0, tiled=True, axis_in...  6.05 us
    all_to_all x1, starting transfers between devices, group_weights(): lax.all_to_all(jnp.stack(halved * 2), 'sp', 0, 0, axis_index_groups=along...  5 us
    ppermute x1, starting transfers between devices, padded(): before = lax.ppermute(last, axis, up)  3.37 us
  transfers between devices with their start and end apart: 7, of which 4 were waited for; matrix products, arithmetic and copies ran while one was open for 8% of the time, Pallas kernels for 0%

profile of v6, /device:TPU:1, one launch (start us, length us, event | category | flops | bytes accessed | tf_op | source)
XLA Modules:
  0.0 154.0 jit_solution(3502079545071065436)
XLA Ops:
  6.5 0.9 fusion.53
  7.4 0.8 fusion.54
  8.2 0.7 pad_maximum_fusion
  9.0 5.0 %all-to-all-start.2 = ((bf16[4,32,1024]{2,1,0:T(8,128)(2,1)}), bf16[4,32,1024]{2,1,0:T(8,128)(2,1)S(1)}, u32[]{:S(2)}, u32[]{:S(2)}) async-start(bf16[4,32,1024]{2,1,0:T(8,128)(2,1)} %pad_maximum_fusion), calls=%async_computation.2 | async-start | bytes 524288 | tf_op jit(solution)/shard_map/all_to_all | solution.py:44
  14.0 0.8 fusion.42
  14.9 0.1 pad_maximum_fusion.11
  15.0 3.4 %collective-permute-start = (bf16[2,128,128]{2,1,0:T(8,128)(2,1)S(1)}, bf16[2,128,128]{2,1,0:T(8,128)(2,1)S(1)}, u32[]{:S(2)}, u32[]{:S(2)}) collective-permute-start(bf16[2,128,128]{2,1,0:T(8,128)(2,1)S(1)} %get-tuple-element.15), channel_id=1, source_target_pairs={{0,8},{8,16},{16,24},{24,32},{32,40},{40,48},{48,56},{56,64},{64,7... | collective-permute-start | bytes 196616 | tf_op jit(solution)/shard_map/ppermute | solution.py:114
  18.4 1.3 collective-permute-start.1
  19.7 0.4 multiply_cosine_fusion.1
  20.1 0.1 pad_dynamic-slice_fusion
  20.2 0.2 copy.26
  20.5 0.7 copy-done.4
  21.3 0.1 abs_compare_fusion
  21.4 0.2 compare_and_fusion
  21.6 0.1 copy.15
  21.8 0.2 copy.19
  22.0 0.2 copy.20
  22.2 2.1 %collective-permute-done.1 = bf16[2,128,128]{2,1,0:T(8,128)(2,1)S(1)} collective-permute-done((bf16[2,128,128]{2,1,0:T(8,128)(2,1)S(1)}, bf16[2,128,128]{2,1,0:T(8,128)(2,1)S(1)}, u32[]{:S(2)}, u32[]{:S(2)}) %collective-permute-start.1) | collective-permute-done | bytes 65568 | tf_op jit(solution)/shard_map/ppermute | solution.py:115
  24.4 0.1 pad_maximum_fusion.8
  24.5 0.1 copy.14
  24.6 0.1 copy.16
  24.8 0.4 fusion.55
  25.3 0.3 fusion.16
  25.6 0.4 fusion.15
  26.0 0.2 copy.22
  26.2 1.8 %convolution_convert_fusion = bf16[384,2048]{1,0:T(8,128)(2,1)} fusion(bf16[256,2048]{1,0:T(8,128)(2,1)S(1)} %copy-done, bf16[48,8,2,128]{3,2,1,0:T(2,128)(2,1)S(1)} %bitcast.84), kind=kOutput, calls=%fused_computation.3 | convolution fusion | flops 403439616 | bytes 2818048 | tf_op jit(solution)/shard_map/dot_general | solution.py:206
  28.0 9.4 %all-to-all-start = ((bf16[8,48,2048]{2,1,0:T(8,128)(2,1)}), bf16[8,48,2048]{2,1,0:T(8,128)(2,1)S(1)}, u32[]{:S(2)}, u32[]{:S(2)}) async-start(bf16[8,48,2048]{2,1,0:T(8,128)(2,1)} %bitcast.69), calls=%async_computation | async-start | bytes 3145728 | tf_op jit(solution)/shard_map/all_to_all | solution.py:127
  37.4 20.6 %all-to-all-done = bf16[8,48,2048]{2,1,0:T(8,128)(2,1)S(1)} async-done(((bf16[8,48,2048]{2,1,0:T(8,128)(2,1)}), bf16[8,48,2048]{2,1,0:T(8,128)(2,1)S(1)}, u32[]{:S(2)}, u32[]{:S(2)}) %all-to-all-start) | async-done | bytes 1572896 | tf_op jit(solution)/shard_map/all_to_all | solution.py:127
  58.0 0.2 convert_reduce_fusion.1
  58.3 0.1 multiply_reduce_fusion.1
  58.4 1.2 fusion.19
  59.6 0.1 fusion.21
  59.7 0.2 broadcast_in_dim.23
  59.9 23.0 %all_to_all.20 = bf16[8,48,2048]{2,1,0:T(8,128)(2,1)S(1)} all-to-all(bf16[8,48,2048]{2,1,0:T(8,128)(2,1)S(1)} %broadcast_in_dim.23), channel_id=1, replica_groups={{0,2,4,6,8,10,12,14},{1,3,5,7,9,11,13,15},{16,18,20,22,24,26,28,30},{17..., dimensions={0} | all-to-all | bytes 3145728 | tf_op jit(solution)/shard_map/all_to_all | solution.py:31
  83.0 1.2 copy-done.3
  84.1 4.0 %collective-permute-start.2 = (bf16[384,2048]{1,0:T(8,128)(2,1)S(1)}, bf16[384,2048]{1,0:T(8,128)(2,1)S(1)}, u32[]{:S(2)}, u32[]{:S(2)}) collective-permute-start(bf16[384,2048]{1,0:T(8,128)(2,1)S(1)} %bitcast.71), channel_id=1, source_target_pairs={{0,1},{1,0},{2,3},{3,2},{4,5},{5,4},{6,7},{7,6},{8,9},{9,8},{10,11... | collective-permute-start | bytes 4718600 | tf_op jit(solution)/shard_map/ppermute | solution.py:18
  88.1 3.0 %collective-permute-done.2.tokens = bf16[384,2048]{1,0:T(8,128)(2,1)S(1)} collective-permute-done((bf16[384,2048]{1,0:T(8,128)(2,1)S(1)}, bf16[384,2048]{1,0:T(8,128)(2,1)S(1)}, u32[]{:S(2)}, u32[]{:S(2)}) %collective-permute-start.2) | collective-permute-done | bytes 1572896 | tf_op jit(solution)/shard_map/ppermute | solution.py:18
  91.2 6.0 %all-gather.2.cloned.1.call-done.both = bf16[2048,1024]{1,0:T(8,128)(2,1)} async-done(((bf16[128,1024]{1,0:T(8,128)(2,1)}), bf16[2048,1024]{1,0:T(8,128)(2,1)}) %all-gather.2.cloned.1.call-update) | async-done | bytes 4194320 | tf_op jit(solution)/shard_map/all_gather | solution.py:45
  97.2 6.1 %ffn_other.1 = bf16[384,2048]{1,0:T(8,128)(2,1)} custom-call(bf16[384,2048]{1,0:T(8,128)(2,1)} %copy-done.2, bf16[2048,1024]{1,0:T(8,128)(2,1)} %all-gather.2.cloned.1.call-done.both), custom_call_target="tpu_custom_call" | custom-call | flops 1610612736 | bytes 7340032 | tf_op jit(solution)/shard_map/ffn_other/pallas_call | solution.py:88
  103.3 11.5 %collective-permute-start.3 = (bf16[384,2048]{1,0:T(8,128)(2,1)}, bf16[384,2048]{1,0:T(8,128)(2,1)S(1)}, u32[]{:S(2)}, u32[]{:S(2)}) collective-permute-start(bf16[384,2048]{1,0:T(8,128)(2,1)} %ffn_other.1), channel_id=1, source_target_pairs={{0,1},{1,0},{2,3},{3,2},{4,5},{5,4},{6,7},{7,6},{8,9},{9,8},{10,11... | collective-permute-start | bytes 4718600 | tf_op jit(solution)/shard_map/ppermute | solution.py:18
  114.9 3.0 %fusion.12 = bf16[384,512]{1,0:T(8,128)(2,1)S(1)} fusion(bf16[384,2048]{1,0:T(8,128)(2,1)} %bitcast.72, bf16[2048,1024]{1,0:T(8,128)(2,1)} %all-gather.2.cloned.1.call-done.both), kind=kOutput, calls=%fused_computation.13 | convolution fusion | flops 805896192 | bytes 4063232 | tf_op jit(solution)/shard_map/dot_general | solution.py:51
  118.0 1.0 fusion
  119.0 0.5 add_convert_fusion
  119.5 26.1 %all_to_all.21 = bf16[8,48,2048]{2,1,0:T(8,128)(2,1)S(1)} all-to-all(bf16[8,48,2048]{2,1,0:T(8,128)(2,1)S(1)} %bitcast.70), channel_id=1, replica_groups={{0,2,4,6,8,10,12,14},{1,3,5,7,9,11,13,15},{16,18,20,22,24,26,28,30},{17..., dimensions={0} | all-to-all | bytes 3145728 | tf_op jit(solution)/shard_map/all_to_all | solution.py:31
  145.7 0.2 convert_reduce_fusion
  145.9 0.1 multiply_reduce_fusion
  146.0 0.3 copy-done.10
  146.4 0.8 fusion.22
  (43 shorter events, 0.5 us)
Async XLA Ops:
  6.5 19.7 %copy-start = (bf16[256,2048]{1,0:T(8,128)(2,1)S(1)}, bf16[256,2048]{1,0:T(8,128)(2,1)}, u32[]{:S(2)}) copy-start(bf16[256,2048]{1,0:T(8,128)(2,1)} %param.18) | copy-start | bytes 3145732
  6.5 7.5 %copy-start.6 = (bf16[384,128]{1,0:T(8,128)(2,1)S(1)}, bf16[384,128]{1,0:T(8,128)(2,1)}, u32[]{:S(2)}) copy-start(bf16[384,128]{1,0:T(8,128)(2,1)} %param.13) | copy-start | bytes 294916
  6.5 8.3 %copy-start.5 = (bf16[384,128]{1,0:T(8,128)(2,1)S(1)}, bf16[384,128]{1,0:T(8,128)(2,1)}, u32[]{:S(2)}) copy-start(bf16[384,128]{1,0:T(8,128)(2,1)} %param.14) | copy-start | bytes 294916
  6.5 13.6 %copy-start.8 = (s32[24576]{0:T(1024)S(1)}, s32[24576]{0:T(1024)}, u32[]{:S(2)}) copy-start(s32[24576]{0:T(1024)} %param.16) | copy-start | bytes 294916
  6.5 13.7 %copy-start.7 = (bf16[384,256]{1,0:T(8,128)(2,1)S(1)}, bf16[384,256]{1,0:T(8,128)(2,1)}, u32[]{:S(2)}) copy-start(bf16[384,256]{1,0:T(8,128)(2,1)} %param.12) | copy-start | bytes 589828
  9.0 11.5 %all-to-all-start.2 = ((bf16[4,32,1024]{2,1,0:T(8,128)(2,1)}), bf16[4,32,1024]{2,1,0:T(8,128)(2,1)S(1)}, u32[]{:S(2)}, u32[]{:S(2)}) async-start(bf16[4,32,1024]{2,1,0:T(8,128)(2,1)} %pad_maximum_fusion), calls=%async_computation.2 | async-start | bytes 524288 | tf_op jit(solution)/shard_map/all_to_all | solution.py:44
  14.0 83.2 %all-gather.2.cloned.1.call-start = ((), (), s32[]{:S(2)}) async-start(), calls=%async_computation.4 | async-start | bytes 4456448 | tf_op jit(solution)/shard_map/all_gather | solution.py:45
  15.0 7.3 %collective-permute-start = (bf16[2,128,128]{2,1,0:T(8,128)(2,1)S(1)}, bf16[2,128,128]{2,1,0:T(8,128)(2,1)S(1)}, u32[]{:S(2)}, u32[]{:S(2)}) collective-permute-start(bf16[2,128,128]{2,1,0:T(8,128)(2,1)S(1)} %get-tuple-element.15), channel_id=1, source_target_pairs={{0,8},{8,16},{16,24},{24,32},{32,40},{40,48},{48,56},{56,64},{64,7... | collective-permute-start | bytes 196616 | tf_op jit(solution)/shard_map/ppermute | solution.py:114
  18.4 6.0 %collective-permute-start.1 = (bf16[2,128,128]{2,1,0:T(8,128)(2,1)S(1)}, bf16[2,128,128]{2,1,0:T(8,128)(2,1)S(1)}, u32[]{:S(2)}, u32[]{:S(2)}) collective-permute-start(bf16[2,128,128]{2,1,0:T(8,128)(2,1)S(1)} %get-tuple-element.16), channel_id=1, source_target_pairs={{8,0},{16,8},{24,16},{32,24},{40,32},{48,40},{56,48},{64,56},{72,6... | collective-permute-start | bytes 196616 | tf_op jit(solution)/shard_map/ppermute | solution.py:115
  20.5 0.7 copy-start.4
  24.5 0.7 copy-start.12
  28.0 30.0 %all-to-all-start = ((bf16[8,48,2048]{2,1,0:T(8,128)(2,1)}), bf16[8,48,2048]{2,1,0:T(8,128)(2,1)S(1)}, u32[]{:S(2)}, u32[]{:S(2)}) async-start(bf16[8,48,2048]{2,1,0:T(8,128)(2,1)} %bitcast.69), calls=%async_computation | async-start | bytes 3145728 | tf_op jit(solution)/shard_map/all_to_all | solution.py:127
  37.4 21.0 %copy-start.9 = (f32[2048]{0:T(1024)S(1)}, f32[2048]{0:T(1024)}, u32[]{:S(2)}) copy-start(f32[2048]{0:T(1024)} %param.19) | copy-start | bytes 24580
  37.4 22.2 %copy-start.11 = (f32[2048]{0:T(1024)S(1)}, f32[2048]{0:T(1024)}, u32[]{:S(2)}) copy-start(f32[2048]{0:T(1024)} %param.22) | copy-start | bytes 24580
  82.9 1.2 copy-start.3
  84.1 7.0 %collective-permute-start.2 = (bf16[384,2048]{1,0:T(8,128)(2,1)S(1)}, bf16[384,2048]{1,0:T(8,128)(2,1)S(1)}, u32[]{:S(2)}, u32[]{:S(2)}) collective-permute-start(bf16[384,2048]{1,0:T(8,128)(2,1)S(1)} %bitcast.71), channel_id=1, source_target_pairs={{0,1},{1,0},{2,3},{3,2},{4,5},{5,4},{6,7},{7,6},{8,9},{9,8},{10,11... | collective-permute-start | bytes 4718600 | tf_op jit(solution)/shard_map/ppermute | solution.py:18
  91.2 6.1 %copy-start.2 = (bf16[384,2048]{1,0:T(8,128)(2,1)}, bf16[384,2048]{1,0:T(8,128)(2,1)S(1)}, u32[]{:S(2)}) copy-start(bf16[384,2048]{1,0:T(8,128)(2,1)S(1)} %collective-permute-done.2.tokens) | copy-start | bytes 4718596
  103.3 14.6 %copy-start.1 = (bf16[2048,1024]{1,0:T(8,128)(2,1)S(1)}, bf16[2048,1024]{1,0:T(8,128)(2,1)}, u32[]{:S(2)}) copy-start(bf16[2048,1024]{1,0:T(8,128)(2,1)} %all-gather.2.cloned.1.call-done.both) | copy-start | bytes 12582916
  103.3 15.6 %collective-permute-start.3 = (bf16[384,2048]{1,0:T(8,128)(2,1)}, bf16[384,2048]{1,0:T(8,128)(2,1)S(1)}, u32[]{:S(2)}, u32[]{:S(2)}) collective-permute-start(bf16[384,2048]{1,0:T(8,128)(2,1)} %ffn_other.1), channel_id=1, source_target_pairs={{0,1},{1,0},{2,3},{3,2},{4,5},{5,4},{6,7},{7,6},{8,9},{9,8},{10,11... | collective-permute-start | bytes 4718600 | tf_op jit(solution)/shard_map/ppermute | solution.py:18
  145.7 0.7 copy-start.10
Sparse Core Ops, SparseCore 0:
  21.3 75.8 all-gather.1

commit v7 on v5

--- a/solution.py
+++ b/solution.py
@@ -161,10 +161,11 @@
     normed = exchanged(jnp.broadcast_to(own_normed[None], (8, *own_normed.shape)))
     normed = normed.reshape(-1, 2048)
     other_normed = swapped(normed)
-    other_part = ffn_down(ffn_up(other_normed, weights), weights).astype(jnp.bfloat16)
+    other_hidden = lax.optimization_barrier(ffn_up(other_normed, weights))
+    other_part = ffn_down(other_hidden, weights).astype(jnp.bfloat16)
     received = swapped(other_part)
     hidden = lax.optimization_barrier(ffn_up(normed, weights))
-    own_part = ffn_down(hidden, weights)
+    own_part = lax.optimization_barrier(ffn_down(hidden, weights))
     both_parts = (own_part + received.astype(jnp.float32)).astype(jnp.bfloat16)
     ffn_out = exchanged(both_parts.reshape(8, -1, 2048)).astype(jnp.float32).sum(axis=0)
     return (after_mix.astype(jnp.float32) + rms_scale(ffn_out, gain_ffn_out)).astype(jnp.bfloat16)

time: 153 us -> 151 us (0.987)
  matrix products: 11.9 us -> 8.88 us
    dot_general x2, matrix products: 6.72 us -> 2.09 us  [ffn_down(): lax.dot_general(hidden, both[:, 512:], across, preferred_element_type=jnp...]
    dot_general x1 -> x2, matrix products: 2.57 us -> 4.2 us  [ffn_up(): up_acts = jnp.dot(normed, both[:, :512], preferred_element_type=jnp.float32)]
where the time goes in v7:
time: 151 us; the launch traced here: 150 us
  blocking collectives  48.9 us (32%)
  starting transfers between devices  34.2 us (23%)
  waiting for transfers between devices  34 us (23%)
  between operations  13.7 us (9%)
  matrix products  8.88 us (6%)
  other arithmetic  6.43 us (4%)
  local copies, waits for them, and re-layouts  4.32 us (3%)
    all_to_all x2, blocking collectives, exchanged(): lax.all_to_all(pieces, ('sp', 'tp'), 0, 0, axis_index_groups=token_groups...  48.9 us
    all_to_all x1, waiting for transfers between devices, summed_on_arrival(): lax.all_to_all(pieces, axis, split_axis=0, concat_axis=0, tiled=True)  20.6 us
    ppermute x2, starting transfers between devices, swapped(): return lax.ppermute(shard, 'tp', [(i, i ^ 1) for i in range(8)])  15.2 us
    all_to_all x1, starting transfers between devices, summed_on_arrival(): lax.all_to_all(pieces, axis, split_axis=0, concat_axis=0, tiled=True)  9.41 us
    all_gather x1, waiting for transfers between devices, group_weights(): lax.all_gather(rows.reshape(128, 1024), 'sp', axis=0, tiled=True, axis_in...  7.14 us
    all_to_all x1, starting transfers between devices, group_weights(): lax.all_to_all(jnp.stack(halved * 2), 'sp', 0, 0, axis_index_groups=along...  5 us
    dot_general x2, matrix products, ffn_up(): up_acts = jnp.dot(normed, both[:, :512], preferred_element_type=jnp.float32)  4.2 us
    ppermute x2, waiting for transfers between devices, swapped(): return lax.ppermute(shard, 'tp', [(i, i ^ 1) for i in range(8)])  4.09 us
  transfers between devices with their start and end apart: 7, of which 5 were waited for; matrix products, arithmetic and copies ran while one was open for 7% of the time, Pallas kernels for 0%

profile of v7, /device:TPU:1, one launch (start us, length us, event | category | flops | bytes accessed | tf_op | source)
XLA Modules:
  0.0 150.4 jit_solution(14726811897370146565)
XLA Ops:
  6.5 0.9 fusion.65
  7.4 0.8 fusion.66
  8.2 0.7 pad_maximum_fusion
  9.0 5.0 %all-to-all-start.2 = ((bf16[4,32,1024]{2,1,0:T(8,128)(2,1)}), bf16[4,32,1024]{2,1,0:T(8,128)(2,1)S(1)}, u32[]{:S(2)}, u32[]{:S(2)}) async-start(bf16[4,32,1024]{2,1,0:T(8,128)(2,1)} %pad_maximum_fusion), calls=%async_computation.2 | async-start | bytes 524288 | tf_op jit(solution)/shard_map/all_to_all | solution.py:41
  14.0 0.8 fusion.54
  15.0 3.4 %collective-permute-start = (bf16[2,128,128]{2,1,0:T(8,128)(2,1)S(1)}, bf16[2,128,128]{2,1,0:T(8,128)(2,1)S(1)}, u32[]{:S(2)}, u32[]{:S(2)}) collective-permute-start(bf16[2,128,128]{2,1,0:T(8,128)(2,1)S(1)} %get-tuple-element.15), channel_id=1, source_target_pairs={{0,8},{8,16},{16,24},{24,32},{32,40},{40,48},{48,56},{56,64},{64,7... | collective-permute-start | bytes 196616 | tf_op jit(solution)/shard_map/ppermute | solution.py:64
  18.4 1.3 collective-permute-start.1
  19.7 0.4 multiply_cosine_fusion.1
  20.2 0.2 copy.26
  20.5 0.7 copy-done.1
  21.3 0.1 abs_compare_fusion
  21.4 0.2 compare_and_fusion
  21.6 0.1 copy.15
  21.8 0.2 copy.19
  22.0 0.2 copy.20
  22.2 2.1 %collective-permute-done.1 = bf16[2,128,128]{2,1,0:T(8,128)(2,1)S(1)} collective-permute-done((bf16[2,128,128]{2,1,0:T(8,128)(2,1)S(1)}, bf16[2,128,128]{2,1,0:T(8,128)(2,1)S(1)}, u32[]{:S(2)}, u32[]{:S(2)}) %collective-permute-start.1) | collective-permute-done | bytes 65568 | tf_op jit(solution)/shard_map/ppermute | solution.py:65
  24.4 0.1 pad_maximum_fusion.8
  24.5 0.1 copy.14
  24.6 0.1 copy.16
  24.8 0.4 fusion.67
  25.3 0.3 fusion.28
  25.6 0.4 fusion.27
  26.0 0.2 copy.22
  26.2 1.7 %convolution_convert_fusion.1 = bf16[384,2048]{1,0:T(8,128)(2,1)} fusion(bf16[256,2048]{1,0:T(8,128)(2,1)S(1)} %copy-done, bf16[48,8,2,128]{3,2,1,0:T(2,128)(2,1)S(1)} %bitcast.86), kind=kOutput, calls=%fused_computation.4 | convolution fusion | flops 403439616 | bytes 2818048 | tf_op jit(solution)/shard_map/dot_general | solution.py:156
  28.0 9.4 %all-to-all-start = ((bf16[8,48,2048]{2,1,0:T(8,128)(2,1)}), bf16[8,48,2048]{2,1,0:T(8,128)(2,1)S(1)}, u32[]{:S(2)}, u32[]{:S(2)}) async-start(bf16[8,48,2048]{2,1,0:T(8,128)(2,1)} %bitcast.71), calls=%async_computation | async-start | bytes 3145728 | tf_op jit(solution)/shard_map/all_to_all | solution.py:77
  37.4 20.6 %all-to-all-done = bf16[8,48,2048]{2,1,0:T(8,128)(2,1)S(1)} async-done(((bf16[8,48,2048]{2,1,0:T(8,128)(2,1)}), bf16[8,48,2048]{2,1,0:T(8,128)(2,1)S(1)}, u32[]{:S(2)}, u32[]{:S(2)}) %all-to-all-start) | async-done | bytes 1572896 | tf_op jit(solution)/shard_map/all_to_all | solution.py:77
  58.0 0.2 convert_reduce_fusion.1
  58.2 0.1 multiply_reduce_fusion.1
  58.4 1.2 fusion.31
  59.6 0.1 fusion.33
  59.7 0.2 broadcast_in_dim.23
  59.9 23.0 %all_to_all.20 = bf16[8,48,2048]{2,1,0:T(8,128)(2,1)S(1)} all-to-all(bf16[8,48,2048]{2,1,0:T(8,128)(2,1)S(1)} %broadcast_in_dim.23), channel_id=1, replica_groups={{0,2,4,6,8,10,12,14},{1,3,5,7,9,11,13,15},{16,18,20,22,24,26,28,30},{17..., dimensions={0} | all-to-all | bytes 3145728 | tf_op jit(solution)/shard_map/all_to_all | solution.py:28
  82.9 4.0 %collective-permute-start.2 = (bf16[384,2048]{1,0:T(8,128)(2,1)S(1)}, bf16[384,2048]{1,0:T(8,128)(2,1)}, u32[]{:S(2)}, u32[]{:S(2)}) collective-permute-start(bf16[384,2048]{1,0:T(8,128)(2,1)S(1)} %bitcast.73), channel_id=1, source_target_pairs={{0,1},{1,0},{2,3},{3,2},{4,5},{5,4},{6,7},{7,6},{8,9},{9,8},{10,11... | collective-permute-start | bytes 4718600 | tf_op jit(solution)/shard_map/ppermute | solution.py:15
  86.9 3.1 %collective-permute-done.2 = bf16[384,2048]{1,0:T(8,128)(2,1)} collective-permute-done((bf16[384,2048]{1,0:T(8,128)(2,1)S(1)}, bf16[384,2048]{1,0:T(8,128)(2,1)}, u32[]{:S(2)}, u32[]{:S(2)}) %collective-permute-start.2) | collective-permute-done | bytes 1572896 | tf_op jit(solution)/shard_map/ppermute | solution.py:15
  90.1 7.1 %all-gather.2.cloned.1.call-done = bf16[2048,1024]{1,0:T(8,128)(2,1)} async-done(((bf16[128,1024]{1,0:T(8,128)(2,1)}), bf16[2048,1024]{1,0:T(8,128)(2,1)}) %all-gather.2.cloned.1.call-update) | async-done | bytes 4194320 | tf_op jit(solution)/shard_map/all_gather | solution.py:42
  97.2 3.2 %fusion.21 = bf16[384,512]{1,0:T(8,128)(2,1)S(1)} fusion(bf16[384,2048]{1,0:T(8,128)(2,1)} %collective-permute-done.2, bf16[2048,1024]{1,0:T(8,128)(2,1)} %all-gather.2.cloned.1.call-done), kind=kOutput, calls=%fused_computation.19 | convolution fusion | flops 805896192 | bytes 4063232 | tf_op jit(solution)/shard_map/dot_general | solution.py:48
  100.4 0.1 copy-done.2
  100.5 1.0 convolution_convert_fusion
  101.6 11.2 %collective-permute-start.3 = (bf16[384,2048]{1,0:T(8,128)(2,1)S(1)}, bf16[384,2048]{1,0:T(8,128)(2,1)S(1)}, u32[]{:S(2)}, u32[]{:S(2)}) collective-permute-start(bf16[384,2048]{1,0:T(8,128)(2,1)S(1)} %convolution_convert_fusion), channel_id=1, source_target_pairs={{0,1},{1,0},{2,3},{3,2},{4,5},{5,4},{6,7},{7,6},{8,9},{9,8},{10,11... | collective-permute-start | bytes 4718600 | tf_op jit(solution)/shard_map/ppermute | solution.py:15
  112.7 1.0 fusion.24
  113.7 1.0 fusion.1
  114.8 0.9 collective-permute-done.3
  115.7 0.5 add_convert_fusion
  116.3 25.8 %all_to_all.21 = bf16[8,48,2048]{2,1,0:T(8,128)(2,1)S(1)} all-to-all(bf16[8,48,2048]{2,1,0:T(8,128)(2,1)S(1)} %bitcast.72), channel_id=1, replica_groups={{0,2,4,6,8,10,12,14},{1,3,5,7,9,11,13,15},{16,18,20,22,24,26,28,30},{17..., dimensions={0} | all-to-all | bytes 3145728 | tf_op jit(solution)/shard_map/all_to_all | solution.py:28
  142.1 0.2 convert_reduce_fusion
  142.3 0.1 multiply_reduce_fusion
  142.5 0.3 copy-done.8
  142.8 0.8 fusion.34
  (40 shorter events, 0.7 us)
Async XLA Ops:
  6.5 19.7 %copy-start = (bf16[256,2048]{1,0:T(8,128)(2,1)S(1)}, bf16[256,2048]{1,0:T(8,128)(2,1)}, u32[]{:S(2)}) copy-start(bf16[256,2048]{1,0:T(8,128)(2,1)} %param.18) | copy-start | bytes 3145732
  6.5 7.5 %copy-start.4 = (bf16[384,128]{1,0:T(8,128)(2,1)S(1)}, bf16[384,128]{1,0:T(8,128)(2,1)}, u32[]{:S(2)}) copy-start(bf16[384,128]{1,0:T(8,128)(2,1)} %param.13) | copy-start | bytes 294916
  6.5 8.3 %copy-start.3 = (bf16[384,128]{1,0:T(8,128)(2,1)S(1)}, bf16[384,128]{1,0:T(8,128)(2,1)}, u32[]{:S(2)}) copy-start(bf16[384,128]{1,0:T(8,128)(2,1)} %param.14) | copy-start | bytes 294916
  6.5 13.6 %copy-start.6 = (s32[24576]{0:T(1024)S(1)}, s32[24576]{0:T(1024)}, u32[]{:S(2)}) copy-start(s32[24576]{0:T(1024)} %param.16) | copy-start | bytes 294916
  6.5 13.7 %copy-start.5 = (bf16[384,256]{1,0:T(8,128)(2,1)S(1)}, bf16[384,256]{1,0:T(8,128)(2,1)}, u32[]{:S(2)}) copy-start(bf16[384,256]{1,0:T(8,128)(2,1)} %param.12) | copy-start | bytes 589828
  9.0 11.5 %all-to-all-start.2 = ((bf16[4,32,1024]{2,1,0:T(8,128)(2,1)}), bf16[4,32,1024]{2,1,0:T(8,128)(2,1)S(1)}, u32[]{:S(2)}, u32[]{:S(2)}) async-start(bf16[4,32,1024]{2,1,0:T(8,128)(2,1)} %pad_maximum_fusion), calls=%async_computation.2 | async-start | bytes 524288 | tf_op jit(solution)/shard_map/all_to_all | solution.py:41
  14.0 83.2 %all-gather.2.cloned.1.call-start = ((), (), s32[]{:S(2)}) async-start(), calls=%async_computation.4 | async-start | bytes 4456448 | tf_op jit(solution)/shard_map/all_gather | solution.py:42
  15.0 7.2 %collective-permute-start = (bf16[2,128,128]{2,1,0:T(8,128)(2,1)S(1)}, bf16[2,128,128]{2,1,0:T(8,128)(2,1)S(1)}, u32[]{:S(2)}, u32[]{:S(2)}) collective-permute-start(bf16[2,128,128]{2,1,0:T(8,128)(2,1)S(1)} %get-tuple-element.15), channel_id=1, source_target_pairs={{0,8},{8,16},{16,24},{24,32},{32,40},{40,48},{48,56},{56,64},{64,7... | collective-permute-start | bytes 196616 | tf_op jit(solution)/shard_map/ppermute | solution.py:64
  18.4 6.0 %collective-permute-start.1 = (bf16[2,128,128]{2,1,0:T(8,128)(2,1)S(1)}, bf16[2,128,128]{2,1,0:T(8,128)(2,1)S(1)}, u32[]{:S(2)}, u32[]{:S(2)}) collective-permute-start(bf16[2,128,128]{2,1,0:T(8,128)(2,1)S(1)} %get-tuple-element.16), channel_id=1, source_target_pairs={{8,0},{16,8},{24,16},{32,24},{40,32},{48,40},{56,48},{64,56},{72,6... | collective-permute-start | bytes 196616 | tf_op jit(solution)/shard_map/ppermute | solution.py:65
  20.5 0.7 copy-start.1
  24.5 0.7 copy-start.10
  28.0 30.0 %all-to-all-start = ((bf16[8,48,2048]{2,1,0:T(8,128)(2,1)}), bf16[8,48,2048]{2,1,0:T(8,128)(2,1)S(1)}, u32[]{:S(2)}, u32[]{:S(2)}) async-start(bf16[8,48,2048]{2,1,0:T(8,128)(2,1)} %bitcast.71), calls=%async_computation | async-start | bytes 3145728 | tf_op jit(solution)/shard_map/all_to_all | solution.py:77
  37.4 21.0 %copy-start.7 = (f32[2048]{0:T(1024)S(1)}, f32[2048]{0:T(1024)}, u32[]{:S(2)}) copy-start(f32[2048]{0:T(1024)} %param.19) | copy-start | bytes 24580
  37.4 22.2 %copy-start.9 = (f32[2048]{0:T(1024)S(1)}, f32[2048]{0:T(1024)}, u32[]{:S(2)}) copy-start(f32[2048]{0:T(1024)} %param.22) | copy-start | bytes 24580
  82.9 7.1 %collective-permute-start.2 = (bf16[384,2048]{1,0:T(8,128)(2,1)S(1)}, bf16[384,2048]{1,0:T(8,128)(2,1)}, u32[]{:S(2)}, u32[]{:S(2)}) collective-permute-start(bf16[384,2048]{1,0:T(8,128)(2,1)S(1)} %bitcast.73), channel_id=1, source_target_pairs={{0,1},{1,0},{2,3},{3,2},{4,5},{5,4},{6,7},{7,6},{8,9},{9,8},{10,11... | collective-permute-start | bytes 4718600 | tf_op jit(solution)/shard_map/ppermute | solution.py:15
  97.2 3.3 %copy-start.2 = (bf16[2048,1024]{1,0:T(8,128)(2,1)S(1)}, bf16[2048,1024]{1,0:T(8,128)(2,1)}, u32[]{:S(2)}) copy-start(bf16[2048,1024]{1,0:T(8,128)(2,1)} %all-gather.2.cloned.1.call-done) | copy-start | bytes 12582916
  101.6 14.2 %collective-permute-start.3 = (bf16[384,2048]{1,0:T(8,128)(2,1)S(1)}, bf16[384,2048]{1,0:T(8,128)(2,1)S(1)}, u32[]{:S(2)}, u32[]{:S(2)}) collective-permute-start(bf16[384,2048]{1,0:T(8,128)(2,1)S(1)} %convolution_convert_fusion), channel_id=1, source_target_pairs={{0,1},{1,0},{2,3},{3,2},{4,5},{5,4},{6,7},{7,6},{8,9},{9,8},{10,11... | collective-permute-start | bytes 4718600 | tf_op jit(solution)/shard_map/ppermute | solution.py:15
  142.1 0.7 copy-start.8
Sparse Core Ops, SparseCore 0:
  21.3 75.8 all-gather.1

commit v8 on v7

--- a/solution.py
+++ b/solution.py
@@ -32,20 +32,21 @@
 
 def group_weights(up_proj, down_proj):
     down_rows = down_proj.T
-    halved = [
-        jnp.concatenate([w[:, at : at + 512] for w in (up_proj, down_rows)], axis=1)
-        for at in (0, 512)
-    ]
+    pieces = jnp.concatenate(
+        [jnp.stack([w[:, :512], w[:, 512:]] * 2) for w in (up_proj, down_rows)], axis=2
+    )
     along_y = [[4 * z + y for y in range(4)] for z in range(16)]
     along_z = [[4 * z + y for z in range(16)] for y in range(4)]
-    rows = lax.all_to_all(jnp.stack(halved * 2), "sp", 0, 0, axis_index_groups=along_y, tiled=True)
+    rows = lax.all_to_all(
+        pieces, "sp", 0, 0, axis_index_groups=along_y, tiled=True
+    )
     return lax.all_gather(
         rows.reshape(128, 1024), "sp", axis=0, tiled=True, axis_index_groups=along_z
     )
 
 
 def ffn_up(normed, both):
-    up_acts = jnp.dot(normed, both[:, :512], preferred_element_type=jnp.float32)
+    up_acts = jnp.dot(normed, both, preferred_element_type=jnp.float32)
     return jnp.square(jax.nn.relu(up_acts)).astype(jnp.bfloat16)
 
 
@@ -161,10 +162,12 @@
     normed = exchanged(jnp.broadcast_to(own_normed[None], (8, *own_normed.shape)))
     normed = normed.reshape(-1, 2048)
     other_normed = swapped(normed)
-    other_hidden = lax.optimization_barrier(ffn_up(other_normed, weights))
+    first = lax.optimization_barrier(ffn_up(other_normed, weights[:, :256]))
+    second = lax.optimization_barrier(ffn_up(other_normed, weights[:, 256:512]))
+    other_hidden = jnp.concatenate([first, second], axis=1)
     other_part = ffn_down(other_hidden, weights).astype(jnp.bfloat16)
     received = swapped(other_part)
-    hidden = lax.optimization_barrier(ffn_up(normed, weights))
+    hidden = lax.optimization_barrier(ffn_up(normed, weights[:, :512]))
     own_part = lax.optimization_barrier(ffn_down(hidden, weights))
     both_parts = (own_part + received.astype(jnp.float32)).astype(jnp.bfloat16)
     ffn_out = exchanged(both_parts.reshape(8, -1, 2048)).astype(jnp.float32).sum(axis=0)

time: 151 us -> 153 us (1.013)
    slice x2 -> x0, local copies, waits for them, and re-layouts: 1.68 us -> none  [group_weights(): w[:, at:at + 512]]
    dot_general x2 -> x3, matrix products: 4.2 us -> 5.44 us  [ffn_up(): up_acts = jnp.dot(normed, both, preferred_element_type=jnp.float32)]
where the time goes in v8:
time: 153 us; the launch traced here: 152 us
  blocking collectives  48.6 us (32%)
  starting transfers between devices  34.9 us (23%)
  waiting for transfers between devices  33.4 us (22%)
  between operations  13.7 us (9%)
  matrix products  10.1 us (7%)
  other arithmetic  7.38 us (5%)
  local copies, waits for them, and re-layouts  4.03 us (3%)
    all_to_all x2, blocking collectives, exchanged(): lax.all_to_all(pieces, ('sp', 'tp'), 0, 0, axis_index_groups=token_groups...  48.6 us
    all_to_all x1, waiting for transfers between devices, summed_on_arrival(): lax.all_to_all(pieces, axis, split_axis=0, concat_axis=0, tiled=True)  20.6 us
    ppermute x2, starting transfers between devices, swapped(): return lax.ppermute(shard, 'tp', [(i, i ^ 1) for i in range(8)])  15.2 us
    all_to_all x1, starting transfers between devices, summed_on_arrival(): lax.all_to_all(pieces, axis, split_axis=0, concat_axis=0, tiled=True)  10.1 us
    all_gather x1, waiting for transfers between devices, group_weights(): lax.all_gather(rows.reshape(128, 1024), 'sp', axis=0, tiled=True, axis_in...  7.2 us
    dot_general x3, matrix products, ffn_up(): up_acts = jnp.dot(normed, both, preferred_element_type=jnp.float32)  5.44 us
    all_to_all x1, starting transfers between devices, group_weights(): lax.all_to_all(pieces, 'sp', 0, 0, axis_index_groups=along_y, tiled=True)  5 us
    ppermute x2, waiting for transfers between devices, swapped(): return lax.ppermute(shard, 'tp', [(i, i ^ 1) for i in range(8)])  4.09 us
  transfers between devices with their start and end apart: 7, of which 5 were waited for; matrix products, arithmetic and copies ran while one was open for 7% of the time, Pallas kernels for 0%

profile of v8, /device:TPU:1, one launch (start us, length us, event | category | flops | bytes accessed | tf_op | source)
XLA Modules:
  0.0 152.2 jit_solution(10841386868831102772)
XLA Ops:
  6.5 0.9 slice_bitcast_fusion.1
  7.5 0.7 maximum_maximum_fusion
  8.2 5.0 %all-to-all-start.2 = ((bf16[4,32,1024]{2,1,0:T(8,128)(2,1)}), bf16[4,32,1024]{2,1,0:T(8,128)(2,1)S(1)}, u32[]{:S(2)}, u32[]{:S(2)}) async-start(bf16[4,32,1024]{2,1,0:T(8,128)(2,1)} %maximum_maximum_fusion), calls=%async_computation.2 | async-start | bytes 524288 | tf_op jit(solution)/shard_map/all_to_all | solution.py:40
  13.2 1.8 %fusion.52 = (bf16[384,1,64]{2,0,1:T(8,128)(2,1)S(1)}, bf16[384,1,64]{2,0,1:T(8,128)(2,1)S(1)}) fusion(f32[64]{0:T(128)S(1)} %multiply_power_fusion, f32[384]{0:T(512)S(1)} %add_convert_fusion.2, bf16[384,1,128]{2,0,1:T(8,128)(2,1)} %bitcast.91), kind=kLoop, calls=%fused_computation.73 | loop fusion | flops 270336 | bytes 198400 | tf_op jit(solution)/shard_map/convert.11
  15.2 3.4 %collective-permute-start = (bf16[2,128,128]{2,1,0:T(8,128)(2,1)S(1)}, bf16[2,128,128]{2,1,0:T(8,128)(2,1)S(1)}, u32[]{:S(2)}, u32[]{:S(2)}) collective-permute-start(bf16[2,128,128]{2,1,0:T(8,128)(2,1)S(1)} %get-tuple-element.15), channel_id=1, source_target_pairs={{0,8},{8,16},{16,24},{24,32},{32,40},{40,48},{48,56},{56,64},{64,7... | collective-permute-start | bytes 196616 | tf_op jit(solution)/shard_map/ppermute | solution.py:65
  18.5 1.3 collective-permute-start.1
  19.9 0.4 multiply_cosine_fusion.1
  20.4 0.2 copy.26
  20.7 0.7 copy-done.1
  21.5 0.1 abs_compare_fusion
  21.6 0.2 compare_and_fusion
  21.8 0.1 copy.15
  22.0 0.2 copy.19
  22.2 0.2 copy.20
  22.4 1.5 collective-permute-done.1
  23.9 0.1 pad_maximum_fusion.7
  24.0 0.1 copy.14
  24.2 0.1 copy.16
  24.3 0.4 fusion.64
  24.8 0.3 fusion.23
  25.1 0.4 fusion.20
  25.6 0.2 copy.22
  25.8 1.8 %convolution_convert_fusion.1 = bf16[384,2048]{1,0:T(8,128)(2,1)} fusion(bf16[256,2048]{1,0:T(8,128)(2,1)S(1)} %copy-done, bf16[48,8,2,128]{3,2,1,0:T(2,128)(2,1)S(1)} %bitcast.90), kind=kOutput, calls=%fused_computation.4 | convolution fusion | flops 403439616 | bytes 2818048 | tf_op jit(solution)/shard_map/dot_general | solution.py:157
  27.5 10.1 %all-to-all-start = ((bf16[8,48,2048]{2,1,0:T(8,128)(2,1)}), bf16[8,48,2048]{2,1,0:T(8,128)(2,1)S(1)}, u32[]{:S(2)}, u32[]{:S(2)}) async-start(bf16[8,48,2048]{2,1,0:T(8,128)(2,1)} %bitcast.75), calls=%async_computation | async-start | bytes 3145728 | tf_op jit(solution)/shard_map/all_to_all | solution.py:78
  37.6 20.6 %all-to-all-done = bf16[8,48,2048]{2,1,0:T(8,128)(2,1)S(1)} async-done(((bf16[8,48,2048]{2,1,0:T(8,128)(2,1)}), bf16[8,48,2048]{2,1,0:T(8,128)(2,1)S(1)}, u32[]{:S(2)}, u32[]{:S(2)}) %all-to-all-start) | async-done | bytes 1572896 | tf_op jit(solution)/shard_map/all_to_all | solution.py:78
  58.2 0.2 convert_reduce_fusion.1
  58.4 0.1 multiply_reduce_fusion.1
  58.6 1.2 fusion.26
  59.8 0.1 fusion.28
  59.9 0.2 broadcast_in_dim.23
  60.1 23.0 %all_to_all.20 = bf16[8,48,2048]{2,1,0:T(8,128)(2,1)S(1)} all-to-all(bf16[8,48,2048]{2,1,0:T(8,128)(2,1)S(1)} %broadcast_in_dim.23), channel_id=1, replica_groups={{0,2,4,6,8,10,12,14},{1,3,5,7,9,11,13,15},{16,18,20,22,24,26,28,30},{17..., dimensions={0} | all-to-all | bytes 3145728 | tf_op jit(solution)/shard_map/all_to_all | solution.py:28
  83.1 4.0 %collective-permute-start.2 = (bf16[384,2048]{1,0:T(8,128)(2,1)S(1)}, bf16[384,2048]{1,0:T(8,128)(2,1)}, u32[]{:S(2)}, u32[]{:S(2)}) collective-permute-start(bf16[384,2048]{1,0:T(8,128)(2,1)S(1)} %bitcast.77), channel_id=1, source_target_pairs={{0,1},{1,0},{2,3},{3,2},{4,5},{5,4},{6,7},{7,6},{8,9},{9,8},{10,11... | collective-permute-start | bytes 4718600 | tf_op jit(solution)/shard_map/ppermute | solution.py:15
  87.1 3.1 %collective-permute-done.2 = bf16[384,2048]{1,0:T(8,128)(2,1)} collective-permute-done((bf16[384,2048]{1,0:T(8,128)(2,1)S(1)}, bf16[384,2048]{1,0:T(8,128)(2,1)}, u32[]{:S(2)}, u32[]{:S(2)}) %collective-permute-start.2) | collective-permute-done | bytes 1572896 | tf_op jit(solution)/shard_map/ppermute | solution.py:15
  90.3 7.2 %all-gather.2.cloned.1.call-done = bf16[2048,1024]{1,0:T(8,128)(2,1)} async-done(((bf16[128,1024]{1,0:T(8,128)(2,1)}), bf16[2048,1024]{1,0:T(8,128)(2,1)}) %all-gather.2.cloned.1.call-update) | async-done | bytes 4194320 | tf_op jit(solution)/shard_map/all_gather | solution.py:43
  97.5 2.4 %fusion.18 = bf16[384,256]{1,0:T(8,128)(2,1)S(1)} fusion(bf16[384,2048]{1,0:T(8,128)(2,1)} %collective-permute-done.2, bf16[2048,1024]{1,0:T(8,128)(2,1)} %all-gather.2.cloned.1.call-done), kind=kOutput, calls=%fused_computation.22 | convolution fusion | flops 402948096 | bytes 2818048 | tf_op jit(solution)/shard_map/dot_general | solution.py:49
  99.9 0.6 copy-done.2
  100.4 2.0 %fusion.19 = bf16[384,256]{1,0:T(8,128)(2,1)S(1)} fusion(bf16[384,2048]{1,0:T(8,128)(2,1)} %collective-permute-done.2, bf16[2048,1024]{1,0:T(8,128)(2,1)S(1)} %copy-done.2), kind=kOutput, calls=%fused_computation.23 | convolution fusion | flops 402948096 | bytes 2818048 | tf_op jit(solution)/shard_map/dot_general | solution.py:49
  102.5 1.0 convolution_convert_fusion
  103.5 11.2 %collective-permute-start.3 = (bf16[384,2048]{1,0:T(8,128)(2,1)S(1)}, bf16[384,2048]{1,0:T(8,128)(2,1)S(1)}, u32[]{:S(2)}, u32[]{:S(2)}) collective-permute-start(bf16[384,2048]{1,0:T(8,128)(2,1)S(1)} %convolution_convert_fusion), channel_id=1, source_target_pairs={{0,1},{1,0},{2,3},{3,2},{4,5},{5,4},{6,7},{7,6},{8,9},{9,8},{10,11... | collective-permute-start | bytes 4718600 | tf_op jit(solution)/shard_map/ppermute | solution.py:15
  114.7 1.0 fusion.13
  115.8 1.0 fusion.3
  116.8 0.9 collective-permute-done.3
  117.8 0.5 add_convert_fusion
  118.3 25.6 %all_to_all.21 = bf16[8,48,2048]{2,1,0:T(8,128)(2,1)S(1)} all-to-all(bf16[8,48,2048]{2,1,0:T(8,128)(2,1)S(1)} %bitcast.76), channel_id=1, replica_groups={{0,2,4,6,8,10,12,14},{1,3,5,7,9,11,13,15},{16,18,20,22,24,26,28,30},{17..., dimensions={0} | all-to-all | bytes 3145728 | tf_op jit(solution)/shard_map/all_to_all | solution.py:28
  143.9 0.2 convert_reduce_fusion
  144.1 0.1 multiply_reduce_fusion
  144.3 0.3 copy-done.7
  144.6 0.8 fusion.29
  (37 shorter events, 0.7 us)
Async XLA Ops:
  6.5 19.2 %copy-start = (bf16[256,2048]{1,0:T(8,128)(2,1)S(1)}, bf16[256,2048]{1,0:T(8,128)(2,1)}, u32[]{:S(2)}) copy-start(bf16[256,2048]{1,0:T(8,128)(2,1)} %param.18) | copy-start | bytes 3145732
  6.5 8.5 %copy-start.3 = (bf16[384,128]{1,0:T(8,128)(2,1)S(1)}, bf16[384,128]{1,0:T(8,128)(2,1)}, u32[]{:S(2)}) copy-start(bf16[384,128]{1,0:T(8,128)(2,1)} %param.14) | copy-start | bytes 294916
  6.5 13.7 %copy-start.5 = (s32[24576]{0:T(1024)S(1)}, s32[24576]{0:T(1024)}, u32[]{:S(2)}) copy-start(s32[24576]{0:T(1024)} %param.16) | copy-start | bytes 294916
  6.5 13.8 %copy-start.4 = (bf16[384,256]{1,0:T(8,128)(2,1)S(1)}, bf16[384,256]{1,0:T(8,128)(2,1)}, u32[]{:S(2)}) copy-start(bf16[384,256]{1,0:T(8,128)(2,1)} %param.12) | copy-start | bytes 589828
  8.2 12.4 %all-to-all-start.2 = ((bf16[4,32,1024]{2,1,0:T(8,128)(2,1)}), bf16[4,32,1024]{2,1,0:T(8,128)(2,1)S(1)}, u32[]{:S(2)}, u32[]{:S(2)}) async-start(bf16[4,32,1024]{2,1,0:T(8,128)(2,1)} %maximum_maximum_fusion), calls=%async_computation.2 | async-start | bytes 524288 | tf_op jit(solution)/shard_map/all_to_all | solution.py:40
  13.2 84.3 %all-gather.2.cloned.1.call-start = ((), (), s32[]{:S(2)}) async-start(), calls=%async_computation.4 | async-start | bytes 4456448 | tf_op jit(solution)/shard_map/all_gather | solution.py:43
  15.2 7.2 %collective-permute-start = (bf16[2,128,128]{2,1,0:T(8,128)(2,1)S(1)}, bf16[2,128,128]{2,1,0:T(8,128)(2,1)S(1)}, u32[]{:S(2)}, u32[]{:S(2)}) collective-permute-start(bf16[2,128,128]{2,1,0:T(8,128)(2,1)S(1)} %get-tuple-element.15), channel_id=1, source_target_pairs={{0,8},{8,16},{16,24},{24,32},{32,40},{40,48},{48,56},{56,64},{64,7... | collective-permute-start | bytes 196616 | tf_op jit(solution)/shard_map/ppermute | solution.py:65
  18.5 5.4 %collective-permute-start.1 = (bf16[2,128,128]{2,1,0:T(8,128)(2,1)S(1)}, bf16[2,128,128]{2,1,0:T(8,128)(2,1)S(1)}, u32[]{:S(2)}, u32[]{:S(2)}) collective-permute-start(bf16[2,128,128]{2,1,0:T(8,128)(2,1)S(1)} %get-tuple-element.16), channel_id=1, source_target_pairs={{8,0},{16,8},{24,16},{32,24},{40,32},{48,40},{56,48},{64,56},{72,6... | collective-permute-start | bytes 196616 | tf_op jit(solution)/shard_map/ppermute | solution.py:66
  20.6 0.7 copy-start.1
  24.0 0.7 copy-start.9
  27.5 30.7 %all-to-all-start = ((bf16[8,48,2048]{2,1,0:T(8,128)(2,1)}), bf16[8,48,2048]{2,1,0:T(8,128)(2,1)S(1)}, u32[]{:S(2)}, u32[]{:S(2)}) async-start(bf16[8,48,2048]{2,1,0:T(8,128)(2,1)} %bitcast.75), calls=%async_computation | async-start | bytes 3145728 | tf_op jit(solution)/shard_map/all_to_all | solution.py:78
  37.6 21.0 %copy-start.6 = (f32[2048]{0:T(1024)S(1)}, f32[2048]{0:T(1024)}, u32[]{:S(2)}) copy-start(f32[2048]{0:T(1024)} %param.19) | copy-start | bytes 24580
  37.6 22.2 %copy-start.8 = (f32[2048]{0:T(1024)S(1)}, f32[2048]{0:T(1024)}, u32[]{:S(2)}) copy-start(f32[2048]{0:T(1024)} %param.22) | copy-start | bytes 24580
  83.1 7.1 %collective-permute-start.2 = (bf16[384,2048]{1,0:T(8,128)(2,1)S(1)}, bf16[384,2048]{1,0:T(8,128)(2,1)}, u32[]{:S(2)}, u32[]{:S(2)}) collective-permute-start(bf16[384,2048]{1,0:T(8,128)(2,1)S(1)} %bitcast.77), channel_id=1, source_target_pairs={{0,1},{1,0},{2,3},{3,2},{4,5},{5,4},{6,7},{7,6},{8,9},{9,8},{10,11... | collective-permute-start | bytes 4718600 | tf_op jit(solution)/shard_map/ppermute | solution.py:15
  97.5 3.0 %copy-start.2 = (bf16[2048,1024]{1,0:T(8,128)(2,1)S(1)}, bf16[2048,1024]{1,0:T(8,128)(2,1)}, u32[]{:S(2)}) copy-start(bf16[2048,1024]{1,0:T(8,128)(2,1)} %all-gather.2.cloned.1.call-done) | copy-start | bytes 12582916
  103.5 14.3 %collective-permute-start.3 = (bf16[384,2048]{1,0:T(8,128)(2,1)S(1)}, bf16[384,2048]{1,0:T(8,128)(2,1)S(1)}, u32[]{:S(2)}, u32[]{:S(2)}) collective-permute-start(bf16[384,2048]{1,0:T(8,128)(2,1)S(1)} %convolution_convert_fusion), channel_id=1, source_target_pairs={{0,1},{1,0},{2,3},{3,2},{4,5},{5,4},{6,7},{7,6},{8,9},{9,8},{10,11... | collective-permute-start | bytes 4718600 | tf_op jit(solution)/shard_map/ppermute | solution.py:15
  143.9 0.7 copy-start.7
Sparse Core Ops, SparseCore 0:
  21.5 75.9 all-gather.1

commit v9 on v8

--- a/solution.py
+++ b/solution.py
@@ -46,7 +46,7 @@
 
 
 def ffn_up(normed, both):
-    up_acts = jnp.dot(normed, both, preferred_element_type=jnp.float32)
+    up_acts = jnp.dot(normed, both[:, :512], preferred_element_type=jnp.float32)
     return jnp.square(jax.nn.relu(up_acts)).astype(jnp.bfloat16)
 
 
@@ -162,14 +162,12 @@
     normed = exchanged(jnp.broadcast_to(own_normed[None], (8, *own_normed.shape)))
     normed = normed.reshape(-1, 2048)
     other_normed = swapped(normed)
-    first = lax.optimization_barrier(ffn_up(other_normed, weights[:, :256]))
-    second = lax.optimization_barrier(ffn_up(other_normed, weights[:, 256:512]))
-    other_hidden = jnp.concatenate([first, second], axis=1)
+    other_hidden = lax.optimization_barrier(ffn_up(other_normed, weights))
     other_part = ffn_down(other_hidden, weights).astype(jnp.bfloat16)
     received = swapped(other_part)
-    hidden = lax.optimization_barrier(ffn_up(normed, weights[:, :512]))
-    own_part = lax.optimization_barrier(ffn_down(hidden, weights))
-    both_parts = (own_part + received.astype(jnp.float32)).astype(jnp.bfloat16)
+    hidden = lax.optimization_barrier(ffn_up(normed, weights))
+    own_part = lax.optimization_barrier(ffn_down(hidden, weights).astype(jnp.bfloat16))
+    both_parts = (own_part.astype(jnp.float32) + received.astype(jnp.float32)).astype(jnp.bfloat16)
     ffn_out = exchanged(both_parts.reshape(8, -1, 2048)).astype(jnp.float32).sum(axis=0)
     return (after_mix.astype(jnp.float32) + rms_scale(ffn_out, gain_ffn_out)).astype(jnp.bfloat16)
 

time: 153 us -> 151 us (0.987)
    dot_general x3 -> x2, matrix products: 5.44 us -> 4.19 us  [ffn_up(): up_acts = jnp.dot(normed, both[:, :512], preferred_element_type=jnp.float32)]
where the time goes in v9:
time: 151 us
  blocking collectives  48.8 us (32%)
  starting transfers between devices  34.8 us (23%)
  waiting for transfers between devices  33.6 us (22%)
  between operations  13.7 us (9%)
  matrix products  8.83 us (6%)
  other arithmetic  7.52 us (5%)
  local copies, waits for them, and re-layouts  3.56 us (2%)
    all_to_all x2, blocking collectives, exchanged(): lax.all_to_all(pieces, ('sp', 'tp'), 0, 0, axis_index_groups=token_groups...  48.8 us
    all_to_all x1, waiting for transfers between devices, summed_on_arrival(): lax.all_to_all(pieces, axis, split_axis=0, concat_axis=0, tiled=True)  20.6 us
    ppermute x2, starting transfers between devices, swapped(): return lax.ppermute(shard, 'tp', [(i, i ^ 1) for i in range(8)])  15 us
    all_to_all x1, starting transfers between devices, summed_on_arrival(): lax.all_to_all(pieces, axis, split_axis=0, concat_axis=0, tiled=True)  10.1 us
    all_gather x1, waiting for transfers between devices, group_weights(): lax.all_gather(rows.reshape(128, 1024), 'sp', axis=0, tiled=True, axis_in...  7.32 us
    all_to_all x1, starting transfers between devices, group_weights(): lax.all_to_all(pieces, 'sp', 0, 0, axis_index_groups=along_y, tiled=True)  5 us
    dot_general x2, matrix products, ffn_up(): up_acts = jnp.dot(normed, both[:, :512], preferred_element_type=jnp.float32)  4.19 us
    ppermute x2, waiting for transfers between devices, swapped(): return lax.ppermute(shard, 'tp', [(i, i ^ 1) for i in range(8)])  4.13 us
  transfers between devices with their start and end apart: 7, of which 5 were waited for; matrix products, arithmetic and copies ran while one was open for 7% of the time, Pallas kernels for 0%

profile of v9, /device:TPU:1, one launch (start us, length us, event | category | flops | bytes accessed | tf_op | source)
XLA Modules:
  0.0 150.7 jit_solution(3714036413258269559)
XLA Ops:
  6.5 0.9 slice_bitcast_fusion.1
  7.5 0.7 maximum_maximum_fusion
  8.2 5.0 %all-to-all-start.2 = ((bf16[4,32,1024]{2,1,0:T(8,128)(2,1)}), bf16[4,32,1024]{2,1,0:T(8,128)(2,1)S(1)}, u32[]{:S(2)}, u32[]{:S(2)}) async-start(bf16[4,32,1024]{2,1,0:T(8,128)(2,1)} %maximum_maximum_fusion), calls=%async_computation.2 | async-start | bytes 524288 | tf_op jit(solution)/shard_map/all_to_all | solution.py:40
  13.2 1.8 %fusion.53 = (bf16[384,1,64]{2,0,1:T(8,128)(2,1)S(1)}, bf16[384,1,64]{2,0,1:T(8,128)(2,1)S(1)}) fusion(f32[64]{0:T(128)S(1)} %multiply_power_fusion, f32[384]{0:T(512)S(1)} %add_convert_fusion.2, bf16[384,1,128]{2,0,1:T(8,128)(2,1)} %bitcast.91), kind=kLoop, calls=%fused_computation.67 | loop fusion | flops 270336 | bytes 198400 | tf_op jit(solution)/shard_map/convert.11
  15.1 0.1 pad_maximum_fusion.10
  15.2 3.4 %collective-permute-start = (bf16[2,128,128]{2,1,0:T(8,128)(2,1)S(1)}, bf16[2,128,128]{2,1,0:T(8,128)(2,1)S(1)}, u32[]{:S(2)}, u32[]{:S(2)}) collective-permute-start(bf16[2,128,128]{2,1,0:T(8,128)(2,1)S(1)} %get-tuple-element.15), channel_id=1, source_target_pairs={{0,8},{8,16},{16,24},{24,32},{32,40},{40,48},{48,56},{56,64},{64,7... | collective-permute-start | bytes 196616 | tf_op jit(solution)/shard_map/ppermute | solution.py:65
  18.5 1.3 collective-permute-start.1
  19.9 0.4 multiply_cosine_fusion.1
  20.4 0.2 copy.26
  20.7 0.7 copy-done.1
  21.5 0.1 abs_compare_fusion
  21.6 0.2 compare_and_fusion
  21.8 0.1 copy.15
  22.0 0.2 copy.19
  22.2 0.2 copy.20
  22.4 1.5 collective-permute-done.1
  23.9 0.1 pad_maximum_fusion.7
  24.0 0.1 copy.14
  24.2 0.1 copy.16
  24.3 0.4 fusion.64
  24.8 0.3 fusion.27
  25.1 0.4 fusion.26
  25.6 0.2 copy.22
  25.8 1.8 %convolution_convert_fusion.2 = bf16[384,2048]{1,0:T(8,128)(2,1)} fusion(bf16[256,2048]{1,0:T(8,128)(2,1)S(1)} %copy-done, bf16[48,8,2,128]{3,2,1,0:T(2,128)(2,1)S(1)} %bitcast.90), kind=kOutput, calls=%fused_computation.5 | convolution fusion | flops 403439616 | bytes 2818048 | tf_op jit(solution)/shard_map/dot_general | solution.py:157
  27.5 10.1 %all-to-all-start = ((bf16[8,48,2048]{2,1,0:T(8,128)(2,1)}), bf16[8,48,2048]{2,1,0:T(8,128)(2,1)S(1)}, u32[]{:S(2)}, u32[]{:S(2)}) async-start(bf16[8,48,2048]{2,1,0:T(8,128)(2,1)} %bitcast.75), calls=%async_computation | async-start | bytes 3145728 | tf_op jit(solution)/shard_map/all_to_all | solution.py:78
  37.6 20.6 %all-to-all-done = bf16[8,48,2048]{2,1,0:T(8,128)(2,1)S(1)} async-done(((bf16[8,48,2048]{2,1,0:T(8,128)(2,1)}), bf16[8,48,2048]{2,1,0:T(8,128)(2,1)S(1)}, u32[]{:S(2)}, u32[]{:S(2)}) %all-to-all-start) | async-done | bytes 1572896 | tf_op jit(solution)/shard_map/all_to_all | solution.py:78
  58.2 0.2 convert_reduce_fusion.1
  58.4 0.1 multiply_reduce_fusion.1
  58.6 1.2 fusion.30
  59.8 0.1 fusion.32
  59.9 0.2 broadcast_in_dim.23
  60.1 23.0 %all_to_all.20 = bf16[8,48,2048]{2,1,0:T(8,128)(2,1)S(1)} all-to-all(bf16[8,48,2048]{2,1,0:T(8,128)(2,1)S(1)} %broadcast_in_dim.23), channel_id=1, replica_groups={{0,2,4,6,8,10,12,14},{1,3,5,7,9,11,13,15},{16,18,20,22,24,26,28,30},{17..., dimensions={0} | all-to-all | bytes 3145728 | tf_op jit(solution)/shard_map/all_to_all | solution.py:28
  83.1 4.0 %collective-permute-start.2 = (bf16[384,2048]{1,0:T(8,128)(2,1)S(1)}, bf16[384,2048]{1,0:T(8,128)(2,1)}, u32[]{:S(2)}, u32[]{:S(2)}) collective-permute-start(bf16[384,2048]{1,0:T(8,128)(2,1)S(1)} %bitcast.77), channel_id=1, source_target_pairs={{0,1},{1,0},{2,3},{3,2},{4,5},{5,4},{6,7},{7,6},{8,9},{9,8},{10,11... | collective-permute-start | bytes 4718600 | tf_op jit(solution)/shard_map/ppermute | solution.py:15
  87.1 3.1 %collective-permute-done.2 = bf16[384,2048]{1,0:T(8,128)(2,1)} collective-permute-done((bf16[384,2048]{1,0:T(8,128)(2,1)S(1)}, bf16[384,2048]{1,0:T(8,128)(2,1)}, u32[]{:S(2)}, u32[]{:S(2)}) %collective-permute-start.2) | collective-permute-done | bytes 1572896 | tf_op jit(solution)/shard_map/ppermute | solution.py:15
  90.3 7.3 %all-gather.2.cloned.1.call-done = bf16[2048,1024]{1,0:T(8,128)(2,1)} async-done(((bf16[128,1024]{1,0:T(8,128)(2,1)}), bf16[2048,1024]{1,0:T(8,128)(2,1)}) %all-gather.2.cloned.1.call-update) | async-done | bytes 4194320 | tf_op jit(solution)/shard_map/all_gather | solution.py:43
  97.6 3.2 %fusion.20 = bf16[384,512]{1,0:T(8,128)(2,1)S(1)} fusion(bf16[384,2048]{1,0:T(8,128)(2,1)} %collective-permute-done.2, bf16[2048,1024]{1,0:T(8,128)(2,1)} %all-gather.2.cloned.1.call-done), kind=kOutput, calls=%fused_computation.19 | convolution fusion | flops 805896192 | bytes 4063232 | tf_op jit(solution)/shard_map/dot_general | solution.py:49
  100.8 0.1 copy-done.9
  100.9 1.0 convolution_convert_fusion
  101.9 11.0 %collective-permute-start.3 = (bf16[384,2048]{1,0:T(8,128)(2,1)S(1)}, bf16[384,2048]{1,0:T(8,128)(2,1)S(1)}, u32[]{:S(2)}, u32[]{:S(2)}) collective-permute-start(bf16[384,2048]{1,0:T(8,128)(2,1)S(1)} %convolution_convert_fusion), channel_id=1, source_target_pairs={{0,1},{1,0},{2,3},{3,2},{4,5},{5,4},{6,7},{7,6},{8,9},{9,8},{10,11... | collective-permute-start | bytes 4718600 | tf_op jit(solution)/shard_map/ppermute | solution.py:15
  112.9 1.0 fusion.23
  114.0 1.0 convolution_convert_fusion.1
  115.0 1.0 collective-permute-done.3
  116.0 0.7 add_convert_fusion
  116.6 25.7 %all_to_all.21 = bf16[8,48,2048]{2,1,0:T(8,128)(2,1)S(1)} all-to-all(bf16[8,48,2048]{2,1,0:T(8,128)(2,1)S(1)} %bitcast.76), channel_id=1, replica_groups={{0,2,4,6,8,10,12,14},{1,3,5,7,9,11,13,15},{16,18,20,22,24,26,28,30},{17..., dimensions={0} | all-to-all | bytes 3145728 | tf_op jit(solution)/shard_map/all_to_all | solution.py:28
  142.4 0.2 convert_reduce_fusion
  142.6 0.1 multiply_reduce_fusion
  142.8 0.3 copy-done.6
  143.1 0.8 fusion.33
  (36 shorter events, 0.6 us)
Async XLA Ops:
  6.5 19.2 %copy-start = (bf16[256,2048]{1,0:T(8,128)(2,1)S(1)}, bf16[256,2048]{1,0:T(8,128)(2,1)}, u32[]{:S(2)}) copy-start(bf16[256,2048]{1,0:T(8,128)(2,1)} %param.18) | copy-start | bytes 3145732
  6.5 8.5 %copy-start.2 = (bf16[384,128]{1,0:T(8,128)(2,1)S(1)}, bf16[384,128]{1,0:T(8,128)(2,1)}, u32[]{:S(2)}) copy-start(bf16[384,128]{1,0:T(8,128)(2,1)} %param.14) | copy-start | bytes 294916
  6.5 13.7 %copy-start.4 = (s32[24576]{0:T(1024)S(1)}, s32[24576]{0:T(1024)}, u32[]{:S(2)}) copy-start(s32[24576]{0:T(1024)} %param.16) | copy-start | bytes 294916
  6.5 13.8 %copy-start.3 = (bf16[384,256]{1,0:T(8,128)(2,1)S(1)}, bf16[384,256]{1,0:T(8,128)(2,1)}, u32[]{:S(2)}) copy-start(bf16[384,256]{1,0:T(8,128)(2,1)} %param.12) | copy-start | bytes 589828
  8.2 12.4 %all-to-all-start.2 = ((bf16[4,32,1024]{2,1,0:T(8,128)(2,1)}), bf16[4,32,1024]{2,1,0:T(8,128)(2,1)S(1)}, u32[]{:S(2)}, u32[]{:S(2)}) async-start(bf16[4,32,1024]{2,1,0:T(8,128)(2,1)} %maximum_maximum_fusion), calls=%async_computation.2 | async-start | bytes 524288 | tf_op jit(solution)/shard_map/all_to_all | solution.py:40
  13.2 84.4 %all-gather.2.cloned.1.call-start = ((), (), s32[]{:S(2)}) async-start(), calls=%async_computation.4 | async-start | bytes 4456448 | tf_op jit(solution)/shard_map/all_gather | solution.py:43
  15.2 7.2 %collective-permute-start = (bf16[2,128,128]{2,1,0:T(8,128)(2,1)S(1)}, bf16[2,128,128]{2,1,0:T(8,128)(2,1)S(1)}, u32[]{:S(2)}, u32[]{:S(2)}) collective-permute-start(bf16[2,128,128]{2,1,0:T(8,128)(2,1)S(1)} %get-tuple-element.15), channel_id=1, source_target_pairs={{0,8},{8,16},{16,24},{24,32},{32,40},{40,48},{48,56},{56,64},{64,7... | collective-permute-start | bytes 196616 | tf_op jit(solution)/shard_map/ppermute | solution.py:65
  18.5 5.4 %collective-permute-start.1 = (bf16[2,128,128]{2,1,0:T(8,128)(2,1)S(1)}, bf16[2,128,128]{2,1,0:T(8,128)(2,1)S(1)}, u32[]{:S(2)}, u32[]{:S(2)}) collective-permute-start(bf16[2,128,128]{2,1,0:T(8,128)(2,1)S(1)} %get-tuple-element.16), channel_id=1, source_target_pairs={{8,0},{16,8},{24,16},{32,24},{40,32},{48,40},{56,48},{64,56},{72,6... | collective-permute-start | bytes 196616 | tf_op jit(solution)/shard_map/ppermute | solution.py:66
  20.6 0.7 copy-start.1
  24.0 0.7 copy-start.8
  27.5 30.7 %all-to-all-start = ((bf16[8,48,2048]{2,1,0:T(8,128)(2,1)}), bf16[8,48,2048]{2,1,0:T(8,128)(2,1)S(1)}, u32[]{:S(2)}, u32[]{:S(2)}) async-start(bf16[8,48,2048]{2,1,0:T(8,128)(2,1)} %bitcast.75), calls=%async_computation | async-start | bytes 3145728 | tf_op jit(solution)/shard_map/all_to_all | solution.py:78
  37.6 21.0 %copy-start.5 = (f32[2048]{0:T(1024)S(1)}, f32[2048]{0:T(1024)}, u32[]{:S(2)}) copy-start(f32[2048]{0:T(1024)} %param.19) | copy-start | bytes 24580
  37.6 22.2 %copy-start.7 = (f32[2048]{0:T(1024)S(1)}, f32[2048]{0:T(1024)}, u32[]{:S(2)}) copy-start(f32[2048]{0:T(1024)} %param.22) | copy-start | bytes 24580
  83.1 7.1 %collective-permute-start.2 = (bf16[384,2048]{1,0:T(8,128)(2,1)S(1)}, bf16[384,2048]{1,0:T(8,128)(2,1)}, u32[]{:S(2)}, u32[]{:S(2)}) collective-permute-start(bf16[384,2048]{1,0:T(8,128)(2,1)S(1)} %bitcast.77), channel_id=1, source_target_pairs={{0,1},{1,0},{2,3},{3,2},{4,5},{5,4},{6,7},{7,6},{8,9},{9,8},{10,11... | collective-permute-start | bytes 4718600 | tf_op jit(solution)/shard_map/ppermute | solution.py:15
  97.6 3.3 %copy-start.9 = (bf16[2048,1024]{1,0:T(8,128)(2,1)S(1)}, bf16[2048,1024]{1,0:T(8,128)(2,1)}, u32[]{:S(2)}) copy-start(bf16[2048,1024]{1,0:T(8,128)(2,1)} %all-gather.2.cloned.1.call-done) | copy-start | bytes 12582916
  101.9 14.1 %collective-permute-start.3 = (bf16[384,2048]{1,0:T(8,128)(2,1)S(1)}, bf16[384,2048]{1,0:T(8,128)(2,1)S(1)}, u32[]{:S(2)}, u32[]{:S(2)}) collective-permute-start(bf16[384,2048]{1,0:T(8,128)(2,1)S(1)} %convolution_convert_fusion), channel_id=1, source_target_pairs={{0,1},{1,0},{2,3},{3,2},{4,5},{5,4},{6,7},{7,6},{8,9},{9,8},{10,11... | collective-permute-start | bytes 4718600 | tf_op jit(solution)/shard_map/ppermute | solution.py:15
  142.4 0.7 copy-start.6
Sparse Core Ops, SparseCore 0:
  21.5 76.0 all-gather.1

commit v10 on v9

--- a/solution.py
+++ b/solution.py
@@ -161,13 +161,13 @@
     own_normed = rms_scale(after_mix.astype(jnp.float32), gain_ffn_in).astype(jnp.bfloat16)
     normed = exchanged(jnp.broadcast_to(own_normed[None], (8, *own_normed.shape)))
     normed = normed.reshape(-1, 2048)
-    other_normed = swapped(normed)
-    other_hidden = lax.optimization_barrier(ffn_up(other_normed, weights))
+    other_normed = [swapped(normed[:, :1024]), swapped(normed[:, 1024:])]
+    other_hidden = lax.optimization_barrier(ffn_up(jnp.concatenate(other_normed, axis=1), weights))
     other_part = ffn_down(other_hidden, weights).astype(jnp.bfloat16)
     received = swapped(other_part)
     hidden = lax.optimization_barrier(ffn_up(normed, weights))
-    own_part = lax.optimization_barrier(ffn_down(hidden, weights).astype(jnp.bfloat16))
-    both_parts = (own_part.astype(jnp.float32) + received.astype(jnp.float32)).astype(jnp.bfloat16)
+    own_part = lax.optimization_barrier(ffn_down(hidden, weights))
+    both_parts = (own_part + received.astype(jnp.float32)).astype(jnp.bfloat16)
     ffn_out = exchanged(both_parts.reshape(8, -1, 2048)).astype(jnp.float32).sum(axis=0)
     return (after_mix.astype(jnp.float32) + rms_scale(ffn_out, gain_ffn_out)).astype(jnp.bfloat16)
 

time: 151 us -> 150 us (level)
  waiting for transfers between devices: 33.6 us -> 29.6 us
  starting transfers between devices: 34.8 us -> 37 us
    ppermute x2 -> x3, starting transfers between devices: 15 us -> 17.3 us  [swapped(): return lax.ppermute(shard, 'tp', [(i, i ^ 1) for i in range(8)])]
    all_gather x1, waiting for transfers between devices: 7.32 us -> 5.07 us  [group_weights(): lax.all_gather(rows.reshape(128, 1024), 'sp', axis=0, tiled=True, axis_in...]
    ppermute x2 -> x3, waiting for transfers between devices: 4.13 us -> 2.44 us  [swapped(): return lax.ppermute(shard, 'tp', [(i, i ^ 1) for i in range(8)])]
  transfers between devices with their start and end apart: 7 -> 8, of which waited for: 5 -> 5; matrix products, arithmetic and copies ran while one was open for 7% -> 7% of each run, Pallas kernels for 0% -> 0%
where the time goes in v10:
time: 150 us
  blocking collectives  48.6 us (32%)
  starting transfers between devices  37 us (25%)
  waiting for transfers between devices  29.6 us (20%)
  between operations  13.7 us (9%)
  matrix products  8.8 us (6%)
  other arithmetic  7.39 us (5%)
  local copies, waits for them, and re-layouts  4.63 us (3%)
    all_to_all x2, blocking collectives, exchanged(): lax.all_to_all(pieces, ('sp', 'tp'), 0, 0, axis_index_groups=token_groups...  48.6 us
    all_to_all x1, waiting for transfers between devices, summed_on_arrival(): lax.all_to_all(pieces, axis, split_axis=0, concat_axis=0, tiled=True)  20.6 us
    ppermute x3, starting transfers between devices, swapped(): return lax.ppermute(shard, 'tp', [(i, i ^ 1) for i in range(8)])  17.3 us
    all_to_all x1, starting transfers between devices, summed_on_arrival(): lax.all_to_all(pieces, axis, split_axis=0, concat_axis=0, tiled=True)  10.1 us
    all_gather x1, waiting for transfers between devices, group_weights(): lax.all_gather(rows.reshape(128, 1024), 'sp', axis=0, tiled=True, axis_in...  5.07 us
    all_to_all x1, starting transfers between devices, group_weights(): lax.all_to_all(pieces, 'sp', 0, 0, axis_index_groups=along_y, tiled=True)  5 us
    dot_general x2, matrix products, ffn_up(): up_acts = jnp.dot(normed, both[:, :512], preferred_element_type=jnp.float32)  4.19 us
    ppermute x1, starting transfers between devices, padded(): before = lax.ppermute(last, axis, up)  3.37 us
  transfers between devices with their start and end apart: 8, of which 5 were waited for; matrix products, arithmetic and copies ran while one was open for 7% of the time, Pallas kernels for 0%

profile of v10, /device:TPU:1, one launch (start us, length us, event | category | flops | bytes accessed | tf_op | source)
XLA Modules:
  0.0 149.8 jit_solution(3054732231637416821)
XLA Ops:
  6.5 0.9 slice_bitcast_fusion.1
  7.5 0.7 maximum_maximum_fusion
  8.2 5.0 %all-to-all-start.2 = ((bf16[4,32,1024]{2,1,0:T(8,128)(2,1)}), bf16[4,32,1024]{2,1,0:T(8,128)(2,1)S(1)}, u32[]{:S(2)}, u32[]{:S(2)}) async-start(bf16[4,32,1024]{2,1,0:T(8,128)(2,1)} %maximum_maximum_fusion), calls=%async_computation.2 | async-start | bytes 524288 | tf_op jit(solution)/shard_map/all_to_all | solution.py:40
  13.2 1.8 %fusion.63 = (bf16[384,1,64]{2,0,1:T(8,128)(2,1)S(1)}, bf16[384,1,64]{2,0,1:T(8,128)(2,1)S(1)}) fusion(f32[64]{0:T(128)S(1)} %multiply_power_fusion, f32[384]{0:T(512)S(1)} %add_convert_fusion.2, bf16[384,1,128]{2,0,1:T(8,128)(2,1)} %bitcast.90), kind=kLoop, calls=%fused_computation.70 | loop fusion | flops 270336 | bytes 198400 | tf_op jit(solution)/shard_map/convert.11
  15.2 3.4 %collective-permute-start = (bf16[2,128,128]{2,1,0:T(8,128)(2,1)S(1)}, bf16[2,128,128]{2,1,0:T(8,128)(2,1)S(1)}, u32[]{:S(2)}, u32[]{:S(2)}) collective-permute-start(bf16[2,128,128]{2,1,0:T(8,128)(2,1)S(1)} %get-tuple-element.17), channel_id=1, source_target_pairs={{0,8},{8,16},{16,24},{24,32},{32,40},{40,48},{48,56},{56,64},{64,7... | collective-permute-start | bytes 196616 | tf_op jit(solution)/shard_map/ppermute | solution.py:65
  18.5 1.3 collective-permute-start.1
  20.0 0.7 copy-done.1
  20.8 0.2 copy.26
  20.9 0.1 abs_compare_fusion
  21.1 0.4 multiply_cosine_fusion.1
  21.6 0.2 compare_and_fusion
  21.8 0.1 copy.15
  22.0 0.2 copy.19
  22.2 0.2 copy.20
  22.4 1.5 collective-permute-done.1
  24.0 0.1 copy.14
  24.2 0.1 copy.16
  24.3 0.4 fusion.76
  24.8 0.3 fusion.37
  25.1 0.4 fusion.36
  25.6 0.2 copy.22
  25.7 1.7 %convolution_convert_fusion.1 = bf16[384,2048]{1,0:T(8,128)(2,1)} fusion(bf16[256,2048]{1,0:T(8,128)(2,1)S(1)} %copy-done, bf16[48,8,2,128]{3,2,1,0:T(2,128)(2,1)S(1)} %bitcast.89), kind=kOutput, calls=%fused_computation.4 | convolution fusion | flops 403439616 | bytes 2818048 | tf_op jit(solution)/shard_map/dot_general | solution.py:157
  27.5 10.1 %all-to-all-start = ((bf16[8,48,2048]{2,1,0:T(8,128)(2,1)}), bf16[8,48,2048]{2,1,0:T(8,128)(2,1)S(1)}, u32[]{:S(2)}, u32[]{:S(2)}) async-start(bf16[8,48,2048]{2,1,0:T(8,128)(2,1)} %bitcast.76), calls=%async_computation | async-start | bytes 3145728 | tf_op jit(solution)/shard_map/all_to_all | solution.py:78
  37.6 20.6 %all-to-all-done = bf16[8,48,2048]{2,1,0:T(8,128)(2,1)S(1)} async-done(((bf16[8,48,2048]{2,1,0:T(8,128)(2,1)}), bf16[8,48,2048]{2,1,0:T(8,128)(2,1)S(1)}, u32[]{:S(2)}, u32[]{:S(2)}) %all-to-all-start) | async-done | bytes 1572896 | tf_op jit(solution)/shard_map/all_to_all | solution.py:78
  58.2 0.2 convert_reduce_fusion.1
  58.4 0.1 multiply_reduce_fusion.1
  58.5 1.2 fusion.40
  59.8 0.1 fusion.42
  59.9 0.2 broadcast_in_dim.23
  60.1 23.0 %all_to_all.20 = bf16[8,48,2048]{2,1,0:T(8,128)(2,1)S(1)} all-to-all(bf16[8,48,2048]{2,1,0:T(8,128)(2,1)S(1)} %broadcast_in_dim.23), channel_id=1, replica_groups={{0,2,4,6,8,10,12,14},{1,3,5,7,9,11,13,15},{16,18,20,22,24,26,28,30},{17..., dimensions={0} | all-to-all | bytes 3145728 | tf_op jit(solution)/shard_map/all_to_all | solution.py:28
  83.1 0.1 fusion.75
  83.2 4.0 %collective-permute-start.2 = (bf16[384,1024]{1,0:T(8,128)(2,1)S(1)}, bf16[384,1024]{1,0:T(8,128)(2,1)S(1)}, u32[]{:S(2)}, u32[]{:S(2)}) collective-permute-start(bf16[384,1024]{1,0:T(8,128)(2,1)S(1)} %get-tuple-element.7), channel_id=1, source_target_pairs={{0,1},{1,0},{2,3},{3,2},{4,5},{5,4},{6,7},{7,6},{8,9},{9,8},{10,11... | collective-permute-start | bytes 2359304 | tf_op jit(solution)/shard_map/ppermute | solution.py:15
  87.2 1.9 %collective-permute-start.3 = (bf16[384,1024]{1,0:T(8,128)(2,1)S(1)}, bf16[384,1024]{1,0:T(8,128)(2,1)}, u32[]{:S(2)}, u32[]{:S(2)}) collective-permute-start(bf16[384,1024]{1,0:T(8,128)(2,1)S(1)} %get-tuple-element.8), channel_id=1, source_target_pairs={{0,1},{1,0},{2,3},{3,2},{4,5},{5,4},{6,7},{7,6},{8,9},{9,8},{10,11... | collective-permute-start | bytes 2359304 | tf_op jit(solution)/shard_map/ppermute | solution.py:15
  89.2 0.9 copy-done.10
  90.1 1.4 collective-permute-done.3
  91.6 5.1 %all-gather.2.cloned.1.call-done = bf16[2048,1024]{1,0:T(8,128)(2,1)} async-done(((bf16[128,1024]{1,0:T(8,128)(2,1)}), bf16[2048,1024]{1,0:T(8,128)(2,1)}) %all-gather.2.cloned.1.call-update) | async-done | bytes 4194320 | tf_op jit(solution)/shard_map/all_gather | solution.py:43
  96.6 3.2 %fusion.31 = bf16[384,512]{1,0:T(8,128)(2,1)S(1)} fusion(bf16[2048,1024]{1,0:T(8,128)(2,1)} %all-gather.2.cloned.1.call-done, bf16[384,1024]{1,0:T(8,128)(2,1)} %collective-permute-done.3, bf16[384,1024]{1,0:T(8,128)(2,1)} %copy-done.10), kind=kOutput, calls=%fused_computation.23 | convolution fusion | flops 809041920 | bytes 4063232 | tf_op jit(solution)/shard_map/dot_general | solution.py:49
  99.9 1.0 convolution_convert_fusion
  100.9 11.4 %collective-permute-start.4 = (bf16[384,2048]{1,0:T(8,128)(2,1)S(1)}, bf16[384,2048]{1,0:T(8,128)(2,1)S(1)}, u32[]{:S(2)}, u32[]{:S(2)}) collective-permute-start(bf16[384,2048]{1,0:T(8,128)(2,1)S(1)} %convolution_convert_fusion), channel_id=1, source_target_pairs={{0,1},{1,0},{2,3},{3,2},{4,5},{5,4},{6,7},{7,6},{8,9},{9,8},{10,11... | collective-permute-start | bytes 4718600 | tf_op jit(solution)/shard_map/ppermute | solution.py:15
  112.4 1.0 fusion.28
  113.4 1.0 fusion.1
  114.4 1.0 collective-permute-done.4
  115.4 0.5 add_convert_fusion
  115.9 25.6 %all_to_all.21 = bf16[8,48,2048]{2,1,0:T(8,128)(2,1)S(1)} all-to-all(bf16[8,48,2048]{2,1,0:T(8,128)(2,1)S(1)} %bitcast.77), channel_id=1, replica_groups={{0,2,4,6,8,10,12,14},{1,3,5,7,9,11,13,15},{16,18,20,22,24,26,28,30},{17..., dimensions={0} | all-to-all | bytes 3145728 | tf_op jit(solution)/shard_map/all_to_all | solution.py:28
  141.5 0.2 convert_reduce_fusion
  141.7 0.1 multiply_reduce_fusion
  141.8 0.3 copy-done.7
  142.2 0.8 fusion.43
  (41 shorter events, 0.9 us)
Async XLA Ops:
  6.5 19.2 %copy-start = (bf16[256,2048]{1,0:T(8,128)(2,1)S(1)}, bf16[256,2048]{1,0:T(8,128)(2,1)}, u32[]{:S(2)}) copy-start(bf16[256,2048]{1,0:T(8,128)(2,1)} %param.18) | copy-start | bytes 3145732
  6.5 8.5 %copy-start.3 = (bf16[384,128]{1,0:T(8,128)(2,1)S(1)}, bf16[384,128]{1,0:T(8,128)(2,1)}, u32[]{:S(2)}) copy-start(bf16[384,128]{1,0:T(8,128)(2,1)} %param.14) | copy-start | bytes 294916
  6.5 13.3 %copy-start.5 = (s32[24576]{0:T(1024)S(1)}, s32[24576]{0:T(1024)}, u32[]{:S(2)}) copy-start(s32[24576]{0:T(1024)} %param.16) | copy-start | bytes 294916
  6.5 14.2 %copy-start.4 = (bf16[384,256]{1,0:T(8,128)(2,1)S(1)}, bf16[384,256]{1,0:T(8,128)(2,1)}, u32[]{:S(2)}) copy-start(bf16[384,256]{1,0:T(8,128)(2,1)} %param.12) | copy-start | bytes 589828
  8.2 11.8 %all-to-all-start.2 = ((bf16[4,32,1024]{2,1,0:T(8,128)(2,1)}), bf16[4,32,1024]{2,1,0:T(8,128)(2,1)S(1)}, u32[]{:S(2)}, u32[]{:S(2)}) async-start(bf16[4,32,1024]{2,1,0:T(8,128)(2,1)} %maximum_maximum_fusion), calls=%async_computation.2 | async-start | bytes 524288 | tf_op jit(solution)/shard_map/all_to_all | solution.py:40
  13.2 83.4 %all-gather.2.cloned.1.call-start = ((), (), s32[]{:S(2)}) async-start(), calls=%async_computation.4 | async-start | bytes 4456448 | tf_op jit(solution)/shard_map/all_gather | solution.py:43
  15.2 7.2 %collective-permute-start = (bf16[2,128,128]{2,1,0:T(8,128)(2,1)S(1)}, bf16[2,128,128]{2,1,0:T(8,128)(2,1)S(1)}, u32[]{:S(2)}, u32[]{:S(2)}) collective-permute-start(bf16[2,128,128]{2,1,0:T(8,128)(2,1)S(1)} %get-tuple-element.17), channel_id=1, source_target_pairs={{0,8},{8,16},{16,24},{24,32},{32,40},{40,48},{48,56},{56,64},{64,7... | collective-permute-start | bytes 196616 | tf_op jit(solution)/shard_map/ppermute | solution.py:65
  18.5 5.4 %collective-permute-start.1 = (bf16[2,128,128]{2,1,0:T(8,128)(2,1)S(1)}, bf16[2,128,128]{2,1,0:T(8,128)(2,1)S(1)}, u32[]{:S(2)}, u32[]{:S(2)}) collective-permute-start(bf16[2,128,128]{2,1,0:T(8,128)(2,1)S(1)} %get-tuple-element.18), channel_id=1, source_target_pairs={{8,0},{16,8},{24,16},{32,24},{40,32},{48,40},{56,48},{64,56},{72,6... | collective-permute-start | bytes 196616 | tf_op jit(solution)/shard_map/ppermute | solution.py:66
  20.0 0.7 copy-start.1
  24.0 0.7 copy-start.9
  27.5 30.7 %all-to-all-start = ((bf16[8,48,2048]{2,1,0:T(8,128)(2,1)}), bf16[8,48,2048]{2,1,0:T(8,128)(2,1)S(1)}, u32[]{:S(2)}, u32[]{:S(2)}) async-start(bf16[8,48,2048]{2,1,0:T(8,128)(2,1)} %bitcast.76), calls=%async_computation | async-start | bytes 3145728 | tf_op jit(solution)/shard_map/all_to_all | solution.py:78
  37.6 21.0 %copy-start.6 = (f32[2048]{0:T(1024)S(1)}, f32[2048]{0:T(1024)}, u32[]{:S(2)}) copy-start(f32[2048]{0:T(1024)} %param.19) | copy-start | bytes 24580
  37.6 22.2 %copy-start.8 = (f32[2048]{0:T(1024)S(1)}, f32[2048]{0:T(1024)}, u32[]{:S(2)}) copy-start(f32[2048]{0:T(1024)} %param.22) | copy-start | bytes 24580
  83.2 5.9 %collective-permute-start.2 = (bf16[384,1024]{1,0:T(8,128)(2,1)S(1)}, bf16[384,1024]{1,0:T(8,128)(2,1)S(1)}, u32[]{:S(2)}, u32[]{:S(2)}) collective-permute-start(bf16[384,1024]{1,0:T(8,128)(2,1)S(1)} %get-tuple-element.7), channel_id=1, source_target_pairs={{0,1},{1,0},{2,3},{3,2},{4,5},{5,4},{6,7},{7,6},{8,9},{9,8},{10,11... | collective-permute-start | bytes 2359304 | tf_op jit(solution)/shard_map/ppermute | solution.py:15
  87.2 4.3 %collective-permute-start.3 = (bf16[384,1024]{1,0:T(8,128)(2,1)S(1)}, bf16[384,1024]{1,0:T(8,128)(2,1)}, u32[]{:S(2)}, u32[]{:S(2)}) collective-permute-start(bf16[384,1024]{1,0:T(8,128)(2,1)S(1)} %get-tuple-element.8), channel_id=1, source_target_pairs={{0,1},{1,0},{2,3},{3,2},{4,5},{5,4},{6,7},{7,6},{8,9},{9,8},{10,11... | collective-permute-start | bytes 2359304 | tf_op jit(solution)/shard_map/ppermute | solution.py:15
  89.2 0.9 copy-start.10
  96.6 3.3 %copy-start.2 = (bf16[2048,1024]{1,0:T(8,128)(2,1)S(1)}, bf16[2048,1024]{1,0:T(8,128)(2,1)}, u32[]{:S(2)}) copy-start(bf16[2048,1024]{1,0:T(8,128)(2,1)} %all-gather.2.cloned.1.call-done) | copy-start | bytes 12582916
  100.9 14.4 %collective-permute-start.4 = (bf16[384,2048]{1,0:T(8,128)(2,1)S(1)}, bf16[384,2048]{1,0:T(8,128)(2,1)S(1)}, u32[]{:S(2)}, u32[]{:S(2)}) collective-permute-start(bf16[384,2048]{1,0:T(8,128)(2,1)S(1)} %convolution_convert_fusion), channel_id=1, source_target_pairs={{0,1},{1,0},{2,3},{3,2},{4,5},{5,4},{6,7},{7,6},{8,9},{9,8},{10,11... | collective-permute-start | bytes 4718600 | tf_op jit(solution)/shard_map/ppermute | solution.py:15
  141.5 0.7 copy-start.7
Sparse Core Ops, SparseCore 0:
  20.8 75.7 all-gather.1
